TPU v7x, 32 devices: a whole 2x2x4 slice. The times are simulated.
32 devices in a mesh: sp: 8 (over z, x), dp: 4 (over y, core).
Axes of the slice: x: 2, y: 2, z: 4, core: 2. Of those that a mesh axis runs over, the one named last changes fastest.
Arguments:
- layer_activity: bfloat16 [4, 1024, 2048], P('dp', 'sp'), may hold values from -6 to 6
- writer_matrix: bfloat16 [2048, 256], P('dp'), may hold values from -0.125 to 0.125
- reader_matrix: bfloat16 [2048, 256], P('dp'), may hold values from -0.125 to 0.125
- source_unfiltered: bfloat16 [4, 1024, 2048], P('dp', 'sp'), may hold values from -6 to 6
- switch_raw_signal: bfloat16 [4, 1024, 2048], P('dp', 'sp'), may hold values from -6 to 6
- saved_result: bfloat16 [4, 1024, 2048], P('dp', 'sp'), may hold values from -6 to 6
- final_adjoint: bfloat16 [4, 1024, 2048], P('dp', 'sp'), may hold values from -6 to 6
- delta_raw: bfloat16 [4, 1024, 32], P('dp', 'sp'), may hold values from -4 to 4
- extra_logdrop: float32 [4, 1024, 32], P('dp', None, 'sp'), may hold values from 0 to 2.1
- source_filter_coefs: float32 [5, 2048], P(None, 'sp'), may hold values from -2.5 to 2.5
- writer_filter_coefs: float32 [5, 256], replicated, may hold values from -2.5 to 2.5
- reader_filter_coefs: float32 [5, 256], replicated, may hold values from -2.5 to 2.5
- delta_offset: float32 [32], P('sp'), may hold values from -7.5 to -6
- fading_exponents: float32 [32], P('sp'), may hold values from -6 to 3.4
- direct_factor: float32 [32], P('sp'), may hold values from 0.1 to 1.9
- rescale_factor: float32 [2048], replicated, may hold values from 0.1 to 1.9
Outputs:
- d_hidden: bfloat16 [4, 1024, 2048], P('dp', 'sp')
- d_x_raw: bfloat16 [4, 1024, 2048], P('dp', 'sp')
- d_gate: bfloat16 [4, 1024, 2048], P('dp', 'sp')
- d_dt_raw: bfloat16 [4, 1024, 32], P('dp', 'sp')
- d_w_b: float32 [2048, 256], P('dp')
- d_w_c: float32 [2048, 256], P('dp')
All inputs are finite; a program needn't handle non-finite values.
Results may differ from a plain program's by a relative error of at most 0.012.
Values may be sent and summed in bfloat16 or wider, within the bound.
No kernel may reach another device: no remote copies, remote signals or barrier semaphores. Data moves between devices by JAX's collectives and lax.ppermute only.
A program may use at most 128 MiB of HBM per device.

v0:
```python
import functools

import jax
import jax.numpy as jnp
from jax import lax
from jax.experimental import pallas as pl
from jax.experimental.pallas import tpu as pltpu
from jax.sharding import PartitionSpec as P


HEADS = 32
HEAD_DIM = 64
STATE = 128
GROUPS = 2
NORM_GROUPS = 8
CONV_K = 5
BLOCK = 128
INNER = 2048
EXTRA = 16
ROWS = 8

EPSILON = 1e-06
f32 = jnp.float32
bf16 = jnp.bfloat16


def nn(a, b, **kw):
    return lax.dot_general(a, b, (((1,), (0,)), ((), ())), preferred_element_type=f32, **kw)


def nt(a, b, **kw):
    return lax.dot_general(a, b, (((1,), (1,)), ((), ())), preferred_element_type=f32, **kw)


def tn(a, b, **kw):
    return lax.dot_general(a, b, (((0,), (0,)), ((), ())), preferred_element_type=f32, **kw)


def pack_rows(rows, width):
    heads = rows.shape[0]
    if width >= BLOCK:
        per = width // BLOCK
        lines = [
            jnp.concatenate([rows[i * per + j : i * per + j + 1] for j in range(per)], axis=1)
            for i in range(heads // per)
        ]
    else:
        lines = [rows[:, i * width : (i + 1) * width] for i in range(BLOCK // width)]
    spare = EXTRA - sum(line.shape[0] for line in lines)
    return jnp.concatenate(lines + [jnp.zeros((spare, width), rows.dtype)], axis=0)


def unpack_rows(lines, heads, width):
    if width >= BLOCK:
        per = width // BLOCK
        rows = [
            lines[i : i + 1, j * BLOCK : (j + 1) * BLOCK]
            for i in range(heads // per)
            for j in range(per)
        ]
    else:
        rows = [jnp.concatenate([lines[i : i + 1] for i in range(BLOCK // width)], axis=1)]
    return jnp.concatenate(rows + [jnp.zeros((ROWS - heads, BLOCK), lines.dtype)], axis=0)


def prep_kernel(saved_ref, switch_ref, final_ref, scale_ref, x_ref, dt_ref, out_ref, gate_ref):
    chunks, _, width = out_ref.shape
    cols = INNER // NORM_GROUPS
    heads = width // HEAD_DIM
    first_row = pl.program_id(0) * chunks * heads
    row = lax.broadcasted_iota(jnp.int32, (max(ROWS, chunks * heads), HEADS), 0)
    pick = (lax.broadcasted_iota(jnp.int32, row.shape, 1) == row + first_row).astype(bf16)
    dt_rows = nt(pick, dt_ref[...])
    for n in range(saved_ref.shape[1] // cols):
        at = slice(n * cols, (n + 1) * cols)
        values = saved_ref[:, at].astype(f32)
        switch = switch_ref[:, at].astype(f32)
        cot = final_ref[:, at].astype(f32) * scale_ref[:, at]
        sig = 1.0 / (1.0 + jnp.exp(-switch))
        silu = switch * sig
        g = values * silu
        inv = lax.rsqrt(jnp.mean(g * g, axis=-1, keepdims=True) + EPSILON)
        scaled = g * inv
        d_g = inv * (cot - scaled * jnp.mean(cot * scaled, axis=-1, keepdims=True))
        d_y = (d_g * silu).astype(bf16)
        gate_ref[:, at] = (d_g * values * (sig * (1.0 + switch * (1.0 - sig)))).astype(bf16)
        for c in range(cols // width):
            i = n * (cols // width) + c
            out_ref[i, :BLOCK, :] = x_ref[:, i * width : (i + 1) * width]
            out_ref[i, BLOCK : 2 * BLOCK, :] = d_y[:, c * width : (c + 1) * width]
            out_ref[i, 2 * BLOCK :, :] = pack_rows(
                dt_rows[i * heads : (i + 1) * heads], width
            ).astype(bf16)


def proj_kernel(at_ref, act_ref, *refs):
    count = len(refs) - 2
    own_ref, other_ref = refs[count:]
    size = act_ref.shape[1] // count
    total = jnp.zeros((act_ref.shape[0], refs[0].shape[1]), f32)
    for k in range(count):
        start = pl.multiple_of((at_ref[0] ^ k) * size, size)
        total = total + nn(act_ref[:, pl.ds(start, size)], refs[k][...])
    wide = total.shape[1] // GROUPS
    low = total[:, :wide].astype(bf16)
    high = total[:, wide:].astype(bf16)
    is_low = jnp.broadcast_to(at_ref[2], low.shape) == 0
    own_ref[...] = jnp.where(is_low, low, high)
    other_ref[...] = jnp.where(is_low, high, low)


def hidden_kernel(at_ref, own_ref, other_ref, *refs):
    count = len(refs) - 1
    out_ref = refs[count]
    size = out_ref.shape[1] // count
    own = own_ref[...]
    other = other_ref[...]
    is_low = jnp.broadcast_to(at_ref[2], own.shape) == 0
    both = jnp.concatenate(
        [jnp.where(is_low, own, other), jnp.where(is_low, other, own)], axis=1
    )
    for k in range(count):
        start = pl.multiple_of((at_ref[0] ^ k) * size, size)
        out_ref[:, pl.ds(start, size)] = nt(both, refs[k][...]).astype(bf16)


def weight_kernel(dp, at_ref, *refs):
    grad_refs = refs[:dp]
    act_refs = refs[dp : 3 * dp]
    out_refs = refs[3 * dp : -1]
    total_ref = refs[-1]
    total = None
    for k in range(dp):
        for part in range(2):
            term = tn(act_refs[part * dp + k][...], grad_refs[k][part])
            total = term if total is None else total + term
    total_ref[...] = total
    size = out_refs[0].shape[0]
    for k, out_ref in enumerate(out_refs):
        start = pl.multiple_of((at_ref[3] ^ k) * size, size)
        out_ref[...] = total_ref[pl.ds(start, size), :].astype(bf16)


def spread_kernel(half, at_ref, *refs):
    outs = refs[2 * half :]
    size = refs[0].shape[0]
    for part in range(2):
        group = at_ref[2] if part == 0 else 1 - at_ref[2]
        lanes = pl.ds(pl.multiple_of(group * STATE, STATE), STATE)
        for k in range(half):
            rows = pl.ds(pl.multiple_of((at_ref[3] ^ k) * size, size), size)
            chunk = refs[part * half + k][...].astype(f32)
            outs[0][rows, lanes] = chunk[:, :STATE]
            outs[1][rows, lanes] = chunk[:, STATE:]


def unpack_kernel(back_ref, dx_ref, dt_ref):
    devices, _, width = back_ref.shape
    heads = width // HEAD_DIM
    rows = []
    for i in range(devices):
        dx_ref[:, i * width : (i + 1) * width] = back_ref[i, :BLOCK, :]
        rows.append(unpack_rows(back_ref[i, BLOCK:, :].astype(f32), heads, width)[:heads])
    dt_ref[...] = jnp.concatenate(rows, axis=0).T.astype(bf16)


def mixer_kernel(
    devices,
    at_ref,
    x_ref,
    drop_ref,
    prm_ref,
    skip_ref,
    xw_ref,
    bcw_ref,
    *refs,
):
    bc_refs = refs[:devices]
    out_ref = refs[devices]
    dbc_refs = refs[devices + 1 : devices + 1 + devices // 2]
    mixer_body(at_ref, x_ref, drop_ref, prm_ref, skip_ref, xw_ref, bcw_ref, bc_refs, out_ref, dbc_refs, *refs[devices + 1 + devices // 2 :])


def split(value, count):
    terms = []
    for _ in range(count):
        terms.append(value.astype(bf16))
        value = value - terms[-1].astype(f32)
    return terms


def mixer_body(
    at_ref,
    x_ref,
    drop_ref,
    prm_ref,
    skip_ref,
    xw_ref,
    bcw_ref,
    bc_refs,
    out_ref,
    dbc_refs,
    xpad,
    bcpad,
    u_s,
    us_s,
    kcs_s,
    kr_s,
    row_s,
    wide_s,
    dr_s,
    gg_s,
    st_s,
    car_s,
    sel_s,
):
    blocks, _, width = x_ref.shape
    heads = width // HEAD_DIM
    pad = 8
    lanes = min(width, BLOCK)
    per = lanes // HEAD_DIM
    all_rows = blocks * ROWS

    def triangle(include):
        r = lax.broadcasted_iota(jnp.int32, (BLOCK, BLOCK), 0)
        c = lax.broadcasted_iota(jnp.int32, (BLOCK, BLOCK), 1)
        return jnp.where(include(r, c), 1.0, 0.0).astype(bf16)

    def expand(count):
        shape = (count * ROWS, width)
        r = lax.broadcasted_iota(jnp.int32, shape, 0) % ROWS
        c = lax.broadcasted_iota(jnp.int32, shape, 1) // HEAD_DIM
        return jnp.where(r == c, 1.0, 0.0)

    r = lax.broadcasted_iota(jnp.int32, (5 * width, BLOCK), 0)
    c = lax.broadcasted_iota(jnp.int32, (5 * width, BLOCK), 1)
    base = jnp.where(r < 2 * width, 0, jnp.where(r < 4 * width, ROWS, 2 * ROWS))
    sel_s[...] = jnp.where(c == base + (r % width) // HEAD_DIM, 1.0, 0.0).astype(bf16)

    xpad[0:pad, :] = jnp.zeros((pad, width), f32)
    xpad[pad + blocks * BLOCK :, :] = jnp.zeros((pad, width), f32)
    bcpad[0:pad, :] = jnp.zeros((pad, 2 * STATE), f32)
    bcpad[pad + blocks * BLOCK :, :] = jnp.zeros((pad, 2 * STATE), f32)

    def load_block(b, _):
        at = pl.multiple_of(b * BLOCK, BLOCK) + pad
        xpad[pl.ds(at, BLOCK), :] = x_ref[b, :BLOCK, :].astype(f32)
        row_s[0, b] = unpack_rows(x_ref[b, 2 * BLOCK :, :].astype(f32), heads, width) + prm_ref[0]
        return 0

    lax.fori_loop(0, blocks, load_block, 0)
    for k, bc_ref in enumerate(bc_refs):
        at = pl.multiple_of((at_ref[1] ^ k) * BLOCK, BLOCK) + pad
        bcpad[pl.ds(at, BLOCK), :] = bc_ref[...].astype(f32)

    raw = row_s[0].reshape(all_rows, BLOCK)
    dt = jnp.maximum(raw, 0.0) + jnp.log1p(jnp.exp(-jnp.abs(raw)))
    fade = jnp.exp(prm_ref[1])
    rate = (dt.reshape(blocks, ROWS, BLOCK) * fade[None] + drop_ref[...]).reshape(all_rows, BLOCK)
    sums = nn(jnp.concatenate(split(rate, 3), axis=0), triangle(lambda r, c: r <= c))
    cum = sums[:all_rows] + sums[all_rows : 2 * all_rows] + sums[2 * all_rows :]
    total = cum[:, BLOCK - 1 :]
    row_s[0] = dt.reshape(blocks, ROWS, BLOCK)
    row_s[1] = cum.reshape(blocks, ROWS, BLOCK)
    row_s[2] = jnp.exp(-cum).reshape(blocks, ROWS, BLOCK)
    row_s[3] = jnp.exp(cum - total).reshape(blocks, ROWS, BLOCK)
    row_s[4] = (1.0 / (1.0 + jnp.exp(-raw))).reshape(blocks, ROWS, BLOCK)

    def conv(pad_ref, b, w_ref, flip):
        win = pad_ref[pl.ds(pl.multiple_of(b * BLOCK, BLOCK), BLOCK + 2 * pad), :]
        total = None
        for k in range(CONV_K):
            shift = (CONV_K - 1) // 2 - k
            moved = win if shift == 0 else pltpu.roll(win, shift % (BLOCK + 2 * pad), 0)
            tap = w_ref[CONV_K - 1 - k : CONV_K - k, :] if flip else w_ref[k : k + 1, :]
            term = moved[pad : pad + BLOCK] * tap
            total = term if total is None else total + term
        return total

    def first(b, _):
        pre = conv(bcpad, b, bcw_ref, False)
        sig = 1.0 / (1.0 + jnp.exp(-pre))
        act = (pre * sig).astype(bf16)
        kcs_s[b] = sig * (1.0 + pre * (1.0 - sig))
        kr_s[b] = act
        pre = conv(xpad, b, xw_ref, False)
        sig = 1.0 / (1.0 + jnp.exp(-pre))
        u = pre * sig
        u_s[b] = u
        us_s[b] = sig * (1.0 + pre * (1.0 - sig))
        rows = jnp.concatenate([row_s[0, b], row_s[2, b], row_s[3, b]], axis=1)
        wide = tn(jnp.concatenate(split(rows, 3), axis=0), expand(3).astype(bf16))
        wide_s[b] = wide
        w_in = wide[BLOCK : 2 * BLOCK]
        w_out = wide[2 * BLOCK :]
        driven = u * wide[:BLOCK]
        g = x_ref[b, BLOCK : 2 * BLOCK, :].astype(f32)
        d_io = jnp.concatenate([driven * w_out, driven * w_in], axis=1).astype(bf16)
        g_io = jnp.concatenate([g * w_in, g * w_out], axis=1).astype(bf16)
        dr_s[b] = d_io
        gg_s[b] = g_io
        st_s[b, :, : 2 * width] = tn(act[:, :STATE], d_io)
        st_s[b, :, 2 * width :] = tn(act[:, STATE:], g_io)
        return 0

    lax.fori_loop(0, blocks, first, 0)

    def scan(slot, back):
        def step(i, carry):
            b = blocks - 1 - i if back else i
            at = slice(slot * width, (slot + 1) * width)
            car_s[b, :, at] = carry.astype(bf16)
            decay = wide_s[b][2 * BLOCK - 1 : 2 * BLOCK]
            return carry * decay + st_s[b, :, at]

        lax.fori_loop(0, blocks, step, jnp.zeros((STATE, width), f32))

    scan(0, False)
    scan(1, True)
    scan(2, True)
    scan(3, False)

    def second(b, _):
        act = kr_s[b]
        keys = act[:, :STATE]
        reads = act[:, STATE:]
        u = u_s[b]
        g16 = x_ref[b, BLOCK : 2 * BLOCK, :]
        cum = row_s[1, b]
        cum_t = cum.T
        wide = wide_s[b]
        w_dt = wide[:BLOCK]
        w_in = wide[BLOCK : 2 * BLOCK]
        w_out = wide[2 * BLOCK :]
        driven = (u * w_dt).astype(bf16)
        d_io = dr_s[b]
        g_io = gg_s[b]
        carry = car_s[b]
        c_s = carry[:, : 2 * width]
        c_g = carry[:, 2 * width :]
        y = nn(reads, c_s)
        c = nn(keys, c_g)
        d_r = nt(g_io, c_s)
        d_k = nt(d_io, c_g)
        scores = nt(keys, reads)
        upper = lax.broadcasted_iota(jnp.int32, (BLOCK, BLOCK), 0) > lax.broadcasted_iota(
            jnp.int32, (BLOCK, BLOCK), 1
        )
        lane = lax.broadcasted_iota(jnp.int32, (BLOCK, lanes), 1) // HEAD_DIM
        column = lax.broadcasted_iota(jnp.int32, (BLOCK, BLOCK), 1)
        row = lax.broadcasted_iota(jnp.int32, (ROWS, BLOCK), 0)
        d_scores = None
        d_driven = []
        by_key = jnp.zeros((BLOCK, BLOCK), f32)
        by_read = jnp.zeros((ROWS, BLOCK), f32)
        none = jnp.zeros((BLOCK, lanes), bf16)
        for p in range(width // lanes):
            at = slice(p * lanes, (p + 1) * lanes)
            g_p = g16[:, at]
            d_p = driven[:, at]
            gu = nt(
                jnp.concatenate([jnp.where(lane == j, d_p, none) for j in range(per)], axis=0), g_p
            )
            s_p = []
            for j in range(per):
                h = p * per + j
                decay = jnp.exp(-jnp.abs(cum_t[:, h : h + 1] - cum[h : h + 1, :]))
                gu_h = gu[j * BLOCK : (j + 1) * BLOCK]
                s = scores * decay
                term = gu_h * decay
                d_scores = term if d_scores is None else d_scores + term
                z = s * gu_h
                z = jnp.where(upper, z, -z)
                by_key = jnp.where(column == h, jnp.sum(z, axis=1, keepdims=True), by_key)
                by_read = jnp.where(row == h, jnp.sum(z, axis=0, keepdims=True), by_read)
                s_p.append(s.astype(bf16))
            d_driven.append(
                nn(
                    jnp.concatenate(s_p, axis=1),
                    jnp.concatenate([jnp.where(lane == j, g_p, none) for j in range(per)], axis=0),
                )
            )
        ds16 = d_scores.astype(bf16)
        d_k = d_k + nn(ds16, reads)
        d_r = d_r + tn(ds16, keys)
        c_x = c[:, :width]
        c_y = c[:, width:]
        d_dr = jnp.concatenate(d_driven, axis=1) + w_out * c_x + w_in * c_y
        prefix = d_io[:, :width].astype(f32) * c_x + g_io[:, width:].astype(f32) * y[:, width:]
        suffix = g_io[:, :width].astype(f32) * y[:, :width] + d_io[:, width:].astype(f32) * c_y
        sums = nn(
            jnp.concatenate(
                split(suffix - prefix, 2) + split(prefix, 2) + [(d_dr * u).astype(bf16)], axis=1
            ),
            sel_s[...],
        )
        sums = sums.T
        by_key = by_key.T
        through = jnp.sum(c_s.astype(f32) * c_g.astype(f32), axis=0, keepdims=True)
        through = (through[:, :width] + through[:, width:]) * wide[2 * BLOCK - 1 : 2 * BLOCK]
        through = jnp.sum(expand(1) * through, axis=1, keepdims=True)
        before = jnp.sum(sums[ROWS : 2 * ROWS], axis=1, keepdims=True) + through
        row_s[5, b] = sums[:ROWS] + by_key[:ROWS] - by_read
        row_s[2, b] = jnp.broadcast_to(before, (ROWS, BLOCK))
        row_s[3, b] = sums[2 * ROWS : 3 * ROWS]
        d_u = d_dr * w_dt + g16.astype(f32) * skip_ref[...]
        at = pl.multiple_of(b * BLOCK, BLOCK) + pad
        xpad[pl.ds(at, BLOCK), :] = d_u * us_s[b]
        bcpad[pl.ds(at, BLOCK), :] = jnp.concatenate([d_k, d_r], axis=1) * kcs_s[b]
        return 0

    lax.fori_loop(0, blocks, second, 0)

    sums = nn(
        jnp.concatenate(split(row_s[5].reshape(all_rows, BLOCK), 3), axis=0),
        triangle(lambda r, c: r >= c),
    )
    sums = sums[:all_rows] + sums[all_rows : 2 * all_rows] + sums[2 * all_rows :]
    d_rate = -(sums.reshape(blocks, ROWS, BLOCK) + row_s[2])
    row_s[0] = (row_s[3] + d_rate * fade[None]) * row_s[4]

    for k, dbc_ref in enumerate(dbc_refs):
        for part in range(2):
            b = at_ref[1] ^ k if part == 0 else at_ref[1] ^ k ^ len(dbc_refs)
            dbc_ref[part] = conv(bcpad, b, bcw_ref, True).astype(bf16)

    def last(b, _):
        out_ref[b, :BLOCK, :] = conv(xpad, b, xw_ref, True).astype(bf16)
        out_ref[b, BLOCK:, :] = pack_rows(row_s[0, b][:heads], width).astype(bf16)
        return 0

    lax.fori_loop(0, blocks, last, 0)


def vmem():
    return pl.BlockSpec(memory_space=pltpu.VMEM)


def smem():
    return pl.BlockSpec(memory_space=pltpu.SMEM)


def run_mixer(at, x, drop, prm, skip, xw, bcw, bc):
    blocks, _, width = x.shape
    length = blocks * BLOCK
    scratch = [
        pltpu.VMEM((length + 16, width), f32),
        pltpu.VMEM((length + 16, 2 * STATE), f32),
        pltpu.VMEM((blocks, BLOCK, width), f32),
        pltpu.VMEM((blocks, BLOCK, width), f32),
        pltpu.VMEM((blocks, BLOCK, 2 * STATE), f32),
        pltpu.VMEM((blocks, BLOCK, 2 * STATE), bf16),
        pltpu.VMEM((6, blocks, ROWS, BLOCK), f32),
        pltpu.VMEM((blocks, 3 * BLOCK, width), f32),
        pltpu.VMEM((blocks, BLOCK, 2 * width), bf16),
        pltpu.VMEM((blocks, BLOCK, 2 * width), bf16),
        pltpu.VMEM((blocks, STATE, 4 * width), f32),
        pltpu.VMEM((blocks, STATE, 4 * width), bf16),
        pltpu.VMEM((5 * width, BLOCK), bf16),
    ]
    half = len(bc) // 2
    outs = pl.pallas_call(
        functools.partial(mixer_kernel, len(bc)),
        out_shape=(jax.ShapeDtypeStruct((blocks, BLOCK + EXTRA, width), bf16),)
        + (jax.ShapeDtypeStruct((2, BLOCK, 2 * STATE), bf16),) * half,
        in_specs=[smem()] + [vmem()] * (6 + len(bc)),
        out_specs=(vmem(),) * (1 + half),
        scratch_shapes=scratch,
        name="mixer",
    )(at, x, drop, prm, skip, xw, bcw, *bc)
    return outs[0], outs[1:]


def swap(value, axis, bits):
    size = lax.axis_size(axis)
    return lax.ppermute(value, axis, [(i, i ^ bits) for i in range(size)])


def call(kernel, outs, *args, scratch=()):
    specs = [smem()] + [vmem()] * (len(args) - 1)
    return pl.pallas_call(
        kernel,
        out_shape=outs,
        in_specs=specs,
        out_specs=jax.tree.map(lambda _: vmem(), outs),
        scratch_shapes=scratch,
    )(*args)


def local(
    layer_activity,
    writer_matrix,
    reader_matrix,
    source_unfiltered,
    switch_raw_signal,
    saved_result,
    final_adjoint,
    delta_raw,
    extra_logdrop,
    source_filter_coefs,
    writer_filter_coefs,
    reader_filter_coefs,
    delta_offset,
    fading_exponents,
    direct_factor,
    rescale_factor,
):
    tokens = layer_activity.shape[1]
    width_in = layer_activity.shape[2]
    dp = lax.axis_size("dp")
    sp = lax.axis_size("sp")
    half = sp // 2
    heads = delta_offset.shape[0]
    width = heads * HEAD_DIM
    me_d = lax.axis_index("dp")
    me_s = lax.axis_index("sp")
    at = jnp.stack([me_d, me_s, me_s // half, me_s % half]).astype(jnp.int32)
    shape = jax.ShapeDtypeStruct
    rows = layer_activity[0]
    share = width_in // dp

    weights = jnp.concatenate(
        [
            m[:, g * STATE : (g + 1) * STATE]
            for g in range(GROUPS)
            for m in (writer_matrix, reader_matrix)
        ],
        axis=1,
    )
    pieces = {0: weights}
    bit = dp // 2
    while bit:
        pieces.update({k ^ bit: swap(v, "dp", bit) for k, v in list(pieces.items())})
        bit //= 2
    pieces = [pieces[k] for k in range(dp)]

    steps = NORM_GROUPS // 2
    wide = INNER // steps
    row_spec = pl.BlockSpec((tokens, wide), lambda i: (0, i))
    packed, d_gate = pl.pallas_call(
        prep_kernel,
        grid=(steps,),
        in_specs=[
            row_spec,
            row_spec,
            row_spec,
            pl.BlockSpec((1, wide), lambda i: (0, i)),
            row_spec,
            pl.BlockSpec((tokens, HEADS), lambda i: (0, 0)),
        ],
        out_specs=(
            pl.BlockSpec((sp // steps, 2 * BLOCK + EXTRA, width), lambda i: (i, 0, 0)),
            row_spec,
        ),
        out_shape=(
            shape((sp, 2 * BLOCK + EXTRA, width), bf16),
            shape((tokens, INNER), bf16),
        ),
        name="prep",
    )(
        saved_result[0],
        switch_raw_signal[0],
        final_adjoint[0],
        rescale_factor[None],
        source_unfiltered[0],
        delta_raw[0],
    )
    heads_x = lax.all_to_all(packed, "sp", 0, 0, tiled=True)

    acts = [lax.dynamic_slice(rows, (0, (me_d ^ k) * share), (tokens, share)) for k in range(dp)]
    acts = [acts[0]] + [swap(acts[k], "dp", k) for k in range(1, dp)]
    for k in range(dp):
        acts.append(swap(acts[k], "sp", half))

    bc = shape((tokens, 2 * STATE), bf16)
    own, other = call(proj_kernel, (bc, bc), at, rows, *pieces)
    other = swap(other, "sp", half)
    all_bc = [own if k == 0 else swap(own, "sp", k) for k in range(half)]
    all_bc += [other if k == 0 else swap(other, "sp", k) for k in range(half)]

    blocks = heads_x.shape[0]
    drop = jnp.pad(
        extra_logdrop[0].reshape(blocks, BLOCK, heads).transpose(0, 2, 1),
        ((0, 0), (0, ROWS - heads), (0, 0)),
    )
    prm = jnp.pad(jnp.stack([delta_offset, fading_exponents]), ((0, 0), (0, ROWS - heads)))
    prm = jnp.broadcast_to(prm[:, :, None], (2, ROWS, BLOCK))
    skip = jnp.repeat(direct_factor, HEAD_DIM)[None]
    bcw = jnp.stack([writer_filter_coefs, reader_filter_coefs], axis=1)
    bcw = bcw.reshape(CONV_K, 2, GROUPS, STATE)
    bcw = lax.dynamic_index_in_dim(bcw, at[2], 2, keepdims=False).reshape(CONV_K, 2 * STATE)

    d_x, d_bc = run_mixer(at, heads_x, drop, prm, skip, source_filter_coefs, bcw, all_bc)

    parts = [d_bc[0]] + [swap(d_bc[k], "sp", k) for k in range(1, half)]
    grads = functools.reduce(jnp.add, [p.astype(f32) for p in parts]).astype(bf16)
    back_x = lax.all_to_all(d_x, "sp", 0, 0, tiled=True)
    all_grads = [grads if k == 0 else swap(grads, "dp", k) for k in range(dp)]
    rest = swap(grads[1], "sp", half)

    chunk = shape((share // half, 2 * STATE), bf16)
    chunks = call(
        functools.partial(weight_kernel, dp),
        (chunk,) * half,
        at,
        *all_grads,
        *acts,
        scratch=[pltpu.VMEM((share, 2 * STATE), f32)],
    )
    chunks = [chunks[0]] + [swap(chunks[k], "sp", k) for k in range(1, half)]
    mine = functools.reduce(jnp.add, [c.astype(f32) for c in chunks]).astype(bf16)
    theirs = swap(mine, "sp", half)
    placed = [mine if k == 0 else swap(mine, "sp", k) for k in range(half)]
    placed += [theirs if k == 0 else swap(theirs, "sp", k) for k in range(half)]

    d_hidden = call(hidden_kernel, shape((tokens, width_in), bf16), at, grads[0], rest, *pieces)
    d_source, d_delta = pl.pallas_call(
        unpack_kernel,
        out_shape=(shape((tokens, INNER), bf16), shape((tokens, HEADS), bf16)),
        in_specs=[vmem()],
        out_specs=(vmem(), vmem()),
        name="unpack",
    )(back_x)
    matrix = shape((share, GROUPS * STATE), f32)
    d_w_b, d_w_c = call(functools.partial(spread_kernel, half), (matrix, matrix), at, *placed)
    return d_hidden[None], d_source[None], d_gate[None], d_delta[None], d_w_b, d_w_c


def solution(mesh):
    in_specs = (
        P("dp", "sp", None),
        P("dp", None),
        P("dp", None),
        P("dp", "sp", None),
        P("dp", "sp", None),
        P("dp", "sp", None),
        P("dp", "sp", None),
        P("dp", "sp", None),
        P("dp", None, "sp"),
        P(None, "sp"),
        P(),
        P(),
        P("sp"),
        P("sp"),
        P("sp"),
        P(),
    )
    out_specs = (
        P("dp", "sp", None),
        P("dp", "sp", None),
        P("dp", "sp", None),
        P("dp", "sp", None),
        P("dp", None),
        P("dp", None),
    )

    return jax.shard_map(local, mesh=mesh, in_specs=in_specs, out_specs=out_specs, check_vma=False)
```

profile of v0, /device:TPU:0, one launch (start us, length us, event | category | flops | bytes accessed | tf_op | source)
XLA Modules:
  0.0 147.2 jit_solution(8721377662755616768)
XLA Ops:
  0.6 1.4 copy.22
  2.0 4.3 %prep.1 = (bf16[8,272,256]{2,1,0:T(8,128)(2,1)}, bf16[128,2048]{1,0:T(8,128)(2,1)}) custom-call(bf16[128,2048]{1,0:T(8,128)(2,1)} %bitcast.40, bf16[128,2048]{1,0:T(8,128)(2,1)} %bitcast.41, bf16[128,2048]{1,0:T(8,128)(2,1)} %bitcast.42, f32[1,2048]{1,0:T(1,128)} %bitcast.49, bf16[128,2048]{1,0:T(8,128)(2,1)} %bitcast.43, bf16[128,32]{1,0:T(8,128)(2,1)} %bitcast.45), custom_call_target="tpu_custom_call" | custom-call | tf_op jit(solution)/shard_map/prep/pallas_call | solution.py:540
  6.3 7.4 %all-to-all-start = ((bf16[8,272,256]{2,1,0:T(8,128)(2,1)}), bf16[8,272,256]{2,1,0:T(8,128)(2,1)S(1)}, u32[]{:S(2)}, u32[]{:S(2)}) async-start(bf16[8,272,256]{2,1,0:T(8,128)(2,1)} %get-tuple-element.23), calls=%async_computation | async-start | bytes 2228224 | tf_op jit(solution)/shard_map/all_to_all | solution.py:568
  14.0 1.6 %collective-permute-start.1 = (bf16[512,512]{1,0:T(8,128)(2,1)S(1)}, bf16[512,512]{1,0:T(8,128)(2,1)S(1)}, u32[]{:S(2)}, u32[]{:S(2)}) collective-permute-start(bf16[512,512]{1,0:T(8,128)(2,1)S(1)} %pad_maximum_fusion.refs_0_), channel_id=1, source_target_pairs={{0,2},{1,3},{2,0},{3,1},{4,6},{5,7},{6,4},{7,5},{8,10},{9,11},{10,... | collective-permute-start | bytes 1572872 | tf_op jit(solution)/shard_map/ppermute | solution.py:476
  15.6 11.9 %collective-permute-done.1.refs_2_ = bf16[512,512]{1,0:T(8,128)(2,1)S(1)} collective-permute-done((bf16[512,512]{1,0:T(8,128)(2,1)S(1)}, bf16[512,512]{1,0:T(8,128)(2,1)S(1)}, u32[]{:S(2)}, u32[]{:S(2)}) %collective-permute-start.1) | collective-permute-done | bytes 524320 | tf_op jit(solution)/shard_map/ppermute | solution.py:476
  27.5 0.8 dynamic-slice_bitcast_fusion
  30.2 2.9 %shard_map.199 = (bf16[128,256]{1,0:T(8,128)(2,1)}, bf16[128,256]{1,0:T(8,128)(2,1)}) custom-call(s32[4]{0:T(128)} %pad_add_fusion.at_ref, bf16[128,2048]{1,0:T(8,128)(2,1)} %bitcast.39, bf16[512,512]{1,0:T(8,128)(2,1)} %copy-done, bf16[512,512]{1,0:T(8,128)(2,1)} %copy-done.5, bf16[512,512]{1,0:T(8,128)(2,1)} %copy-done.4, ...), custom_call_target="tpu_custom_call" | custom-call | tf_op jit(solution)/shard_map/pallas_call | solution.py:481
  33.1 1.7 %collective-permute-start.3 = (bf16[128,256]{1,0:T(8,128)(2,1)}, bf16[128,256]{1,0:T(8,128)(2,1)S(1)}, u32[]{:S(2)}, u32[]{:S(2)}) collective-permute-start(bf16[128,256]{1,0:T(8,128)(2,1)} %get-tuple-element.24.refs_0_), channel_id=1, source_target_pairs={{0,4},{4,0},{8,12},{12,8},{16,20},{20,16},{24,28},{28,24},{1,5},{5... | collective-permute-start | bytes 196616 | tf_op jit(solution)/shard_map/ppermute | solution.py:476
  34.8 1.5 collective-permute-start.4
  36.3 2.4 %collective-permute-start.6 = (bf16[128,256]{1,0:T(8,128)(2,1)}, bf16[128,256]{1,0:T(8,128)(2,1)S(1)}, u32[]{:S(2)}, u32[]{:S(2)}) collective-permute-start(bf16[128,256]{1,0:T(8,128)(2,1)} %get-tuple-element.25), channel_id=1, source_target_pairs={{0,16},{4,20},{8,24},{12,28},{16,0},{20,4},{24,8},{28,12},{1,17},{... | collective-permute-start | bytes 196616 | tf_op jit(solution)/shard_map/ppermute | solution.py:476
  41.2 2.7 %collective-permute-done.6.refs_4_ = bf16[128,256]{1,0:T(8,128)(2,1)S(1)} collective-permute-done((bf16[128,256]{1,0:T(8,128)(2,1)}, bf16[128,256]{1,0:T(8,128)(2,1)S(1)}, u32[]{:S(2)}, u32[]{:S(2)}) %collective-permute-start.6) | collective-permute-done | bytes 65568 | tf_op jit(solution)/shard_map/ppermute | solution.py:476
  43.9 1.4 collective-permute-start.7
  45.3 2.1 %collective-permute-start.9 = (bf16[128,256]{1,0:T(8,128)(2,1)S(1)}, bf16[128,256]{1,0:T(8,128)(2,1)S(1)}, u32[]{:S(2)}, u32[]{:S(2)}) collective-permute-start(bf16[128,256]{1,0:T(8,128)(2,1)S(1)} %collective-permute-done.6.refs_4_), channel_id=1, source_target_pairs={{0,12},{4,8},{8,4},{12,0},{16,28},{20,24},{24,20},{28,16},{1,13},{... | collective-permute-start | bytes 196616 | tf_op jit(solution)/shard_map/ppermute | solution.py:476
  47.4 1.6 %collective-permute-start.18 = (bf16[128,512]{1,0:T(8,128)(2,1)S(1)}, bf16[128,512]{1,0:T(8,128)(2,1)S(1)}, u32[]{:S(2)}, u32[]{:S(2)}) collective-permute-start(bf16[128,512]{1,0:T(8,128)(2,1)S(1)} %copy-done.22), channel_id=1, source_target_pairs={{0,2},{1,3},{2,0},{3,1},{4,6},{5,7},{6,4},{7,5},{8,10},{9,11},{10,... | collective-permute-start | bytes 393224 | tf_op jit(solution)/shard_map/ppermute | solution.py:476
  49.5 1.0 collective-permute-done.9.refs_7_
  51.6 16.4 %mixer.1 = (bf16[8,144,256]{2,1,0:T(8,128)(2,1)}, bf16[2,128,256]{2,1,0:T(8,128)(2,1)}, bf16[2,128,256]{2,1,0:T(8,128)(2,1)}, bf16[2,128,256]{2,1,0:T(8,128)(2,1)}, bf16[2,128,256]{2,1,0:T(8,128)(2,1)}) custom-call(s32[4]{0:T(128)} %pad_add_fusion.at_ref, bf16[8,272,256]{2,1,0:T(8,128)(2,1)} %copy-done.1, f32[8,8,128]{2,1,0:T(8,128)} %pad.8.drop_ref, ...), custom_call_target="tpu_custom_call" | custom-call | tf_op jit(solution)/shard_map/mixer/pallas_call | solution.py:462
  68.0 1.2 collective-permute-start.10
  69.2 1.4 collective-permute-start.11
  70.7 0.9 collective-permute-start.12
  71.6 3.5 %all-to-all-start.1 = ((bf16[8,144,256]{2,1,0:T(8,128)(2,1)}), bf16[8,144,256]{2,1,0:T(8,128)(2,1)S(1)}, u32[]{:S(2)}, u32[]{:S(2)}) async-start(bf16[8,144,256]{2,1,0:T(8,128)(2,1)} %get-tuple-element.30), calls=%async_computation.1 | async-start | bytes 1179648 | tf_op jit(solution)/shard_map/all_to_all | solution.py:597
  75.1 3.0 %collective-permute-start.20 = (bf16[128,512]{1,0:T(8,128)(2,1)S(1)}, bf16[128,512]{1,0:T(8,128)(2,1)S(1)}, u32[]{:S(2)}, u32[]{:S(2)}) collective-permute-start(bf16[128,512]{1,0:T(8,128)(2,1)S(1)} %get-tuple-element.48.refs_4_), channel_id=1, source_target_pairs={{0,16},{4,20},{8,24},{12,28},{16,0},{20,4},{24,8},{28,12},{1,17},{... | collective-permute-start | bytes 393224 | tf_op jit(solution)/shard_map/ppermute | solution.py:476
  78.2 2.8 %collective-permute-start.22 = (bf16[128,512]{1,0:T(8,128)(2,1)S(1)}, bf16[128,512]{1,0:T(8,128)(2,1)S(1)}, u32[]{:S(2)}, u32[]{:S(2)}) collective-permute-start(bf16[128,512]{1,0:T(8,128)(2,1)S(1)} %collective-permute-done.18.refs_6_), channel_id=1, source_target_pairs={{0,16},{4,20},{8,24},{12,28},{16,0},{20,4},{24,8},{28,12},{1,17},{... | collective-permute-start | bytes 393224 | tf_op jit(solution)/shard_map/ppermute | solution.py:476
  81.3 25.1 %collective-permute-done.20.refs_8_ = bf16[128,512]{1,0:T(8,128)(2,1)S(1)} collective-permute-done((bf16[128,512]{1,0:T(8,128)(2,1)S(1)}, bf16[128,512]{1,0:T(8,128)(2,1)S(1)}, u32[]{:S(2)}, u32[]{:S(2)}) %collective-permute-start.20) | collective-permute-done | bytes 131104 | tf_op jit(solution)/shard_map/ppermute | solution.py:476
  106.4 0.8 collective-permute-start.15
  107.2 2.0 %collective-permute-done.21.refs_9_ = bf16[128,512]{1,0:T(8,128)(2,1)S(1)} collective-permute-done((bf16[128,512]{1,0:T(8,128)(2,1)S(1)}, bf16[128,512]{1,0:T(8,128)(2,1)S(1)}, u32[]{:S(2)}, u32[]{:S(2)}) %collective-permute-start.21) | collective-permute-done | bytes 131104 | tf_op jit(solution)/shard_map/ppermute | solution.py:476
  109.2 2.4 %collective-permute-done.22.refs_10_ = bf16[128,512]{1,0:T(8,128)(2,1)S(1)} collective-permute-done((bf16[128,512]{1,0:T(8,128)(2,1)S(1)}, bf16[128,512]{1,0:T(8,128)(2,1)S(1)}, u32[]{:S(2)}, u32[]{:S(2)}) %collective-permute-start.22) | collective-permute-done | bytes 131104 | tf_op jit(solution)/shard_map/ppermute | solution.py:476
  111.6 1.4 collective-permute-done.23.refs_11_
  113.1 1.3 collective-permute-done.16.refs_3_
  115.1 2.9 %shard_map.201 = (bf16[128,256]{1,0:T(8,128)(2,1)}, bf16[128,256]{1,0:T(8,128)(2,1)}, bf16[128,256]{1,0:T(8,128)(2,1)}, bf16[128,256]{1,0:T(8,128)(2,1)}) custom-call(s32[4]{0:T(128)} %pad_add_fusion.at_ref, bf16[2,128,256]{2,1,0:T(8,128)(2,1)} %copy-done.6, bf16[2,128,256]{2,1,0:T(8,128)(2,1)} %copy-done.19, bf16[2,128,256]{2,1,0:T(8,128)(2,1)} %copy-done.20, ...), custom_call_target="tpu_custom_call" | custom-call | tf_op jit(solution)/shard_map/pallas_call | solution.py:481
  118.0 1.3 collective-permute-start.24
  119.3 2.2 %collective-permute-start.26 = (bf16[128,256]{1,0:T(8,128)(2,1)}, bf16[128,256]{1,0:T(8,128)(2,1)S(1)}, u32[]{:S(2)}, u32[]{:S(2)}) collective-permute-start(bf16[128,256]{1,0:T(8,128)(2,1)} %get-tuple-element.37), channel_id=1, source_target_pairs={{0,12},{4,8},{8,4},{12,0},{16,28},{20,24},{24,20},{28,16},{1,13},{... | collective-permute-start | bytes 196616 | tf_op jit(solution)/shard_map/ppermute | solution.py:476
  121.5 1.5 %slice_bitcast_fusion = (bf16[128,256]{1,0:T(8,128)(2,1)S(1)}, bf16[128,256]{1,0:T(8,128)(2,1)}) fusion(bf16[2,128,256]{2,1,0:T(8,128)(2,1)} %copy-done.6), kind=kLoop, calls=%fused_computation.7 | loop fusion | bytes 262144 | tf_op jit(solution)/shard_map/squeeze | solution.py:599
  123.0 1.0 collective-permute-done.25
  124.0 0.9 collective-permute-done.26
  124.9 0.9 add_convert_fusion.1.refs_0_
  125.8 1.3 collective-permute-start.30
  127.1 1.7 %collective-permute-start.13 = (bf16[128,256]{1,0:T(8,128)(2,1)S(1)}, bf16[128,256]{1,0:T(8,128)(2,1)S(1)}, u32[]{:S(2)}, u32[]{:S(2)}) collective-permute-start(bf16[128,256]{1,0:T(8,128)(2,1)S(1)} %get-tuple-element.54), channel_id=1, source_target_pairs={{0,16},{4,20},{8,24},{12,28},{16,0},{20,4},{24,8},{28,12},{1,17},{... | collective-permute-start | bytes 196616 | tf_op jit(solution)/shard_map/ppermute | solution.py:476
  128.8 1.3 collective-permute-start.27
  130.0 1.3 collective-permute-start.28
  131.3 0.9 collective-permute-start.29
  132.3 1.3 collective-permute-start.31
  133.5 1.3 collective-permute-start.32
  134.8 1.6 %collective-permute-start.33 = (bf16[128,256]{1,0:T(8,128)(2,1)S(1)}, bf16[128,256]{1,0:T(8,128)(2,1)S(1)}, u32[]{:S(2)}, u32[]{:S(2)}) collective-permute-start(bf16[128,256]{1,0:T(8,128)(2,1)S(1)} %collective-permute-done.30.refs_4_), channel_id=1, source_target_pairs={{0,12},{4,8},{8,4},{12,0},{16,28},{20,24},{24,20},{28,16},{1,13},{... | collective-permute-start | bytes 196616 | tf_op jit(solution)/shard_map/ppermute | solution.py:476
  136.4 3.2 %shard_map.200 = bf16[128,2048]{1,0:T(8,128)(2,1)} custom-call(s32[4]{0:T(128)} %pad_add_fusion.at_ref, bf16[128,256]{1,0:T(8,128)(2,1)} %get-tuple-element.55.own_ref, bf16[128,256]{1,0:T(8,128)(2,1)} %copy-done.35, bf16[512,512]{1,0:T(8,128)(2,1)} %copy-done, bf16[512,512]{1,0:T(8,128)(2,1)} %copy-done.5, bf16[512,512]{1,0:T(8,128)(2,1)} %copy-done.4, ...), custom_call_target="tpu_custom_call" | custom-call | tf_op jit(solution)/shard_map/pallas_call | solution.py:481
  140.9 2.1 %shard_map.202 = (f32[512,256]{1,0:T(8,128)}, f32[512,256]{1,0:T(8,128)}) custom-call(s32[4]{0:T(128)} %pad_add_fusion.at_ref, bf16[128,256]{1,0:T(8,128)(2,1)} %copy-done.8, bf16[128,256]{1,0:T(8,128)(2,1)} %copy-done.28, bf16[128,256]{1,0:T(8,128)(2,1)} %copy-done.30, bf16[128,256]{1,0:T(8,128)(2,1)} %copy-done.31, bf16[128,256]{1,0:T(8,128)(2,1)} %copy-done.26, ...), custom_call_target="tpu_custom_call" | custom-call | tf_op jit(solution)/shard_map/pallas_call | solution.py:481
  143.0 0.9 copy-done.2
  143.9 1.9 %unpack.1 = (bf16[128,2048]{1,0:T(8,128)(2,1)}, bf16[128,32]{1,0:T(8,128)(2,1)}) custom-call(bf16[8,144,256]{2,1,0:T(8,128)(2,1)} %copy-done.2), custom_call_target="tpu_custom_call" | custom-call | tf_op jit(solution)/shard_map/unpack/pallas_call | solution.py:617
  145.8 1.4 copy.25
  (139 shorter events, 8.4 us)
Async XLA Ops:
  6.3 44.2 %all-to-all-start = ((bf16[8,272,256]{2,1,0:T(8,128)(2,1)}), bf16[8,272,256]{2,1,0:T(8,128)(2,1)S(1)}, u32[]{:S(2)}, u32[]{:S(2)}) async-start(bf16[8,272,256]{2,1,0:T(8,128)(2,1)} %get-tuple-element.23), calls=%async_computation | async-start | bytes 2228224 | tf_op jit(solution)/shard_map/all_to_all | solution.py:568
  13.9 14.8 %copy-start.39 = (f32[5,256]{1,0:T(8,128)S(1)}, f32[5,256]{1,0:T(8,128)}, u32[]{:S(2)}) copy-start(f32[5,256]{1,0:T(8,128)} %param.26) | copy-start | bytes 15364
  13.9 14.8 %copy-start.40 = (f32[5,256]{1,0:T(8,128)S(1)}, f32[5,256]{1,0:T(8,128)}, u32[]{:S(2)}) copy-start(f32[5,256]{1,0:T(8,128)} %param.27) | copy-start | bytes 15364
  14.0 15.5 %copy-start = (bf16[512,512]{1,0:T(8,128)(2,1)}, bf16[512,512]{1,0:T(8,128)(2,1)S(1)}, u32[]{:S(2)}) copy-start(bf16[512,512]{1,0:T(8,128)(2,1)S(1)} %pad_maximum_fusion.refs_0_) | copy-start | bytes 1572868
  14.0 13.4 %collective-permute-start.1 = (bf16[512,512]{1,0:T(8,128)(2,1)S(1)}, bf16[512,512]{1,0:T(8,128)(2,1)S(1)}, u32[]{:S(2)}, u32[]{:S(2)}) collective-permute-start(bf16[512,512]{1,0:T(8,128)(2,1)S(1)} %pad_maximum_fusion.refs_0_), channel_id=1, source_target_pairs={{0,2},{1,3},{2,0},{3,1},{4,6},{5,7},{6,4},{7,5},{8,10},{9,11},{10,... | collective-permute-start | bytes 1572872 | tf_op jit(solution)/shard_map/ppermute | solution.py:476
  15.6 13.8 %collective-permute-start = (bf16[512,512]{1,0:T(8,128)(2,1)S(1)}, bf16[512,512]{1,0:T(8,128)(2,1)S(1)}, u32[]{:S(2)}, u32[]{:S(2)}) collective-permute-start(bf16[512,512]{1,0:T(8,128)(2,1)S(1)} %pad_maximum_fusion.refs_0_), channel_id=1, source_target_pairs={{0,1},{1,0},{2,3},{3,2},{4,5},{5,4},{6,7},{7,6},{8,9},{9,8},{10,11... | collective-permute-start | bytes 1572872 | tf_op jit(solution)/shard_map/ppermute | solution.py:476
  27.5 2.0 %collective-permute-start.2 = (bf16[512,512]{1,0:T(8,128)(2,1)S(1)}, bf16[512,512]{1,0:T(8,128)(2,1)}, u32[]{:S(2)}, u32[]{:S(2)}) collective-permute-start(bf16[512,512]{1,0:T(8,128)(2,1)S(1)} %collective-permute-done.1.refs_2_), channel_id=1, source_target_pairs={{0,1},{1,0},{2,3},{3,2},{4,5},{5,4},{6,7},{7,6},{8,9},{9,8},{10,11... | collective-permute-start | bytes 1572872 | tf_op jit(solution)/shard_map/ppermute | solution.py:476
  28.3 86.1 %copy-start.7 = (bf16[128,512]{1,0:T(8,128)(2,1)}, bf16[128,512]{1,0:T(8,128)(2,1)S(1)}, u32[]{:S(2)}) copy-start(bf16[128,512]{1,0:T(8,128)(2,1)S(1)} %get-tuple-element.48.refs_4_) | copy-start | bytes 393220
  28.3 42.4 %collective-permute-start.17 = (bf16[128,512]{1,0:T(8,128)(2,1)}, bf16[128,512]{1,0:T(8,128)(2,1)S(1)}, u32[]{:S(2)}, u32[]{:S(2)}) collective-permute-start(bf16[128,512]{1,0:T(8,128)(2,1)} %get-tuple-element.47), channel_id=1, source_target_pairs={{0,1},{1,0},{2,3},{3,2},{4,5},{5,4},{6,7},{7,6},{8,9},{9,8},{10,11... | collective-permute-start | bytes 393224 | tf_op jit(solution)/shard_map/ppermute | solution.py:476
  30.2 17.2 %copy-start.42 = (f32[4]{0:T(128)S(1)}, f32[4]{0:T(128)}, u32[]{:S(2)}) copy-start(f32[4]{0:T(128)} %param.29) | copy-start | bytes 52
  30.2 17.2 %copy-start.43 = (f32[4]{0:T(128)S(1)}, f32[4]{0:T(128)}, u32[]{:S(2)}) copy-start(f32[4]{0:T(128)} %param.28) | copy-start | bytes 52
  30.2 17.2 %copy-start.22 = (bf16[128,512]{1,0:T(8,128)(2,1)S(1)}, bf16[128,512]{1,0:T(8,128)(2,1)}, u32[]{:S(2)}) copy-start(bf16[128,512]{1,0:T(8,128)(2,1)} %get-tuple-element.49) | copy-start | bytes 393220
  33.1 12.2 %collective-permute-start.3 = (bf16[128,256]{1,0:T(8,128)(2,1)}, bf16[128,256]{1,0:T(8,128)(2,1)S(1)}, u32[]{:S(2)}, u32[]{:S(2)}) collective-permute-start(bf16[128,256]{1,0:T(8,128)(2,1)} %get-tuple-element.24.refs_0_), channel_id=1, source_target_pairs={{0,4},{4,0},{8,12},{12,8},{16,20},{20,16},{24,28},{28,24},{1,5},{5... | collective-permute-start | bytes 196616 | tf_op jit(solution)/shard_map/ppermute | solution.py:476
  34.8 10.4 %collective-permute-start.4 = (bf16[128,256]{1,0:T(8,128)(2,1)}, bf16[128,256]{1,0:T(8,128)(2,1)S(1)}, u32[]{:S(2)}, u32[]{:S(2)}) collective-permute-start(bf16[128,256]{1,0:T(8,128)(2,1)} %get-tuple-element.24.refs_0_), channel_id=1, source_target_pairs={{0,8},{4,12},{8,0},{12,4},{16,24},{20,28},{24,16},{28,20},{1,9},{5... | collective-permute-start | bytes 196616 | tf_op jit(solution)/shard_map/ppermute | solution.py:476
  36.3 7.6 %collective-permute-start.6 = (bf16[128,256]{1,0:T(8,128)(2,1)}, bf16[128,256]{1,0:T(8,128)(2,1)S(1)}, u32[]{:S(2)}, u32[]{:S(2)}) collective-permute-start(bf16[128,256]{1,0:T(8,128)(2,1)} %get-tuple-element.25), channel_id=1, source_target_pairs={{0,16},{4,20},{8,24},{12,28},{16,0},{20,4},{24,8},{28,12},{1,17},{... | collective-permute-start | bytes 196616 | tf_op jit(solution)/shard_map/ppermute | solution.py:476
  40.6 6.8 %collective-permute-start.5 = (bf16[128,256]{1,0:T(8,128)(2,1)}, bf16[128,256]{1,0:T(8,128)(2,1)S(1)}, u32[]{:S(2)}, u32[]{:S(2)}) collective-permute-start(bf16[128,256]{1,0:T(8,128)(2,1)} %get-tuple-element.24.refs_0_), channel_id=1, source_target_pairs={{0,12},{4,8},{8,4},{12,0},{16,28},{20,24},{24,20},{28,16},{1,13},{... | collective-permute-start | bytes 196616 | tf_op jit(solution)/shard_map/ppermute | solution.py:476
  43.9 5.1 %collective-permute-start.7 = (bf16[128,256]{1,0:T(8,128)(2,1)S(1)}, bf16[128,256]{1,0:T(8,128)(2,1)S(1)}, u32[]{:S(2)}, u32[]{:S(2)}) collective-permute-start(bf16[128,256]{1,0:T(8,128)(2,1)S(1)} %collective-permute-done.6.refs_4_), channel_id=1, source_target_pairs={{0,4},{4,0},{8,12},{12,8},{16,20},{20,16},{24,28},{28,24},{1,5},{5... | collective-permute-start | bytes 196616 | tf_op jit(solution)/shard_map/ppermute | solution.py:476
  45.3 4.3 %collective-permute-start.8 = (bf16[128,256]{1,0:T(8,128)(2,1)S(1)}, bf16[128,256]{1,0:T(8,128)(2,1)S(1)}, u32[]{:S(2)}, u32[]{:S(2)}) collective-permute-start(bf16[128,256]{1,0:T(8,128)(2,1)S(1)} %collective-permute-done.6.refs_4_), channel_id=1, source_target_pairs={{0,8},{4,12},{8,0},{12,4},{16,24},{20,28},{24,16},{28,20},{1,9},{5... | collective-permute-start | bytes 196616 | tf_op jit(solution)/shard_map/ppermute | solution.py:476
  45.3 5.2 %collective-permute-start.9 = (bf16[128,256]{1,0:T(8,128)(2,1)S(1)}, bf16[128,256]{1,0:T(8,128)(2,1)S(1)}, u32[]{:S(2)}, u32[]{:S(2)}) collective-permute-start(bf16[128,256]{1,0:T(8,128)(2,1)S(1)} %collective-permute-done.6.refs_4_), channel_id=1, source_target_pairs={{0,12},{4,8},{8,4},{12,0},{16,28},{20,24},{24,20},{28,16},{1,13},{... | collective-permute-start | bytes 196616 | tf_op jit(solution)/shard_map/ppermute | solution.py:476
  47.4 27.7 %collective-permute-start.18 = (bf16[128,512]{1,0:T(8,128)(2,1)S(1)}, bf16[128,512]{1,0:T(8,128)(2,1)S(1)}, u32[]{:S(2)}, u32[]{:S(2)}) collective-permute-start(bf16[128,512]{1,0:T(8,128)(2,1)S(1)} %copy-done.22), channel_id=1, source_target_pairs={{0,2},{1,3},{2,0},{3,1},{4,6},{5,7},{6,4},{7,5},{8,10},{9,11},{10,... | collective-permute-start | bytes 393224 | tf_op jit(solution)/shard_map/ppermute | solution.py:476
  49.0 29.1 %collective-permute-start.19 = (bf16[128,512]{1,0:T(8,128)(2,1)S(1)}, bf16[128,512]{1,0:T(8,128)(2,1)S(1)}, u32[]{:S(2)}, u32[]{:S(2)}) collective-permute-start(bf16[128,512]{1,0:T(8,128)(2,1)S(1)} %get-tuple-element.46), channel_id=1, source_target_pairs={{0,3},{1,2},{2,1},{3,0},{4,7},{5,6},{6,5},{7,4},{8,11},{9,10},{10,... | collective-permute-start | bytes 393224 | tf_op jit(solution)/shard_map/ppermute | solution.py:476
  68.0 10.2 %collective-permute-start.10 = (bf16[2,128,256]{2,1,0:T(8,128)(2,1)}, bf16[2,128,256]{2,1,0:T(8,128)(2,1)S(1)}, u32[]{:S(2)}, u32[]{:S(2)}) collective-permute-start(bf16[2,128,256]{2,1,0:T(8,128)(2,1)} %get-tuple-element.27), channel_id=1, source_target_pairs={{0,4},{4,0},{8,12},{12,8},{16,20},{20,16},{24,28},{28,24},{1,5},{5... | collective-permute-start | bytes 393224 | tf_op jit(solution)/shard_map/ppermute | solution.py:476
  69.2 11.8 %collective-permute-start.11 = (bf16[2,128,256]{2,1,0:T(8,128)(2,1)}, bf16[2,128,256]{2,1,0:T(8,128)(2,1)S(1)}, u32[]{:S(2)}, u32[]{:S(2)}) collective-permute-start(bf16[2,128,256]{2,1,0:T(8,128)(2,1)} %get-tuple-element.28), channel_id=1, source_target_pairs={{0,8},{4,12},{8,0},{12,4},{16,24},{20,28},{24,16},{28,20},{1,9},{5... | collective-permute-start | bytes 393224 | tf_op jit(solution)/shard_map/ppermute | solution.py:476
  70.7 43.7 %copy-start.11 = (bf16[128,512]{1,0:T(8,128)(2,1)}, bf16[128,512]{1,0:T(8,128)(2,1)S(1)}, u32[]{:S(2)}) copy-start(bf16[128,512]{1,0:T(8,128)(2,1)S(1)} %collective-permute-done.17.refs_5_) | copy-start | bytes 393220
  70.7 10.5 %collective-permute-start.12 = (bf16[2,128,256]{2,1,0:T(8,128)(2,1)}, bf16[2,128,256]{2,1,0:T(8,128)(2,1)S(1)}, u32[]{:S(2)}, u32[]{:S(2)}) collective-permute-start(bf16[2,128,256]{2,1,0:T(8,128)(2,1)} %get-tuple-element.29), channel_id=1, source_target_pairs={{0,12},{4,8},{8,4},{12,0},{16,28},{20,24},{24,20},{28,16},{1,13},{... | collective-permute-start | bytes 393224 | tf_op jit(solution)/shard_map/ppermute | solution.py:476
  71.6 71.5 %all-to-all-start.1 = ((bf16[8,144,256]{2,1,0:T(8,128)(2,1)}), bf16[8,144,256]{2,1,0:T(8,128)(2,1)S(1)}, u32[]{:S(2)}, u32[]{:S(2)}) async-start(bf16[8,144,256]{2,1,0:T(8,128)(2,1)} %get-tuple-element.30), calls=%async_computation.1 | async-start | bytes 1179648 | tf_op jit(solution)/shard_map/all_to_all | solution.py:597
  75.1 39.2 %copy-start.12 = (bf16[128,512]{1,0:T(8,128)(2,1)}, bf16[128,512]{1,0:T(8,128)(2,1)S(1)}, u32[]{:S(2)}) copy-start(bf16[128,512]{1,0:T(8,128)(2,1)S(1)} %collective-permute-done.18.refs_6_) | copy-start | bytes 393220
  75.1 31.3 %collective-permute-start.20 = (bf16[128,512]{1,0:T(8,128)(2,1)S(1)}, bf16[128,512]{1,0:T(8,128)(2,1)S(1)}, u32[]{:S(2)}, u32[]{:S(2)}) collective-permute-start(bf16[128,512]{1,0:T(8,128)(2,1)S(1)} %get-tuple-element.48.refs_4_), channel_id=1, source_target_pairs={{0,16},{4,20},{8,24},{12,28},{16,0},{20,4},{24,8},{28,12},{1,17},{... | collective-permute-start | bytes 393224 | tf_op jit(solution)/shard_map/ppermute | solution.py:476
  78.1 36.3 %copy-start.13 = (bf16[128,512]{1,0:T(8,128)(2,1)}, bf16[128,512]{1,0:T(8,128)(2,1)S(1)}, u32[]{:S(2)}) copy-start(bf16[128,512]{1,0:T(8,128)(2,1)S(1)} %collective-permute-done.19.refs_7_) | copy-start | bytes 393220
  78.1 31.1 %collective-permute-start.21 = (bf16[128,512]{1,0:T(8,128)(2,1)S(1)}, bf16[128,512]{1,0:T(8,128)(2,1)S(1)}, u32[]{:S(2)}, u32[]{:S(2)}) collective-permute-start(bf16[128,512]{1,0:T(8,128)(2,1)S(1)} %collective-permute-done.17.refs_5_), channel_id=1, source_target_pairs={{0,16},{4,20},{8,24},{12,28},{16,0},{20,4},{24,8},{28,12},{1,17},{... | collective-permute-start | bytes 393224 | tf_op jit(solution)/shard_map/ppermute | solution.py:476
  78.2 33.4 %collective-permute-start.22 = (bf16[128,512]{1,0:T(8,128)(2,1)S(1)}, bf16[128,512]{1,0:T(8,128)(2,1)S(1)}, u32[]{:S(2)}, u32[]{:S(2)}) collective-permute-start(bf16[128,512]{1,0:T(8,128)(2,1)S(1)} %collective-permute-done.18.refs_6_), channel_id=1, source_target_pairs={{0,16},{4,20},{8,24},{12,28},{16,0},{20,4},{24,8},{28,12},{1,17},{... | collective-permute-start | bytes 393224 | tf_op jit(solution)/shard_map/ppermute | solution.py:476
  81.0 32.0 %collective-permute-start.23 = (bf16[128,512]{1,0:T(8,128)(2,1)S(1)}, bf16[128,512]{1,0:T(8,128)(2,1)S(1)}, u32[]{:S(2)}, u32[]{:S(2)}) collective-permute-start(bf16[128,512]{1,0:T(8,128)(2,1)S(1)} %collective-permute-done.19.refs_7_), channel_id=1, source_target_pairs={{0,16},{4,20},{8,24},{12,28},{16,0},{20,4},{24,8},{28,12},{1,17},{... | collective-permute-start | bytes 393224 | tf_op jit(solution)/shard_map/ppermute | solution.py:476
  81.2 33.2 %copy-start.6 = (bf16[2,128,256]{2,1,0:T(8,128)(2,1)}, bf16[2,128,256]{2,1,0:T(8,128)(2,1)S(1)}, u32[]{:S(2)}) copy-start(bf16[2,128,256]{2,1,0:T(8,128)(2,1)S(1)} %add_convert_fusion.refs_0_) | copy-start | bytes 393220
  81.2 31.8 %collective-permute-start.14 = (bf16[2,128,256]{2,1,0:T(8,128)(2,1)S(1)}, bf16[2,128,256]{2,1,0:T(8,128)(2,1)S(1)}, u32[]{:S(2)}, u32[]{:S(2)}) collective-permute-start(bf16[2,128,256]{2,1,0:T(8,128)(2,1)S(1)} %add_convert_fusion.refs_0_), channel_id=1, source_target_pairs={{0,1},{1,0},{2,3},{3,2},{4,5},{5,4},{6,7},{7,6},{8,9},{9,8},{10,11... | collective-permute-start | bytes 393224 | tf_op jit(solution)/shard_map/ppermute | solution.py:476
  106.4 6.6 %collective-permute-start.15 = (bf16[2,128,256]{2,1,0:T(8,128)(2,1)S(1)}, bf16[2,128,256]{2,1,0:T(8,128)(2,1)S(1)}, u32[]{:S(2)}, u32[]{:S(2)}) collective-permute-start(bf16[2,128,256]{2,1,0:T(8,128)(2,1)S(1)} %add_convert_fusion.refs_0_), channel_id=1, source_target_pairs={{0,2},{1,3},{2,0},{3,1},{4,6},{5,7},{6,4},{7,5},{8,10},{9,11},{10,... | collective-permute-start | bytes 393224 | tf_op jit(solution)/shard_map/ppermute | solution.py:476
  109.2 5.1 %collective-permute-start.16 = (bf16[2,128,256]{2,1,0:T(8,128)(2,1)S(1)}, bf16[2,128,256]{2,1,0:T(8,128)(2,1)S(1)}, u32[]{:S(2)}, u32[]{:S(2)}) collective-permute-start(bf16[2,128,256]{2,1,0:T(8,128)(2,1)S(1)} %add_convert_fusion.refs_0_), channel_id=1, source_target_pairs={{0,3},{1,2},{2,1},{3,0},{4,7},{5,6},{6,5},{7,4},{8,11},{9,10},{10,... | collective-permute-start | bytes 393224 | tf_op jit(solution)/shard_map/ppermute | solution.py:476
  118.0 5.0 %collective-permute-start.24 = (bf16[128,256]{1,0:T(8,128)(2,1)}, bf16[128,256]{1,0:T(8,128)(2,1)S(1)}, u32[]{:S(2)}, u32[]{:S(2)}) collective-permute-start(bf16[128,256]{1,0:T(8,128)(2,1)} %get-tuple-element.35), channel_id=1, source_target_pairs={{0,4},{4,0},{8,12},{12,8},{16,20},{20,16},{24,28},{28,24},{1,5},{5... | collective-permute-start | bytes 196616 | tf_op jit(solution)/shard_map/ppermute | solution.py:476
  119.3 4.7 %collective-permute-start.25 = (bf16[128,256]{1,0:T(8,128)(2,1)}, bf16[128,256]{1,0:T(8,128)(2,1)S(1)}, u32[]{:S(2)}, u32[]{:S(2)}) collective-permute-start(bf16[128,256]{1,0:T(8,128)(2,1)} %get-tuple-element.36), channel_id=1, source_target_pairs={{0,8},{4,12},{8,0},{12,4},{16,24},{20,28},{24,16},{28,20},{1,9},{5... | collective-permute-start | bytes 196616 | tf_op jit(solution)/shard_map/ppermute | solution.py:476
  119.3 5.6 %collective-permute-start.26 = (bf16[128,256]{1,0:T(8,128)(2,1)}, bf16[128,256]{1,0:T(8,128)(2,1)S(1)}, u32[]{:S(2)}, u32[]{:S(2)}) collective-permute-start(bf16[128,256]{1,0:T(8,128)(2,1)} %get-tuple-element.37), channel_id=1, source_target_pairs={{0,12},{4,8},{8,4},{12,0},{16,28},{20,24},{24,20},{28,16},{1,13},{... | collective-permute-start | bytes 196616 | tf_op jit(solution)/shard_map/ppermute | solution.py:476
  125.8 13.8 %copy-start.8 = (bf16[128,256]{1,0:T(8,128)(2,1)}, bf16[128,256]{1,0:T(8,128)(2,1)S(1)}, u32[]{:S(2)}) copy-start(bf16[128,256]{1,0:T(8,128)(2,1)S(1)} %add_convert_fusion.1.refs_0_) | copy-start | bytes 196612
  125.8 6.5 %collective-permute-start.30 = (bf16[128,256]{1,0:T(8,128)(2,1)S(1)}, bf16[128,256]{1,0:T(8,128)(2,1)S(1)}, u32[]{:S(2)}, u32[]{:S(2)}) collective-permute-start(bf16[128,256]{1,0:T(8,128)(2,1)S(1)} %add_convert_fusion.1.refs_0_), channel_id=1, source_target_pairs={{0,16},{4,20},{8,24},{12,28},{16,0},{20,4},{24,8},{28,12},{1,17},{... | collective-permute-start | bytes 196616 | tf_op jit(solution)/shard_map/ppermute | solution.py:476
  127.1 6.4 %collective-permute-start.13 = (bf16[128,256]{1,0:T(8,128)(2,1)S(1)}, bf16[128,256]{1,0:T(8,128)(2,1)S(1)}, u32[]{:S(2)}, u32[]{:S(2)}) collective-permute-start(bf16[128,256]{1,0:T(8,128)(2,1)S(1)} %get-tuple-element.54), channel_id=1, source_target_pairs={{0,16},{4,20},{8,24},{12,28},{16,0},{20,4},{24,8},{28,12},{1,17},{... | collective-permute-start | bytes 196616 | tf_op jit(solution)/shard_map/ppermute | solution.py:476
  128.8 6.0 %collective-permute-start.27 = (bf16[128,256]{1,0:T(8,128)(2,1)S(1)}, bf16[128,256]{1,0:T(8,128)(2,1)S(1)}, u32[]{:S(2)}, u32[]{:S(2)}) collective-permute-start(bf16[128,256]{1,0:T(8,128)(2,1)S(1)} %add_convert_fusion.1.refs_0_), channel_id=1, source_target_pairs={{0,4},{4,0},{8,12},{12,8},{16,20},{20,16},{24,28},{28,24},{1,5},{5... | collective-permute-start | bytes 196616 | tf_op jit(solution)/shard_map/ppermute | solution.py:476
  130.0 9.6 %collective-permute-start.28 = (bf16[128,256]{1,0:T(8,128)(2,1)S(1)}, bf16[128,256]{1,0:T(8,128)(2,1)S(1)}, u32[]{:S(2)}, u32[]{:S(2)}) collective-permute-start(bf16[128,256]{1,0:T(8,128)(2,1)S(1)} %add_convert_fusion.1.refs_0_), channel_id=1, source_target_pairs={{0,8},{4,12},{8,0},{12,4},{16,24},{20,28},{24,16},{28,20},{1,9},{5... | collective-permute-start | bytes 196616 | tf_op jit(solution)/shard_map/ppermute | solution.py:476
  131.3 8.3 %collective-permute-start.29 = (bf16[128,256]{1,0:T(8,128)(2,1)S(1)}, bf16[128,256]{1,0:T(8,128)(2,1)S(1)}, u32[]{:S(2)}, u32[]{:S(2)}) collective-permute-start(bf16[128,256]{1,0:T(8,128)(2,1)S(1)} %add_convert_fusion.1.refs_0_), channel_id=1, source_target_pairs={{0,12},{4,8},{8,4},{12,0},{16,28},{20,24},{24,20},{28,16},{1,13},{... | collective-permute-start | bytes 196616 | tf_op jit(solution)/shard_map/ppermute | solution.py:476
  132.3 7.4 %collective-permute-start.31 = (bf16[128,256]{1,0:T(8,128)(2,1)S(1)}, bf16[128,256]{1,0:T(8,128)(2,1)S(1)}, u32[]{:S(2)}, u32[]{:S(2)}) collective-permute-start(bf16[128,256]{1,0:T(8,128)(2,1)S(1)} %collective-permute-done.30.refs_4_), channel_id=1, source_target_pairs={{0,4},{4,0},{8,12},{12,8},{16,20},{20,16},{24,28},{28,24},{1,5},{5... | collective-permute-start | bytes 196616 | tf_op jit(solution)/shard_map/ppermute | solution.py:476
  133.5 6.1 %collective-permute-start.32 = (bf16[128,256]{1,0:T(8,128)(2,1)S(1)}, bf16[128,256]{1,0:T(8,128)(2,1)S(1)}, u32[]{:S(2)}, u32[]{:S(2)}) collective-permute-start(bf16[128,256]{1,0:T(8,128)(2,1)S(1)} %collective-permute-done.30.refs_4_), channel_id=1, source_target_pairs={{0,8},{4,12},{8,0},{12,4},{16,24},{20,28},{24,16},{28,20},{1,9},{5... | collective-permute-start | bytes 196616 | tf_op jit(solution)/shard_map/ppermute | solution.py:476
  134.8 5.2 %collective-permute-start.33 = (bf16[128,256]{1,0:T(8,128)(2,1)S(1)}, bf16[128,256]{1,0:T(8,128)(2,1)S(1)}, u32[]{:S(2)}, u32[]{:S(2)}) collective-permute-start(bf16[128,256]{1,0:T(8,128)(2,1)S(1)} %collective-permute-done.30.refs_4_), channel_id=1, source_target_pairs={{0,12},{4,8},{8,4},{12,0},{16,28},{20,24},{24,20},{28,16},{1,13},{... | collective-permute-start | bytes 196616 | tf_op jit(solution)/shard_map/ppermute | solution.py:476
  (32 other events, 132.5 us)
where the time goes:
time: 148 us; the launch traced here: 147 us
  waiting for transfers between devices  50.6 us (34%)
  starting transfers between devices  48.6 us (33%)
  Pallas kernels  33.7 us (23%)
  local copies, waits for them, and re-layouts  11.5 us (8%)
  other arithmetic  1.68 us (1%)
    ppermute x34, waiting for transfers between devices, swap(): return lax.ppermute(value, axis, [(i, i ^ bits) for i in range(size)])  50.6 us
    ppermute x34, starting transfers between devices, swap(): return lax.ppermute(value, axis, [(i, i ^ bits) for i in range(size)])  37.7 us
    pallas_call x1, Pallas kernels, run_mixer(): pl.pallas_call(functools.partial(mixer_kernel, len(bc)), out_shape=(jax.S...  16.4 us
    pallas_call x4, Pallas kernels, call(): pl.pallas_call(kernel, out_shape=outs, in_specs=specs, out_specs=jax.tree...  11.1 us
    all_to_all x1, starting transfers between devices, local(): heads_x = lax.all_to_all(packed, 'sp', 0, 0, tiled=True)  7.42 us
    unnamed x91, local copies, waits for them, and re-layouts  6.95 us
    pallas_call x1, Pallas kernels, local(): pl.pallas_call(prep_kernel, grid=(steps,), in_specs=[row_spec, row_spec,...  4.29 us
    all_to_all x1, starting transfers between devices, local(): back_x = lax.all_to_all(d_x, 'sp', 0, 0, tiled=True)  3.55 us
  transfers between devices with their start and end apart: 36, of which 13 were waited for; matrix products, arithmetic and copies ran while one was open for 5% of the time, Pallas kernels for 19%

commit v1 on v0

--- a/solution.py
+++ b/solution.py
@@ -64,13 +64,10 @@
 
 
 def prep_kernel(saved_ref, switch_ref, final_ref, scale_ref, x_ref, dt_ref, out_ref, gate_ref):
-    chunks, _, width = out_ref.shape
+    _, _, width = out_ref.shape
     cols = INNER // NORM_GROUPS
     heads = width // HEAD_DIM
-    first_row = pl.program_id(0) * chunks * heads
-    row = lax.broadcasted_iota(jnp.int32, (max(ROWS, chunks * heads), HEADS), 0)
-    pick = (lax.broadcasted_iota(jnp.int32, row.shape, 1) == row + first_row).astype(bf16)
-    dt_rows = nt(pick, dt_ref[...])
+    dt_rows = dt_ref[...].astype(f32)
     for n in range(saved_ref.shape[1] // cols):
         at = slice(n * cols, (n + 1) * cols)
         values = saved_ref[:, at].astype(f32)
@@ -126,13 +123,16 @@
 
 def weight_kernel(dp, at_ref, *refs):
     grad_refs = refs[:dp]
-    act_refs = refs[dp : 3 * dp]
-    out_refs = refs[3 * dp : -1]
+    act_refs = refs[dp : 2 * dp]
+    far_ref, last_ref = refs[2 * dp : 2 * dp + 2]
+    out_refs = refs[2 * dp + 2 : -1]
     total_ref = refs[-1]
     total = None
     for k in range(dp):
         for part in range(2):
-            term = tn(act_refs[part * dp + k][...], grad_refs[k][part])
+            far = last_ref[...] if k == dp - 1 else far_ref[k]
+            acts = act_refs[k][...] if part == 0 else far
+            term = tn(acts, grad_refs[k][part])
             total = term if total is None else total + term
     total_ref[...] = total
     size = out_refs[0].shape[0]
@@ -154,6 +154,11 @@
             outs[1][rows, lanes] = chunk[:, STATE:]
 
 
+def gather_kernel(at_ref, *refs):
+    for k, ref in enumerate(refs[:-1]):
+        refs[-1][k] = ref[...]
+
+
 def unpack_kernel(back_ref, dx_ref, dt_ref):
     devices, _, width = back_ref.shape
     heads = width // HEAD_DIM
@@ -161,24 +166,7 @@
     for i in range(devices):
         dx_ref[:, i * width : (i + 1) * width] = back_ref[i, :BLOCK, :]
         rows.append(unpack_rows(back_ref[i, BLOCK:, :].astype(f32), heads, width)[:heads])
-    dt_ref[...] = jnp.concatenate(rows, axis=0).T.astype(bf16)
-
-
-def mixer_kernel(
-    devices,
-    at_ref,
-    x_ref,
-    drop_ref,
-    prm_ref,
-    skip_ref,
-    xw_ref,
-    bcw_ref,
-    *refs,
-):
-    bc_refs = refs[:devices]
-    out_ref = refs[devices]
-    dbc_refs = refs[devices + 1 : devices + 1 + devices // 2]
-    mixer_body(at_ref, x_ref, drop_ref, prm_ref, skip_ref, xw_ref, bcw_ref, bc_refs, out_ref, dbc_refs, *refs[devices + 1 + devices // 2 :])
+    dt_ref[...] = jnp.concatenate(rows, axis=0).astype(bf16)
 
 
 def split(value, count):
@@ -189,48 +177,130 @@
     return terms
 
 
-def mixer_body(
-    at_ref,
+def per_head(ref, index):
+    total = jnp.zeros(index.shape, f32)
+    for h in range(ref.shape[0]):
+        total = jnp.where(index == h, ref[h], total)
+    return total
+
+
+def triangle(include):
+    r = lax.broadcasted_iota(jnp.int32, (BLOCK, BLOCK), 0)
+    c = lax.broadcasted_iota(jnp.int32, (BLOCK, BLOCK), 1)
+    return jnp.where(include(r, c), 1.0, 0.0).astype(bf16)
+
+
+def expand(count, width):
+    shape = (count * ROWS, width)
+    r = lax.broadcasted_iota(jnp.int32, shape, 0) % ROWS
+    c = lax.broadcasted_iota(jnp.int32, shape, 1) // HEAD_DIM
+    return jnp.where(r == c, 1.0, 0.0)
+
+
+PAD = 8
+
+
+def conv(pad_ref, b, w_ref, flip):
+    win = pad_ref[pl.ds(pl.multiple_of(b * BLOCK, BLOCK), BLOCK + 2 * PAD), :]
+    total = None
+    for k in range(CONV_K):
+        shift = (CONV_K - 1) // 2 - k
+        moved = win if shift == 0 else pltpu.roll(win, shift % (BLOCK + 2 * PAD), 0)
+        tap = w_ref[CONV_K - 1 - k : CONV_K - k, :] if flip else w_ref[k : k + 1, :]
+        term = moved[PAD : PAD + BLOCK] * tap
+        total = term if total is None else total + term
+    return total
+
+
+def enter_kernel(
+    offset_ref,
+    fading_ref,
     x_ref,
     drop_ref,
-    prm_ref,
-    skip_ref,
     xw_ref,
-    bcw_ref,
-    bc_refs,
-    out_ref,
-    dbc_refs,
+    u_ref,
+    us_ref,
+    row_ref,
+    wide_ref,
+    dr_ref,
+    gg_ref,
     xpad,
-    bcpad,
-    u_s,
-    us_s,
-    kcs_s,
-    kr_s,
-    row_s,
-    wide_s,
-    dr_s,
-    gg_s,
-    st_s,
-    car_s,
-    sel_s,
 ):
     blocks, _, width = x_ref.shape
     heads = width // HEAD_DIM
-    pad = 8
+    all_rows = blocks * ROWS
+    rows_of = lax.broadcasted_iota(jnp.int32, (ROWS, BLOCK), 0)
+    offset = per_head(offset_ref, rows_of)
+    fade = jnp.exp(per_head(fading_ref, rows_of))
+    xpad[0:PAD, :] = jnp.zeros((PAD, width), f32)
+    xpad[PAD + blocks * BLOCK :, :] = jnp.zeros((PAD, width), f32)
+
+    def load_block(b, _):
+        at = pl.multiple_of(b * BLOCK, BLOCK) + PAD
+        xpad[pl.ds(at, BLOCK), :] = x_ref[b, :BLOCK, :].astype(f32)
+        lines = x_ref[b, 2 * BLOCK :, :].astype(f32)
+        row_ref[0, b] = unpack_rows(lines, heads, width) + offset
+        drop = drop_ref[:, pl.ds(pl.multiple_of(b * BLOCK, BLOCK), BLOCK)]
+        row_ref[1, b] = jnp.concatenate([drop, jnp.zeros((ROWS - heads, BLOCK), f32)], axis=0)
+        return 0
+
+    lax.fori_loop(0, blocks, load_block, 0)
+    raw = row_ref[0].reshape(all_rows, BLOCK)
+    dt = jnp.maximum(raw, 0.0) + jnp.log1p(jnp.exp(-jnp.abs(raw)))
+    rate = (dt.reshape(blocks, ROWS, BLOCK) * fade[None] + row_ref[1]).reshape(all_rows, BLOCK)
+    sums = nn(jnp.concatenate(split(rate, 3), axis=0), triangle(lambda r, c: r <= c))
+    cum = sums[:all_rows] + sums[all_rows : 2 * all_rows] + sums[2 * all_rows :]
+    total = cum[:, BLOCK - 1 :]
+    row_ref[0] = dt.reshape(blocks, ROWS, BLOCK)
+    row_ref[1] = cum.reshape(blocks, ROWS, BLOCK)
+    row_ref[2] = jnp.exp(-cum).reshape(blocks, ROWS, BLOCK)
+    row_ref[3] = jnp.exp(cum - total).reshape(blocks, ROWS, BLOCK)
+    row_ref[4] = (1.0 / (1.0 + jnp.exp(-raw))).reshape(blocks, ROWS, BLOCK)
+
+    def body(b, _):
+        pre = conv(xpad, b, xw_ref, False)
+        sig = 1.0 / (1.0 + jnp.exp(-pre))
+        u = pre * sig
+        u_ref[b] = u
+        us_ref[b] = sig * (1.0 + pre * (1.0 - sig))
+        rows = jnp.concatenate([row_ref[0, b], row_ref[2, b], row_ref[3, b]], axis=1)
+        wide = tn(jnp.concatenate(split(rows, 3), axis=0), expand(3, width).astype(bf16))
+        wide_ref[b] = wide
+        w_in = wide[BLOCK : 2 * BLOCK]
+        w_out = wide[2 * BLOCK :]
+        driven = u * wide[:BLOCK]
+        g = x_ref[b, BLOCK : 2 * BLOCK, :].astype(f32)
+        dr_ref[b] = jnp.concatenate([driven * w_out, driven * w_in], axis=1).astype(bf16)
+        gg_ref[b] = jnp.concatenate([g * w_in, g * w_out], axis=1).astype(bf16)
+        return 0
+
+    lax.fori_loop(0, blocks, body, 0, unroll=2)
+
+
+def mixer_kernel(
+    devices,
+    at_ref,
+    fading_ref,
+    direct_ref,
+    *refs,
+):
+    x_ref, u_s, us_s, rows_in, wide_s, dr_s, gg_s, xw_ref, write_ref, read_ref = refs[:10]
+    bc_refs = refs[10 : 10 + devices]
+    refs = refs[10 + devices :]
+    out_ref = refs[0]
+    dbc_refs = refs[1 : 1 + devices // 2]
+    xpad, bcpad, kcs_s, kr_s, row_s, st_s, car_s, sel_s, bcw_ref = refs[1 + devices // 2 :]
+    blocks, _, width = x_ref.shape
+    heads = width // HEAD_DIM
+    pad = PAD
     lanes = min(width, BLOCK)
     per = lanes // HEAD_DIM
     all_rows = blocks * ROWS
-
-    def triangle(include):
-        r = lax.broadcasted_iota(jnp.int32, (BLOCK, BLOCK), 0)
-        c = lax.broadcasted_iota(jnp.int32, (BLOCK, BLOCK), 1)
-        return jnp.where(include(r, c), 1.0, 0.0).astype(bf16)
-
-    def expand(count):
-        shape = (count * ROWS, width)
-        r = lax.broadcasted_iota(jnp.int32, shape, 0) % ROWS
-        c = lax.broadcasted_iota(jnp.int32, shape, 1) // HEAD_DIM
-        return jnp.where(r == c, 1.0, 0.0)
+    fade = jnp.exp(per_head(fading_ref, lax.broadcasted_iota(jnp.int32, (ROWS, BLOCK), 0)))
+
+    mine = pl.ds(pl.multiple_of(at_ref[2] * STATE, STATE), STATE)
+    bcw_ref[:CONV_K, :STATE] = write_ref[:, mine]
+    bcw_ref[:CONV_K, STATE:] = read_ref[:, mine]
 
     r = lax.broadcasted_iota(jnp.int32, (5 * width, BLOCK), 0)
     c = lax.broadcasted_iota(jnp.int32, (5 * width, BLOCK), 1)
@@ -241,41 +311,9 @@
     xpad[pad + blocks * BLOCK :, :] = jnp.zeros((pad, width), f32)
     bcpad[0:pad, :] = jnp.zeros((pad, 2 * STATE), f32)
     bcpad[pad + blocks * BLOCK :, :] = jnp.zeros((pad, 2 * STATE), f32)
-
-    def load_block(b, _):
-        at = pl.multiple_of(b * BLOCK, BLOCK) + pad
-        xpad[pl.ds(at, BLOCK), :] = x_ref[b, :BLOCK, :].astype(f32)
-        row_s[0, b] = unpack_rows(x_ref[b, 2 * BLOCK :, :].astype(f32), heads, width) + prm_ref[0]
-        return 0
-
-    lax.fori_loop(0, blocks, load_block, 0)
     for k, bc_ref in enumerate(bc_refs):
         at = pl.multiple_of((at_ref[1] ^ k) * BLOCK, BLOCK) + pad
         bcpad[pl.ds(at, BLOCK), :] = bc_ref[...].astype(f32)
-
-    raw = row_s[0].reshape(all_rows, BLOCK)
-    dt = jnp.maximum(raw, 0.0) + jnp.log1p(jnp.exp(-jnp.abs(raw)))
-    fade = jnp.exp(prm_ref[1])
-    rate = (dt.reshape(blocks, ROWS, BLOCK) * fade[None] + drop_ref[...]).reshape(all_rows, BLOCK)
-    sums = nn(jnp.concatenate(split(rate, 3), axis=0), triangle(lambda r, c: r <= c))
-    cum = sums[:all_rows] + sums[all_rows : 2 * all_rows] + sums[2 * all_rows :]
-    total = cum[:, BLOCK - 1 :]
-    row_s[0] = dt.reshape(blocks, ROWS, BLOCK)
-    row_s[1] = cum.reshape(blocks, ROWS, BLOCK)
-    row_s[2] = jnp.exp(-cum).reshape(blocks, ROWS, BLOCK)
-    row_s[3] = jnp.exp(cum - total).reshape(blocks, ROWS, BLOCK)
-    row_s[4] = (1.0 / (1.0 + jnp.exp(-raw))).reshape(blocks, ROWS, BLOCK)
-
-    def conv(pad_ref, b, w_ref, flip):
-        win = pad_ref[pl.ds(pl.multiple_of(b * BLOCK, BLOCK), BLOCK + 2 * pad), :]
-        total = None
-        for k in range(CONV_K):
-            shift = (CONV_K - 1) // 2 - k
-            moved = win if shift == 0 else pltpu.roll(win, shift % (BLOCK + 2 * pad), 0)
-            tap = w_ref[CONV_K - 1 - k : CONV_K - k, :] if flip else w_ref[k : k + 1, :]
-            term = moved[pad : pad + BLOCK] * tap
-            total = term if total is None else total + term
-        return total
 
     def first(b, _):
         pre = conv(bcpad, b, bcw_ref, False)
@@ -283,27 +321,11 @@
         act = (pre * sig).astype(bf16)
         kcs_s[b] = sig * (1.0 + pre * (1.0 - sig))
         kr_s[b] = act
-        pre = conv(xpad, b, xw_ref, False)
-        sig = 1.0 / (1.0 + jnp.exp(-pre))
-        u = pre * sig
-        u_s[b] = u
-        us_s[b] = sig * (1.0 + pre * (1.0 - sig))
-        rows = jnp.concatenate([row_s[0, b], row_s[2, b], row_s[3, b]], axis=1)
-        wide = tn(jnp.concatenate(split(rows, 3), axis=0), expand(3).astype(bf16))
-        wide_s[b] = wide
-        w_in = wide[BLOCK : 2 * BLOCK]
-        w_out = wide[2 * BLOCK :]
-        driven = u * wide[:BLOCK]
-        g = x_ref[b, BLOCK : 2 * BLOCK, :].astype(f32)
-        d_io = jnp.concatenate([driven * w_out, driven * w_in], axis=1).astype(bf16)
-        g_io = jnp.concatenate([g * w_in, g * w_out], axis=1).astype(bf16)
-        dr_s[b] = d_io
-        gg_s[b] = g_io
-        st_s[b, :, : 2 * width] = tn(act[:, :STATE], d_io)
-        st_s[b, :, 2 * width :] = tn(act[:, STATE:], g_io)
+        st_s[b, :, : 2 * width] = tn(act[:, :STATE], dr_s[b])
+        st_s[b, :, 2 * width :] = tn(act[:, STATE:], gg_s[b])
         return 0
 
-    lax.fori_loop(0, blocks, first, 0)
+    lax.fori_loop(0, blocks, first, 0, unroll=2)
 
     def scan(slot, back):
         def step(i, carry):
@@ -326,7 +348,7 @@
         reads = act[:, STATE:]
         u = u_s[b]
         g16 = x_ref[b, BLOCK : 2 * BLOCK, :]
-        cum = row_s[1, b]
+        cum = rows_in[1, b]
         cum_t = cum.T
         wide = wide_s[b]
         w_dt = wide[:BLOCK]
@@ -398,26 +420,27 @@
         by_key = by_key.T
         through = jnp.sum(c_s.astype(f32) * c_g.astype(f32), axis=0, keepdims=True)
         through = (through[:, :width] + through[:, width:]) * wide[2 * BLOCK - 1 : 2 * BLOCK]
-        through = jnp.sum(expand(1) * through, axis=1, keepdims=True)
+        through = jnp.sum(expand(1, width) * through, axis=1, keepdims=True)
         before = jnp.sum(sums[ROWS : 2 * ROWS], axis=1, keepdims=True) + through
-        row_s[5, b] = sums[:ROWS] + by_key[:ROWS] - by_read
-        row_s[2, b] = jnp.broadcast_to(before, (ROWS, BLOCK))
-        row_s[3, b] = sums[2 * ROWS : 3 * ROWS]
-        d_u = d_dr * w_dt + g16.astype(f32) * skip_ref[...]
+        row_s[0, b] = sums[:ROWS] + by_key[:ROWS] - by_read
+        row_s[1, b] = jnp.broadcast_to(before, (ROWS, BLOCK))
+        row_s[2, b] = sums[2 * ROWS : 3 * ROWS]
+        skip = per_head(direct_ref, lax.broadcasted_iota(jnp.int32, (1, width), 1) // HEAD_DIM)
+        d_u = d_dr * w_dt + g16.astype(f32) * skip
         at = pl.multiple_of(b * BLOCK, BLOCK) + pad
         xpad[pl.ds(at, BLOCK), :] = d_u * us_s[b]
         bcpad[pl.ds(at, BLOCK), :] = jnp.concatenate([d_k, d_r], axis=1) * kcs_s[b]
         return 0
 
-    lax.fori_loop(0, blocks, second, 0)
+    lax.fori_loop(0, blocks, second, 0, unroll=2)
 
     sums = nn(
-        jnp.concatenate(split(row_s[5].reshape(all_rows, BLOCK), 3), axis=0),
+        jnp.concatenate(split(row_s[0].reshape(all_rows, BLOCK), 3), axis=0),
         triangle(lambda r, c: r >= c),
     )
     sums = sums[:all_rows] + sums[all_rows : 2 * all_rows] + sums[2 * all_rows :]
-    d_rate = -(sums.reshape(blocks, ROWS, BLOCK) + row_s[2])
-    row_s[0] = (row_s[3] + d_rate * fade[None]) * row_s[4]
+    d_rate = -(sums.reshape(blocks, ROWS, BLOCK) + row_s[1])
+    row_s[0] = (row_s[2] + d_rate * fade[None]) * rows_in[4]
 
     for k, dbc_ref in enumerate(dbc_refs):
         for part in range(2):
@@ -432,6 +455,10 @@
     lax.fori_loop(0, blocks, last, 0)
 
 
+def limit(mib):
+    return pltpu.CompilerParams(vmem_limit_bytes=mib << 20)
+
+
 def vmem():
     return pl.BlockSpec(memory_space=pltpu.VMEM)
 
@@ -440,34 +467,52 @@
     return pl.BlockSpec(memory_space=pltpu.SMEM)
 
 
-def run_mixer(at, x, drop, prm, skip, xw, bcw, bc):
+def run_enter(offset, fading, x, drop, xw):
+    blocks, _, width = x.shape
+    shape = jax.ShapeDtypeStruct
+    return pl.pallas_call(
+        enter_kernel,
+        out_shape=(
+            shape((blocks, BLOCK, width), f32),
+            shape((blocks, BLOCK, width), f32),
+            shape((5, blocks, ROWS, BLOCK), f32),
+            shape((blocks, 3 * BLOCK, width), f32),
+            shape((blocks, BLOCK, 2 * width), bf16),
+            shape((blocks, BLOCK, 2 * width), bf16),
+        ),
+        in_specs=[smem()] * 2 + [vmem()] * 3,
+        out_specs=(vmem(),) * 6,
+        scratch_shapes=[pltpu.VMEM((blocks * BLOCK + 2 * PAD, width), f32)],
+        compiler_params=limit(24),
+        name="enter",
+    )(offset, fading, x, drop, xw)
+
+
+def run_mixer(at, fading, direct, x, entered, filters, bc):
     blocks, _, width = x.shape
     length = blocks * BLOCK
     scratch = [
-        pltpu.VMEM((length + 16, width), f32),
-        pltpu.VMEM((length + 16, 2 * STATE), f32),
-        pltpu.VMEM((blocks, BLOCK, width), f32),
-        pltpu.VMEM((blocks, BLOCK, width), f32),
+        pltpu.VMEM((length + 2 * PAD, width), f32),
+        pltpu.VMEM((length + 2 * PAD, 2 * STATE), f32),
         pltpu.VMEM((blocks, BLOCK, 2 * STATE), f32),
         pltpu.VMEM((blocks, BLOCK, 2 * STATE), bf16),
-        pltpu.VMEM((6, blocks, ROWS, BLOCK), f32),
-        pltpu.VMEM((blocks, 3 * BLOCK, width), f32),
-        pltpu.VMEM((blocks, BLOCK, 2 * width), bf16),
-        pltpu.VMEM((blocks, BLOCK, 2 * width), bf16),
+        pltpu.VMEM((3, blocks, ROWS, BLOCK), f32),
         pltpu.VMEM((blocks, STATE, 4 * width), f32),
         pltpu.VMEM((blocks, STATE, 4 * width), bf16),
         pltpu.VMEM((5 * width, BLOCK), bf16),
+        pltpu.VMEM((ROWS, 2 * STATE), f32),
     ]
     half = len(bc) // 2
     outs = pl.pallas_call(
         functools.partial(mixer_kernel, len(bc)),
         out_shape=(jax.ShapeDtypeStruct((blocks, BLOCK + EXTRA, width), bf16),)
         + (jax.ShapeDtypeStruct((2, BLOCK, 2 * STATE), bf16),) * half,
-        in_specs=[smem()] + [vmem()] * (6 + len(bc)),
+        in_specs=[smem()] * 3 + [vmem()] * (10 + len(bc)),
         out_specs=(vmem(),) * (1 + half),
         scratch_shapes=scratch,
+        compiler_params=limit(36),
         name="mixer",
-    )(at, x, drop, prm, skip, xw, bcw, *bc)
+    )(at, fading, direct, x, *entered, *filters, *bc)
     return outs[0], outs[1:]
 
 
@@ -484,6 +529,7 @@
         in_specs=specs,
         out_specs=jax.tree.map(lambda _: vmem(), outs),
         scratch_shapes=scratch,
+        compiler_params=limit(16),
     )(*args)
 
 
@@ -530,7 +576,8 @@
     pieces = {0: weights}
     bit = dp // 2
     while bit:
-        pieces.update({k ^ bit: swap(v, "dp", bit) for k, v in list(pieces.items())})
+        moved = {k ^ bit: swap(v, "dp", bit) for k, v in list(pieces.items())}
+        pieces.update(moved)
         bit //= 2
     pieces = [pieces[k] for k in range(dp)]
 
@@ -546,7 +593,7 @@
             row_spec,
             pl.BlockSpec((1, wide), lambda i: (0, i)),
             row_spec,
-            pl.BlockSpec((tokens, HEADS), lambda i: (0, 0)),
+            pl.BlockSpec((HEADS // steps, tokens), lambda i: (i, 0)),
         ],
         out_specs=(
             pl.BlockSpec((sp // steps, 2 * BLOCK + EXTRA, width), lambda i: (i, 0, 0)),
@@ -563,14 +610,14 @@
         final_adjoint[0],
         rescale_factor[None],
         source_unfiltered[0],
-        delta_raw[0],
+        delta_raw[0].T,
     )
     heads_x = lax.all_to_all(packed, "sp", 0, 0, tiled=True)
 
     acts = [lax.dynamic_slice(rows, (0, (me_d ^ k) * share), (tokens, share)) for k in range(dp)]
     acts = [acts[0]] + [swap(acts[k], "dp", k) for k in range(1, dp)]
-    for k in range(dp):
-        acts.append(swap(acts[k], "sp", half))
+    gathered = call(gather_kernel, shape((dp - 1, tokens, share), bf16), at, *acts[: dp - 1])
+    acts += [swap(gathered, "sp", half), swap(acts[dp - 1], "sp", half)]
 
     bc = shape((tokens, 2 * STATE), bf16)
     own, other = call(proj_kernel, (bc, bc), at, rows, *pieces)
@@ -578,19 +625,11 @@
     all_bc = [own if k == 0 else swap(own, "sp", k) for k in range(half)]
     all_bc += [other if k == 0 else swap(other, "sp", k) for k in range(half)]
 
-    blocks = heads_x.shape[0]
-    drop = jnp.pad(
-        extra_logdrop[0].reshape(blocks, BLOCK, heads).transpose(0, 2, 1),
-        ((0, 0), (0, ROWS - heads), (0, 0)),
-    )
-    prm = jnp.pad(jnp.stack([delta_offset, fading_exponents]), ((0, 0), (0, ROWS - heads)))
-    prm = jnp.broadcast_to(prm[:, :, None], (2, ROWS, BLOCK))
-    skip = jnp.repeat(direct_factor, HEAD_DIM)[None]
-    bcw = jnp.stack([writer_filter_coefs, reader_filter_coefs], axis=1)
-    bcw = bcw.reshape(CONV_K, 2, GROUPS, STATE)
-    bcw = lax.dynamic_index_in_dim(bcw, at[2], 2, keepdims=False).reshape(CONV_K, 2 * STATE)
-
-    d_x, d_bc = run_mixer(at, heads_x, drop, prm, skip, source_filter_coefs, bcw, all_bc)
+    entered = run_enter(
+        delta_offset, fading_exponents, heads_x, extra_logdrop[0].T, source_filter_coefs
+    )
+    filters = (source_filter_coefs, writer_filter_coefs, reader_filter_coefs)
+    d_x, d_bc = run_mixer(at, fading_exponents, direct_factor, heads_x, entered, filters, all_bc)
 
     parts = [d_bc[0]] + [swap(d_bc[k], "sp", k) for k in range(1, half)]
     grads = functools.reduce(jnp.add, [p.astype(f32) for p in parts]).astype(bf16)
@@ -616,14 +655,15 @@
     d_hidden = call(hidden_kernel, shape((tokens, width_in), bf16), at, grads[0], rest, *pieces)
     d_source, d_delta = pl.pallas_call(
         unpack_kernel,
-        out_shape=(shape((tokens, INNER), bf16), shape((tokens, HEADS), bf16)),
+        out_shape=(shape((tokens, INNER), bf16), shape((HEADS, tokens), bf16)),
         in_specs=[vmem()],
         out_specs=(vmem(), vmem()),
+        compiler_params=limit(16),
         name="unpack",
     )(back_x)
     matrix = shape((share, GROUPS * STATE), f32)
     d_w_b, d_w_c = call(functools.partial(spread_kernel, half), (matrix, matrix), at, *placed)
-    return d_hidden[None], d_source[None], d_gate[None], d_delta[None], d_w_b, d_w_c
+    return d_hidden[None], d_source[None], d_gate[None], d_delta.T[None], d_w_b, d_w_c
 
 
 def solution(mesh):

time: 148 us -> 144 us (0.973)
  waiting for transfers between devices: 50.6 us -> 56.9 us
  Pallas kernels: 33.7 us -> 28 us
  starting transfers between devices: 48.6 us -> 45.9 us
    ppermute x34 -> x32, waiting for transfers between devices: 50.6 us -> 56.9 us  [swap(): return lax.ppermute(value, axis, [(i, i ^ bits) for i in range(size)])]
    pallas_call x1, Pallas kernels: 16.4 us -> 11.6 us  [run_mixer(): pl.pallas_call(functools.partial(mixer_kernel, len(bc)), out_shape=(jax.S...]
    unnamed x91 -> x46, local copies, waits for them, and re-layouts: 6.95 us -> 10.6 us
    ppermute x34 -> x32, starting transfers between devices: 37.7 us -> 34.8 us  [swap(): return lax.ppermute(value, axis, [(i, i ^ bits) for i in range(size)])]
    pallas_call x0 -> x1, Pallas kernels: none -> 2.73 us  [run_enter(): pl.pallas_call(enter_kernel, out_shape=(shape((blocks, BLOCK, width), f32...]
    pallas_call x4 -> x5, Pallas kernels: 11.1 us -> 8.48 us  [call(): pl.pallas_call(kernel, out_shape=outs, in_specs=specs, out_specs=jax.tree...]
    squeeze x1, local copies, waits for them, and re-layouts: 1.5 us -> 0.01 us  [local(): rest = swap(grads[1], 'sp', half)]
  transfers between devices with their start and end apart: 36 -> 34, of which waited for: 13 -> 9; matrix products, arithmetic and copies ran while one was open for 5% -> 1% of each run, Pallas kernels for 19% -> 16%
where the time goes in v1:
time: 144 us; the launch traced here: 143 us
  waiting for transfers between devices  56.9 us (40%)
  starting transfers between devices  45.9 us (32%)
  Pallas kernels  28 us (19%)
  local copies, waits for them, and re-layouts  11.4 us (8%)
    ppermute x32, waiting for transfers between devices, swap(): return lax.ppermute(value, axis, [(i, i ^ bits) for i in range(size)])  56.9 us
    ppermute x32, starting transfers between devices, swap(): return lax.ppermute(value, axis, [(i, i ^ bits) for i in range(size)])  34.8 us
    pallas_call x1, Pallas kernels, run_mixer(): pl.pallas_call(functools.partial(mixer_kernel, len(bc)), out_shape=(jax.S...  11.6 us
    unnamed x46, local copies, waits for them, and re-layouts  10.6 us
    pallas_call x5, Pallas kernels, call(): pl.pallas_call(kernel, out_shape=outs, in_specs=specs, out_specs=jax.tree...  8.48 us
    all_to_all x1, starting transfers between devices, local(): heads_x = lax.all_to_all(packed, 'sp', 0, 0, tiled=True)  7.42 us
    pallas_call x1, Pallas kernels, local(): pl.pallas_call(prep_kernel, grid=(steps,), in_specs=[row_spec, row_spec,...  4.29 us
    all_to_all x1, starting transfers between devices, local(): back_x = lax.all_to_all(d_x, 'sp', 0, 0, tiled=True)  3.68 us
  transfers between devices with their start and end apart: 34, of which 9 were waited for; matrix products, arithmetic and copies ran while one was open for 1% of the time, Pallas kernels for 16%

profile of v1, /device:TPU:0, one launch (start us, length us, event | category | flops | bytes accessed | tf_op | source)
XLA Modules:
  0.0 143.3 jit_solution(6361360196978698801)
XLA Ops:
  0.6 4.3 %prep.1 = (bf16[8,272,256]{2,1,0:T(8,128)(2,1)}, bf16[128,2048]{1,0:T(8,128)(2,1)}) custom-call(bf16[128,2048]{1,0:T(8,128)(2,1)} %bitcast.36, bf16[128,2048]{1,0:T(8,128)(2,1)} %bitcast.37, bf16[128,2048]{1,0:T(8,128)(2,1)} %bitcast.38, f32[1,2048]{1,0:T(1,128)} %bitcast.41, bf16[128,2048]{1,0:T(8,128)(2,1)} %bitcast.39, bf16[32,128]{1,0:T(8,128)(2,1)} %bitcast.42), custom_call_target="tpu_custom_call" | custom-call | tf_op jit(solution)/shard_map/prep/pallas_call | solution.py:587
  4.9 7.4 %all-to-all-start = ((bf16[8,272,256]{2,1,0:T(8,128)(2,1)}), bf16[8,272,256]{2,1,0:T(8,128)(2,1)S(1)}, u32[]{:S(2)}, u32[]{:S(2)}) async-start(bf16[8,272,256]{2,1,0:T(8,128)(2,1)} %get-tuple-element.29), calls=%async_computation | async-start | bytes 2228224 | tf_op jit(solution)/shard_map/all_to_all | solution.py:615
  12.6 1.6 %collective-permute-start.1 = (bf16[512,512]{1,0:T(8,128)(2,1)S(1)}, bf16[512,512]{1,0:T(8,128)(2,1)S(1)}, u32[]{:S(2)}, u32[]{:S(2)}) collective-permute-start(bf16[512,512]{1,0:T(8,128)(2,1)S(1)} %pad_maximum_fusion.refs_0_), channel_id=1, source_target_pairs={{0,2},{1,3},{2,0},{3,1},{4,6},{5,7},{6,4},{7,5},{8,10},{9,11},{10,... | collective-permute-start | bytes 1572872 | tf_op jit(solution)/shard_map/ppermute | solution.py:521
  14.1 11.9 %collective-permute-done.1.refs_2_ = bf16[512,512]{1,0:T(8,128)(2,1)S(1)} collective-permute-done((bf16[512,512]{1,0:T(8,128)(2,1)S(1)}, bf16[512,512]{1,0:T(8,128)(2,1)S(1)}, u32[]{:S(2)}, u32[]{:S(2)}) %collective-permute-start.1) | collective-permute-done | bytes 524320 | tf_op jit(solution)/shard_map/ppermute | solution.py:521
  26.1 2.0 %collective-permute-done.2.refs_3_ = bf16[512,512]{1,0:T(8,128)(2,1)} collective-permute-done((bf16[512,512]{1,0:T(8,128)(2,1)S(1)}, bf16[512,512]{1,0:T(8,128)(2,1)}, u32[]{:S(2)}, u32[]{:S(2)}) %collective-permute-start.2) | collective-permute-done | bytes 524320 | tf_op jit(solution)/shard_map/ppermute | solution.py:521
  28.1 1.6 %shard_map.199 = (bf16[128,256]{1,0:T(8,128)(2,1)S(1)}, bf16[128,256]{1,0:T(8,128)(2,1)S(1)}) custom-call(s32[4]{0:T(128)S(1)} %pad_add_fusion.at_ref, bf16[128,2048]{1,0:T(8,128)(2,1)S(1)} %bitcast.34, bf16[512,512]{1,0:T(8,128)(2,1)S(1)} %pad_maximum_fusion.refs_0_, bf16[512,512]{1,0:T(8,128)(2,1)S(1)} %collective-permute-done.refs_1_, ...), custom_call_target="tpu_custom_call" | custom-call | tf_op jit(solution)/shard_map/pallas_call | solution.py:526
  29.6 1.8 %collective-permute-start.3 = (bf16[128,256]{1,0:T(8,128)(2,1)S(1)}, bf16[128,256]{1,0:T(8,128)(2,1)S(1)}, u32[]{:S(2)}, u32[]{:S(2)}) collective-permute-start(bf16[128,256]{1,0:T(8,128)(2,1)S(1)} %get-tuple-element.36.refs_10_), channel_id=1, source_target_pairs={{0,4},{4,0},{8,12},{12,8},{16,20},{20,16},{24,28},{28,24},{1,5},{5... | collective-permute-start | bytes 196616 | tf_op jit(solution)/shard_map/ppermute | solution.py:521
  31.4 1.5 %collective-permute-start.4 = (bf16[128,256]{1,0:T(8,128)(2,1)S(1)}, bf16[128,256]{1,0:T(8,128)(2,1)S(1)}, u32[]{:S(2)}, u32[]{:S(2)}) collective-permute-start(bf16[128,256]{1,0:T(8,128)(2,1)S(1)} %get-tuple-element.36.refs_10_), channel_id=1, source_target_pairs={{0,8},{4,12},{8,0},{12,4},{16,24},{20,28},{24,16},{28,20},{1,9},{5... | collective-permute-start | bytes 196616 | tf_op jit(solution)/shard_map/ppermute | solution.py:521
  32.9 2.4 %collective-permute-start.6 = (bf16[128,256]{1,0:T(8,128)(2,1)S(1)}, bf16[128,256]{1,0:T(8,128)(2,1)}, u32[]{:S(2)}, u32[]{:S(2)}) collective-permute-start(bf16[128,256]{1,0:T(8,128)(2,1)S(1)} %get-tuple-element.37), channel_id=1, source_target_pairs={{0,16},{4,20},{8,24},{12,28},{16,0},{20,4},{24,8},{28,12},{1,17},{... | collective-permute-start | bytes 196616 | tf_op jit(solution)/shard_map/ppermute | solution.py:521
  35.2 0.7 dynamic-slice_bitcast_fusion
  36.5 6.0 %collective-permute-done.6.refs_14_ = bf16[128,256]{1,0:T(8,128)(2,1)} collective-permute-done((bf16[128,256]{1,0:T(8,128)(2,1)S(1)}, bf16[128,256]{1,0:T(8,128)(2,1)}, u32[]{:S(2)}, u32[]{:S(2)}) %collective-permute-start.6) | collective-permute-done | bytes 65568 | tf_op jit(solution)/shard_map/ppermute | solution.py:521
  42.5 1.4 collective-permute-start.7
  45.2 2.1 %collective-permute-start.9 = (bf16[128,256]{1,0:T(8,128)(2,1)}, bf16[128,256]{1,0:T(8,128)(2,1)S(1)}, u32[]{:S(2)}, u32[]{:S(2)}) collective-permute-start(bf16[128,256]{1,0:T(8,128)(2,1)} %collective-permute-done.6.refs_14_), channel_id=1, source_target_pairs={{0,12},{4,8},{8,4},{12,0},{16,28},{20,24},{24,20},{28,16},{1,13},{... | collective-permute-start | bytes 196616 | tf_op jit(solution)/shard_map/ppermute | solution.py:521
  47.9 1.5 %collective-permute-start.18 = (bf16[128,512]{1,0:T(8,128)(2,1)}, bf16[128,512]{1,0:T(8,128)(2,1)}, u32[]{:S(2)}, u32[]{:S(2)}) collective-permute-start(bf16[128,512]{1,0:T(8,128)(2,1)} %get-tuple-element.55), channel_id=1, source_target_pairs={{0,2},{1,3},{2,0},{3,1},{4,6},{5,7},{6,4},{7,5},{8,10},{9,11},{10,... | collective-permute-start | bytes 393224 | tf_op jit(solution)/shard_map/ppermute | solution.py:521
  49.5 0.7 copy-done.15
  50.9 2.7 %enter.1 = (f32[8,128,256]{2,1,0:T(8,128)S(1)}, f32[8,128,256]{2,1,0:T(8,128)S(1)}, f32[5,8,8,128]{3,2,1,0:T(8,128)S(1)}, f32[8,384,256]{2,1,0:T(8,128)S(1)}, bf...) custom-call(f32[4]{0:T(128)S(1)} %copy-done.19, f32[4]{0:T(128)S(1)} %copy-done.18, ...), custom_call_target="tpu_custom_call" | custom-call | tf_op jit(solution)/shard_map/enter/pallas_call | solution.py:473
  55.5 0.8 copy-done.9
  56.4 0.8 copy-done.11
  57.2 0.8 copy-done.13
  58.0 0.7 copy-done.16
  58.7 0.7 copy-done.17
  60.1 11.6 %mixer.1 = (bf16[8,144,256]{2,1,0:T(8,128)(2,1)S(1)}, bf16[2,128,256]{2,1,0:T(8,128)(2,1)S(1)}, bf16[2,128,256]{2,1,0:T(8,128)(2,1)S(1)}, bf16[2,128,256]{2,1,0:T(8,128)(2,1)}, bf16[2,128,256]{2,1,0:T(8,128)(2,1)}) custom-call(s32[4]{0:T(128)S(1)} %pad_add_fusion.at_ref, f32[4]{0:T(128)S(1)} %copy-done.18, f32[4]{0:T(128)S(1)} %copy-done.20, ...), custom_call_target="tpu_custom_call" | custom-call | tf_op jit(solution)/shard_map/mixer/pallas_call | solution.py:506
  71.7 0.8 copy-done.1
  72.5 1.4 collective-permute-start.10
  74.0 2.1 %collective-permute-start.12 = (bf16[2,128,256]{2,1,0:T(8,128)(2,1)}, bf16[2,128,256]{2,1,0:T(8,128)(2,1)S(1)}, u32[]{:S(2)}, u32[]{:S(2)}) collective-permute-start(bf16[2,128,256]{2,1,0:T(8,128)(2,1)} %get-tuple-element.41), channel_id=1, source_target_pairs={{0,12},{4,8},{8,4},{12,0},{16,28},{20,24},{24,20},{28,16},{1,13},{... | collective-permute-start | bytes 393224 | tf_op jit(solution)/shard_map/ppermute | solution.py:521
  76.0 3.7 %all-to-all-start.1 = ((bf16[8,144,256]{2,1,0:T(8,128)(2,1)}), bf16[8,144,256]{2,1,0:T(8,128)(2,1)S(1)}, u32[]{:S(2)}, u32[]{:S(2)}) async-start(bf16[8,144,256]{2,1,0:T(8,128)(2,1)} %copy-done.1), calls=%async_computation.1 | async-start | bytes 1179648 | tf_op jit(solution)/shard_map/all_to_all | solution.py:636
  79.7 0.9 shard_map.201
  80.7 3.0 %collective-permute-start.20 = (bf16[3,128,512]{2,1,0:T(8,128)(2,1)S(1)}, bf16[3,128,512]{2,1,0:T(8,128)(2,1)S(1)}, u32[]{:S(2)}, u32[]{:S(2)}) collective-permute-start(bf16[3,128,512]{2,1,0:T(8,128)(2,1)S(1)} %shard_map.201), channel_id=1, source_target_pairs={{0,16},{4,20},{8,24},{12,28},{16,0},{20,4},{24,8},{28,12},{1,17},{... | collective-permute-start | bytes 1179656 | tf_op jit(solution)/shard_map/ppermute | solution.py:521
  84.5 1.3 collective-permute-start.16
  85.8 32.3 %collective-permute-done.21.refs_9_ = bf16[128,512]{1,0:T(8,128)(2,1)S(1)} collective-permute-done((bf16[128,512]{1,0:T(8,128)(2,1)}, bf16[128,512]{1,0:T(8,128)(2,1)S(1)}, u32[]{:S(2)}, u32[]{:S(2)}) %collective-permute-start.21) | collective-permute-done | bytes 131104 | tf_op jit(solution)/shard_map/ppermute | solution.py:521
  118.1 1.7 %shard_map.202 = (bf16[128,256]{1,0:T(8,128)(2,1)S(1)}, bf16[128,256]{1,0:T(8,128)(2,1)S(1)}, bf16[128,256]{1,0:T(8,128)(2,1)S(1)}, bf16[128,256]{1,0:T(8,128)(2,1)S(1)}) custom-call(s32[4]{0:T(128)S(1)} %pad_add_fusion.at_ref, bf16[2,128,256]{2,1,0:T(8,128)(2,1)S(1)} %add_convert_fusion.refs_0_, bf16[2,128,256]{2,1,0:T(8,128)(2,1)S(1)} %collective-permute-done.14.refs_1_, ...), custom_call_target="tpu_custom_call" | custom-call | tf_op jit(solution)/shard_map/pallas_call | solution.py:526
  119.8 1.5 %collective-permute-start.22 = (bf16[128,256]{1,0:T(8,128)(2,1)S(1)}, bf16[128,256]{1,0:T(8,128)(2,1)S(1)}, u32[]{:S(2)}, u32[]{:S(2)}) collective-permute-start(bf16[128,256]{1,0:T(8,128)(2,1)S(1)} %get-tuple-element.47), channel_id=1, source_target_pairs={{0,4},{4,0},{8,12},{12,8},{16,20},{20,16},{24,28},{28,24},{1,5},{5... | collective-permute-start | bytes 196616 | tf_op jit(solution)/shard_map/ppermute | solution.py:521
  121.4 2.0 %collective-permute-start.24 = (bf16[128,256]{1,0:T(8,128)(2,1)S(1)}, bf16[128,256]{1,0:T(8,128)(2,1)S(1)}, u32[]{:S(2)}, u32[]{:S(2)}) collective-permute-start(bf16[128,256]{1,0:T(8,128)(2,1)S(1)} %get-tuple-element.49), channel_id=1, source_target_pairs={{0,12},{4,8},{8,4},{12,0},{16,28},{20,24},{24,20},{28,16},{1,13},{... | collective-permute-start | bytes 196616 | tf_op jit(solution)/shard_map/ppermute | solution.py:521
  123.4 1.5 %collective-permute-done.22 = bf16[128,256]{1,0:T(8,128)(2,1)S(1)} collective-permute-done((bf16[128,256]{1,0:T(8,128)(2,1)S(1)}, bf16[128,256]{1,0:T(8,128)(2,1)S(1)}, u32[]{:S(2)}, u32[]{:S(2)}) %collective-permute-start.22) | collective-permute-done | bytes 65568 | tf_op jit(solution)/shard_map/ppermute | solution.py:521
  124.9 0.8 collective-permute-done.23
  125.7 0.9 collective-permute-done.24
  126.6 2.1 %collective-permute-start.28 = (bf16[128,256]{1,0:T(8,128)(2,1)S(1)}, bf16[128,256]{1,0:T(8,128)(2,1)S(1)}, u32[]{:S(2)}, u32[]{:S(2)}) collective-permute-start(bf16[128,256]{1,0:T(8,128)(2,1)S(1)} %add_convert_fusion.1.refs_0_), channel_id=1, source_target_pairs={{0,16},{4,20},{8,24},{12,28},{16,0},{20,4},{24,8},{28,12},{1,17},{... | collective-permute-start | bytes 196616 | tf_op jit(solution)/shard_map/ppermute | solution.py:521
  128.7 0.9 collective-permute-start.13
  129.6 1.3 collective-permute-start.25
  130.9 1.3 collective-permute-start.26
  132.2 0.9 collective-permute-start.27
  133.1 1.3 collective-permute-start.29
  134.4 1.2 collective-permute-start.30
  135.7 1.0 collective-permute-start.31
  136.6 2.7 %shard_map.200 = bf16[128,2048]{1,0:T(8,128)(2,1)} custom-call(s32[4]{0:T(128)S(1)} %pad_add_fusion.at_ref, bf16[128,256]{1,0:T(8,128)(2,1)S(1)} %get-tuple-element.61.own_ref, bf16[128,256]{1,0:T(8,128)(2,1)S(1)} %collective-permute-done.13.other_ref, bf16[512,512]{1,0:T(8,128)(2,1)S(1)} %pad_maximum_fusion.refs_0_, ...), custom_call_target="tpu_custom_call" | custom-call | tf_op jit(solution)/shard_map/pallas_call | solution.py:526
  139.3 1.5 %collective-permute-done.31.refs_7_ = bf16[128,256]{1,0:T(8,128)(2,1)S(1)} collective-permute-done((bf16[128,256]{1,0:T(8,128)(2,1)S(1)}, bf16[128,256]{1,0:T(8,128)(2,1)S(1)}, u32[]{:S(2)}, u32[]{:S(2)}) %collective-permute-start.31) | collective-permute-done | bytes 65568 | tf_op jit(solution)/shard_map/ppermute | solution.py:521
  140.8 1.6 %shard_map.203 = (f32[512,256]{1,0:T(8,128)}, f32[512,256]{1,0:T(8,128)}) custom-call(s32[4]{0:T(128)S(1)} %pad_add_fusion.at_ref, bf16[128,256]{1,0:T(8,128)(2,1)S(1)} %add_convert_fusion.1.refs_0_, bf16[128,256]{1,0:T(8,128)(2,1)S(1)} %collective-permute-done.25.refs_1_, bf16[128,256]{1,0:T(8,128)(2,1)S(1)} %collective-permute-done.26.refs_2_, ...), custom_call_target="tpu_custom_call" | custom-call | tf_op jit(solution)/shard_map/pallas_call | solution.py:526
  142.4 0.9 unpack.1
  (82 shorter events, 6.9 us)
Async XLA Ops:
  4.9 7.4 %copy-start.21 = (bf16[512,256]{1,0:T(8,128)(2,1)S(1)}, bf16[512,256]{1,0:T(8,128)(2,1)}, u32[]{:S(2)}) copy-start(bf16[512,256]{1,0:T(8,128)(2,1)} %param.17) | copy-start | bytes 786436
  4.9 7.4 %copy-start.22 = (bf16[512,256]{1,0:T(8,128)(2,1)S(1)}, bf16[512,256]{1,0:T(8,128)(2,1)}, u32[]{:S(2)}) copy-start(bf16[512,256]{1,0:T(8,128)(2,1)} %param.18) | copy-start | bytes 786436
  4.9 44.5 %all-to-all-start = ((bf16[8,272,256]{2,1,0:T(8,128)(2,1)}), bf16[8,272,256]{2,1,0:T(8,128)(2,1)S(1)}, u32[]{:S(2)}, u32[]{:S(2)}) async-start(bf16[8,272,256]{2,1,0:T(8,128)(2,1)} %get-tuple-element.29), calls=%async_computation | async-start | bytes 2228224 | tf_op jit(solution)/shard_map/all_to_all | solution.py:615
  12.4 15.7 %copy-start = (bf16[1,128,2048]{2,1,0:T(8,128)(2,1)S(1)}, bf16[1,128,2048]{2,1,0:T(8,128)(2,1)}, u32[]{:S(2)}) copy-start(bf16[1,128,2048]{2,1,0:T(8,128)(2,1)} %param.16) | copy-start | bytes 1572868
  12.6 13.4 %collective-permute-start.1 = (bf16[512,512]{1,0:T(8,128)(2,1)S(1)}, bf16[512,512]{1,0:T(8,128)(2,1)S(1)}, u32[]{:S(2)}, u32[]{:S(2)}) collective-permute-start(bf16[512,512]{1,0:T(8,128)(2,1)S(1)} %pad_maximum_fusion.refs_0_), channel_id=1, source_target_pairs={{0,2},{1,3},{2,0},{3,1},{4,6},{5,7},{6,4},{7,5},{8,10},{9,11},{10,... | collective-permute-start | bytes 1572872 | tf_op jit(solution)/shard_map/ppermute | solution.py:521
  14.1 11.9 %collective-permute-start = (bf16[512,512]{1,0:T(8,128)(2,1)S(1)}, bf16[512,512]{1,0:T(8,128)(2,1)S(1)}, u32[]{:S(2)}, u32[]{:S(2)}) collective-permute-start(bf16[512,512]{1,0:T(8,128)(2,1)S(1)} %pad_maximum_fusion.refs_0_), channel_id=1, source_target_pairs={{0,1},{1,0},{2,3},{3,2},{4,5},{5,4},{6,7},{7,6},{8,9},{9,8},{10,11... | collective-permute-start | bytes 1572872 | tf_op jit(solution)/shard_map/ppermute | solution.py:521
  26.0 2.0 %collective-permute-start.2 = (bf16[512,512]{1,0:T(8,128)(2,1)S(1)}, bf16[512,512]{1,0:T(8,128)(2,1)}, u32[]{:S(2)}, u32[]{:S(2)}) collective-permute-start(bf16[512,512]{1,0:T(8,128)(2,1)S(1)} %collective-permute-done.1.refs_2_), channel_id=1, source_target_pairs={{0,1},{1,0},{2,3},{3,2},{4,5},{5,4},{6,7},{7,6},{8,9},{9,8},{10,11... | collective-permute-start | bytes 1572872 | tf_op jit(solution)/shard_map/ppermute | solution.py:521
  28.1 21.4 %copy-start.14 = (f32[5,256]{1,0:T(8,128)S(1)}, f32[5,256]{1,0:T(8,128)}, u32[]{:S(2)}) copy-start(f32[5,256]{1,0:T(8,128)} %refs_7_.1) | copy-start | bytes 15364
  28.1 21.4 %copy-start.18 = (f32[4]{0:T(128)S(1)}, f32[4]{0:T(128)}, u32[]{:S(2)}) copy-start(f32[4]{0:T(128)} %fading_ref.3) | copy-start | bytes 52
  29.6 14.3 %collective-permute-start.3 = (bf16[128,256]{1,0:T(8,128)(2,1)S(1)}, bf16[128,256]{1,0:T(8,128)(2,1)S(1)}, u32[]{:S(2)}, u32[]{:S(2)}) collective-permute-start(bf16[128,256]{1,0:T(8,128)(2,1)S(1)} %get-tuple-element.36.refs_10_), channel_id=1, source_target_pairs={{0,4},{4,0},{8,12},{12,8},{16,20},{20,16},{24,28},{28,24},{1,5},{5... | collective-permute-start | bytes 196616 | tf_op jit(solution)/shard_map/ppermute | solution.py:521
  31.4 13.2 %collective-permute-start.4 = (bf16[128,256]{1,0:T(8,128)(2,1)S(1)}, bf16[128,256]{1,0:T(8,128)(2,1)S(1)}, u32[]{:S(2)}, u32[]{:S(2)}) collective-permute-start(bf16[128,256]{1,0:T(8,128)(2,1)S(1)} %get-tuple-element.36.refs_10_), channel_id=1, source_target_pairs={{0,8},{4,12},{8,0},{12,4},{16,24},{20,28},{24,16},{28,20},{1,9},{5... | collective-permute-start | bytes 196616 | tf_op jit(solution)/shard_map/ppermute | solution.py:521
  32.9 9.7 %collective-permute-start.6 = (bf16[128,256]{1,0:T(8,128)(2,1)S(1)}, bf16[128,256]{1,0:T(8,128)(2,1)}, u32[]{:S(2)}, u32[]{:S(2)}) collective-permute-start(bf16[128,256]{1,0:T(8,128)(2,1)S(1)} %get-tuple-element.37), channel_id=1, source_target_pairs={{0,16},{4,20},{8,24},{12,28},{16,0},{20,4},{24,8},{28,12},{1,17},{... | collective-permute-start | bytes 196616 | tf_op jit(solution)/shard_map/ppermute | solution.py:521
  36.0 38.0 %collective-permute-start.17 = (bf16[128,512]{1,0:T(8,128)(2,1)S(1)}, bf16[128,512]{1,0:T(8,128)(2,1)S(1)}, u32[]{:S(2)}, u32[]{:S(2)}) collective-permute-start(bf16[128,512]{1,0:T(8,128)(2,1)S(1)} %get-tuple-element.53), channel_id=1, source_target_pairs={{0,1},{1,0},{2,3},{3,2},{4,5},{5,4},{6,7},{7,6},{8,9},{9,8},{10,11... | collective-permute-start | bytes 393224 | tf_op jit(solution)/shard_map/ppermute | solution.py:521
  36.0 11.3 %collective-permute-start.5 = (bf16[128,256]{1,0:T(8,128)(2,1)S(1)}, bf16[128,256]{1,0:T(8,128)(2,1)S(1)}, u32[]{:S(2)}, u32[]{:S(2)}) collective-permute-start(bf16[128,256]{1,0:T(8,128)(2,1)S(1)} %get-tuple-element.36.refs_10_), channel_id=1, source_target_pairs={{0,12},{4,8},{8,4},{12,0},{16,28},{20,24},{24,20},{28,16},{1,13},{... | collective-permute-start | bytes 196616 | tf_op jit(solution)/shard_map/ppermute | solution.py:521
  42.5 11.1 %collective-permute-start.7 = (bf16[128,256]{1,0:T(8,128)(2,1)}, bf16[128,256]{1,0:T(8,128)(2,1)S(1)}, u32[]{:S(2)}, u32[]{:S(2)}) collective-permute-start(bf16[128,256]{1,0:T(8,128)(2,1)} %collective-permute-done.6.refs_14_), channel_id=1, source_target_pairs={{0,4},{4,0},{8,12},{12,8},{16,20},{20,16},{24,28},{28,24},{1,5},{5... | collective-permute-start | bytes 196616 | tf_op jit(solution)/shard_map/ppermute | solution.py:521
  44.6 9.7 %collective-permute-start.8 = (bf16[128,256]{1,0:T(8,128)(2,1)}, bf16[128,256]{1,0:T(8,128)(2,1)S(1)}, u32[]{:S(2)}, u32[]{:S(2)}) collective-permute-start(bf16[128,256]{1,0:T(8,128)(2,1)} %collective-permute-done.6.refs_14_), channel_id=1, source_target_pairs={{0,8},{4,12},{8,0},{12,4},{16,24},{20,28},{24,16},{28,20},{1,9},{5... | collective-permute-start | bytes 196616 | tf_op jit(solution)/shard_map/ppermute | solution.py:521
  44.6 10.9 %copy-start.3 = (bf16[128,256]{1,0:T(8,128)(2,1)S(1)}, bf16[128,256]{1,0:T(8,128)(2,1)}, u32[]{:S(2)}) copy-start(bf16[128,256]{1,0:T(8,128)(2,1)} %copy-done.2) | copy-start | bytes 196612
  45.2 9.6 %collective-permute-start.9 = (bf16[128,256]{1,0:T(8,128)(2,1)}, bf16[128,256]{1,0:T(8,128)(2,1)S(1)}, u32[]{:S(2)}, u32[]{:S(2)}) collective-permute-start(bf16[128,256]{1,0:T(8,128)(2,1)} %collective-permute-done.6.refs_14_), channel_id=1, source_target_pairs={{0,12},{4,8},{8,4},{12,0},{16,28},{20,24},{24,20},{28,16},{1,13},{... | collective-permute-start | bytes 196616 | tf_op jit(solution)/shard_map/ppermute | solution.py:521
  47.9 31.8 %collective-permute-start.18 = (bf16[128,512]{1,0:T(8,128)(2,1)}, bf16[128,512]{1,0:T(8,128)(2,1)}, u32[]{:S(2)}, u32[]{:S(2)}) collective-permute-start(bf16[128,512]{1,0:T(8,128)(2,1)} %get-tuple-element.55), channel_id=1, source_target_pairs={{0,2},{1,3},{2,0},{3,1},{4,6},{5,7},{6,4},{7,5},{8,10},{9,11},{10,... | collective-permute-start | bytes 393224 | tf_op jit(solution)/shard_map/ppermute | solution.py:521
  49.4 6.1 %copy-start.5 = (bf16[128,256]{1,0:T(8,128)(2,1)S(1)}, bf16[128,256]{1,0:T(8,128)(2,1)}, u32[]{:S(2)}) copy-start(bf16[128,256]{1,0:T(8,128)(2,1)} %copy-done.4) | copy-start | bytes 196612
  49.5 6.1 %copy-start.7 = (bf16[128,256]{1,0:T(8,128)(2,1)S(1)}, bf16[128,256]{1,0:T(8,128)(2,1)}, u32[]{:S(2)}) copy-start(bf16[128,256]{1,0:T(8,128)(2,1)} %copy-done.6) | copy-start | bytes 196612
  49.5 0.8 copy-start.15
  54.2 29.4 %collective-permute-start.19 = (bf16[128,512]{1,0:T(8,128)(2,1)}, bf16[128,512]{1,0:T(8,128)(2,1)}, u32[]{:S(2)}, u32[]{:S(2)}) collective-permute-start(bf16[128,512]{1,0:T(8,128)(2,1)} %get-tuple-element.52), channel_id=1, source_target_pairs={{0,3},{1,2},{2,1},{3,0},{4,7},{5,6},{6,5},{7,4},{8,11},{9,10},{10,... | collective-permute-start | bytes 393224 | tf_op jit(solution)/shard_map/ppermute | solution.py:521
  55.5 0.8 copy-start.9
  56.4 0.8 copy-start.11
  57.2 0.8 copy-start.13
  58.0 0.7 copy-start.16
  71.7 0.8 copy-start.1
  72.5 11.2 %collective-permute-start.10 = (bf16[2,128,256]{2,1,0:T(8,128)(2,1)S(1)}, bf16[2,128,256]{2,1,0:T(8,128)(2,1)S(1)}, u32[]{:S(2)}, u32[]{:S(2)}) collective-permute-start(bf16[2,128,256]{2,1,0:T(8,128)(2,1)S(1)} %get-tuple-element.39), channel_id=1, source_target_pairs={{0,4},{4,0},{8,12},{12,8},{16,20},{20,16},{24,28},{28,24},{1,5},{5... | collective-permute-start | bytes 393224 | tf_op jit(solution)/shard_map/ppermute | solution.py:521
  73.9 9.8 %collective-permute-start.11 = (bf16[2,128,256]{2,1,0:T(8,128)(2,1)}, bf16[2,128,256]{2,1,0:T(8,128)(2,1)S(1)}, u32[]{:S(2)}, u32[]{:S(2)}) collective-permute-start(bf16[2,128,256]{2,1,0:T(8,128)(2,1)} %get-tuple-element.40), channel_id=1, source_target_pairs={{0,8},{4,12},{8,0},{12,4},{16,24},{20,28},{24,16},{28,20},{1,9},{5... | collective-permute-start | bytes 393224 | tf_op jit(solution)/shard_map/ppermute | solution.py:521
  74.0 9.8 %collective-permute-start.12 = (bf16[2,128,256]{2,1,0:T(8,128)(2,1)}, bf16[2,128,256]{2,1,0:T(8,128)(2,1)S(1)}, u32[]{:S(2)}, u32[]{:S(2)}) collective-permute-start(bf16[2,128,256]{2,1,0:T(8,128)(2,1)} %get-tuple-element.41), channel_id=1, source_target_pairs={{0,12},{4,8},{8,4},{12,0},{16,28},{20,24},{24,20},{28,16},{1,13},{... | collective-permute-start | bytes 393224 | tf_op jit(solution)/shard_map/ppermute | solution.py:521
  76.0 66.4 %all-to-all-start.1 = ((bf16[8,144,256]{2,1,0:T(8,128)(2,1)}), bf16[8,144,256]{2,1,0:T(8,128)(2,1)S(1)}, u32[]{:S(2)}, u32[]{:S(2)}) async-start(bf16[8,144,256]{2,1,0:T(8,128)(2,1)} %copy-done.1), calls=%async_computation.1 | async-start | bytes 1179648 | tf_op jit(solution)/shard_map/all_to_all | solution.py:636
  80.7 37.4 %collective-permute-start.20 = (bf16[3,128,512]{2,1,0:T(8,128)(2,1)S(1)}, bf16[3,128,512]{2,1,0:T(8,128)(2,1)S(1)}, u32[]{:S(2)}, u32[]{:S(2)}) collective-permute-start(bf16[3,128,512]{2,1,0:T(8,128)(2,1)S(1)} %shard_map.201), channel_id=1, source_target_pairs={{0,16},{4,20},{8,24},{12,28},{16,0},{20,4},{24,8},{28,12},{1,17},{... | collective-permute-start | bytes 1179656 | tf_op jit(solution)/shard_map/ppermute | solution.py:521
  83.6 34.4 %collective-permute-start.21 = (bf16[128,512]{1,0:T(8,128)(2,1)}, bf16[128,512]{1,0:T(8,128)(2,1)S(1)}, u32[]{:S(2)}, u32[]{:S(2)}) collective-permute-start(bf16[128,512]{1,0:T(8,128)(2,1)} %collective-permute-done.19.refs_7_), channel_id=1, source_target_pairs={{0,16},{4,20},{8,24},{12,28},{16,0},{20,4},{24,8},{28,12},{1,17},{... | collective-permute-start | bytes 393224 | tf_op jit(solution)/shard_map/ppermute | solution.py:521
  83.8 34.3 %collective-permute-start.14 = (bf16[2,128,256]{2,1,0:T(8,128)(2,1)S(1)}, bf16[2,128,256]{2,1,0:T(8,128)(2,1)S(1)}, u32[]{:S(2)}, u32[]{:S(2)}) collective-permute-start(bf16[2,128,256]{2,1,0:T(8,128)(2,1)S(1)} %add_convert_fusion.refs_0_), channel_id=1, source_target_pairs={{0,1},{1,0},{2,3},{3,2},{4,5},{5,4},{6,7},{7,6},{8,9},{9,8},{10,11... | collective-permute-start | bytes 393224 | tf_op jit(solution)/shard_map/ppermute | solution.py:521
  83.9 34.2 %collective-permute-start.15 = (bf16[2,128,256]{2,1,0:T(8,128)(2,1)S(1)}, bf16[2,128,256]{2,1,0:T(8,128)(2,1)S(1)}, u32[]{:S(2)}, u32[]{:S(2)}) collective-permute-start(bf16[2,128,256]{2,1,0:T(8,128)(2,1)S(1)} %add_convert_fusion.refs_0_), channel_id=1, source_target_pairs={{0,2},{1,3},{2,0},{3,1},{4,6},{5,7},{6,4},{7,5},{8,10},{9,11},{10,... | collective-permute-start | bytes 393224 | tf_op jit(solution)/shard_map/ppermute | solution.py:521
  84.5 33.6 %collective-permute-start.16 = (bf16[2,128,256]{2,1,0:T(8,128)(2,1)S(1)}, bf16[2,128,256]{2,1,0:T(8,128)(2,1)S(1)}, u32[]{:S(2)}, u32[]{:S(2)}) collective-permute-start(bf16[2,128,256]{2,1,0:T(8,128)(2,1)S(1)} %add_convert_fusion.refs_0_), channel_id=1, source_target_pairs={{0,3},{1,2},{2,1},{3,0},{4,7},{5,6},{6,5},{7,4},{8,11},{9,10},{10,... | collective-permute-start | bytes 393224 | tf_op jit(solution)/shard_map/ppermute | solution.py:521
  119.8 5.0 %collective-permute-start.22 = (bf16[128,256]{1,0:T(8,128)(2,1)S(1)}, bf16[128,256]{1,0:T(8,128)(2,1)S(1)}, u32[]{:S(2)}, u32[]{:S(2)}) collective-permute-start(bf16[128,256]{1,0:T(8,128)(2,1)S(1)} %get-tuple-element.47), channel_id=1, source_target_pairs={{0,4},{4,0},{8,12},{12,8},{16,20},{20,16},{24,28},{28,24},{1,5},{5... | collective-permute-start | bytes 196616 | tf_op jit(solution)/shard_map/ppermute | solution.py:521
  121.4 4.3 %collective-permute-start.23 = (bf16[128,256]{1,0:T(8,128)(2,1)S(1)}, bf16[128,256]{1,0:T(8,128)(2,1)S(1)}, u32[]{:S(2)}, u32[]{:S(2)}) collective-permute-start(bf16[128,256]{1,0:T(8,128)(2,1)S(1)} %get-tuple-element.48), channel_id=1, source_target_pairs={{0,8},{4,12},{8,0},{12,4},{16,24},{20,28},{24,16},{28,20},{1,9},{5... | collective-permute-start | bytes 196616 | tf_op jit(solution)/shard_map/ppermute | solution.py:521
  121.4 5.2 %collective-permute-start.24 = (bf16[128,256]{1,0:T(8,128)(2,1)S(1)}, bf16[128,256]{1,0:T(8,128)(2,1)S(1)}, u32[]{:S(2)}, u32[]{:S(2)}) collective-permute-start(bf16[128,256]{1,0:T(8,128)(2,1)S(1)} %get-tuple-element.49), channel_id=1, source_target_pairs={{0,12},{4,8},{8,4},{12,0},{16,28},{20,24},{24,20},{28,16},{1,13},{... | collective-permute-start | bytes 196616 | tf_op jit(solution)/shard_map/ppermute | solution.py:521
  126.6 6.5 %collective-permute-start.28 = (bf16[128,256]{1,0:T(8,128)(2,1)S(1)}, bf16[128,256]{1,0:T(8,128)(2,1)S(1)}, u32[]{:S(2)}, u32[]{:S(2)}) collective-permute-start(bf16[128,256]{1,0:T(8,128)(2,1)S(1)} %add_convert_fusion.1.refs_0_), channel_id=1, source_target_pairs={{0,16},{4,20},{8,24},{12,28},{16,0},{20,4},{24,8},{28,12},{1,17},{... | collective-permute-start | bytes 196616 | tf_op jit(solution)/shard_map/ppermute | solution.py:521
  128.7 5.8 %collective-permute-start.13 = (bf16[128,256]{1,0:T(8,128)(2,1)S(1)}, bf16[128,256]{1,0:T(8,128)(2,1)S(1)}, u32[]{:S(2)}, u32[]{:S(2)}) collective-permute-start(bf16[128,256]{1,0:T(8,128)(2,1)S(1)} %get-tuple-element.60), channel_id=1, source_target_pairs={{0,16},{4,20},{8,24},{12,28},{16,0},{20,4},{24,8},{28,12},{1,17},{... | collective-permute-start | bytes 196616 | tf_op jit(solution)/shard_map/ppermute | solution.py:521
  129.6 6.1 %collective-permute-start.25 = (bf16[128,256]{1,0:T(8,128)(2,1)S(1)}, bf16[128,256]{1,0:T(8,128)(2,1)S(1)}, u32[]{:S(2)}, u32[]{:S(2)}) collective-permute-start(bf16[128,256]{1,0:T(8,128)(2,1)S(1)} %add_convert_fusion.1.refs_0_), channel_id=1, source_target_pairs={{0,4},{4,0},{8,12},{12,8},{16,20},{20,16},{24,28},{28,24},{1,5},{5... | collective-permute-start | bytes 196616 | tf_op jit(solution)/shard_map/ppermute | solution.py:521
  130.9 8.4 %collective-permute-start.26 = (bf16[128,256]{1,0:T(8,128)(2,1)S(1)}, bf16[128,256]{1,0:T(8,128)(2,1)S(1)}, u32[]{:S(2)}, u32[]{:S(2)}) collective-permute-start(bf16[128,256]{1,0:T(8,128)(2,1)S(1)} %add_convert_fusion.1.refs_0_), channel_id=1, source_target_pairs={{0,8},{4,12},{8,0},{12,4},{16,24},{20,28},{24,16},{28,20},{1,9},{5... | collective-permute-start | bytes 196616 | tf_op jit(solution)/shard_map/ppermute | solution.py:521
  132.2 7.1 %collective-permute-start.27 = (bf16[128,256]{1,0:T(8,128)(2,1)S(1)}, bf16[128,256]{1,0:T(8,128)(2,1)S(1)}, u32[]{:S(2)}, u32[]{:S(2)}) collective-permute-start(bf16[128,256]{1,0:T(8,128)(2,1)S(1)} %add_convert_fusion.1.refs_0_), channel_id=1, source_target_pairs={{0,12},{4,8},{8,4},{12,0},{16,28},{20,24},{24,20},{28,16},{1,13},{... | collective-permute-start | bytes 196616 | tf_op jit(solution)/shard_map/ppermute | solution.py:521
  133.1 6.2 %collective-permute-start.29 = (bf16[128,256]{1,0:T(8,128)(2,1)S(1)}, bf16[128,256]{1,0:T(8,128)(2,1)S(1)}, u32[]{:S(2)}, u32[]{:S(2)}) collective-permute-start(bf16[128,256]{1,0:T(8,128)(2,1)S(1)} %collective-permute-done.28.refs_4_), channel_id=1, source_target_pairs={{0,4},{4,0},{8,12},{12,8},{16,20},{20,16},{24,28},{28,24},{1,5},{5... | collective-permute-start | bytes 196616 | tf_op jit(solution)/shard_map/ppermute | solution.py:521
  134.4 4.9 %collective-permute-start.30 = (bf16[128,256]{1,0:T(8,128)(2,1)S(1)}, bf16[128,256]{1,0:T(8,128)(2,1)S(1)}, u32[]{:S(2)}, u32[]{:S(2)}) collective-permute-start(bf16[128,256]{1,0:T(8,128)(2,1)S(1)} %collective-permute-done.28.refs_4_), channel_id=1, source_target_pairs={{0,8},{4,12},{8,0},{12,4},{16,24},{20,28},{24,16},{28,20},{1,9},{5... | collective-permute-start | bytes 196616 | tf_op jit(solution)/shard_map/ppermute | solution.py:521
  135.7 5.2 %collective-permute-start.31 = (bf16[128,256]{1,0:T(8,128)(2,1)S(1)}, bf16[128,256]{1,0:T(8,128)(2,1)S(1)}, u32[]{:S(2)}, u32[]{:S(2)}) collective-permute-start(bf16[128,256]{1,0:T(8,128)(2,1)S(1)} %collective-permute-done.28.refs_4_), channel_id=1, source_target_pairs={{0,12},{4,8},{8,4},{12,0},{16,28},{20,24},{24,20},{28,16},{1,13},{... | collective-permute-start | bytes 196616 | tf_op jit(solution)/shard_map/ppermute | solution.py:521
  (9 other events, 5.8 us)

commit v2 on v1

--- a/solution.py
+++ b/solution.py
@@ -16,7 +16,7 @@
 CONV_K = 5
 BLOCK = 128
 INNER = 2048
-EXTRA = 16
+EXTRA = 8
 ROWS = 8
 
 EPSILON = 1e-06
@@ -154,9 +154,10 @@
             outs[1][rows, lanes] = chunk[:, STATE:]
 
 
-def gather_kernel(at_ref, *refs):
-    for k, ref in enumerate(refs[:-1]):
-        refs[-1][k] = ref[...]
+def gather_kernel(at_ref, drop_ref, *refs):
+    for k, ref in enumerate(refs[:-2]):
+        refs[-2][k] = ref[...]
+    refs[-1][...] = drop_ref[...]
 
 
 def unpack_kernel(back_ref, dx_ref, dt_ref):
@@ -177,10 +178,10 @@
     return terms
 
 
-def per_head(ref, index):
+def per_head(ref, line, index):
     total = jnp.zeros(index.shape, f32)
-    for h in range(ref.shape[0]):
-        total = jnp.where(index == h, ref[h], total)
+    for h in range(ref.shape[1]):
+        total = jnp.where(index == h, ref[line, h], total)
     return total
 
 
@@ -213,8 +214,7 @@
 
 
 def enter_kernel(
-    offset_ref,
-    fading_ref,
+    head_ref,
     x_ref,
     drop_ref,
     xw_ref,
@@ -230,8 +230,8 @@
     heads = width // HEAD_DIM
     all_rows = blocks * ROWS
     rows_of = lax.broadcasted_iota(jnp.int32, (ROWS, BLOCK), 0)
-    offset = per_head(offset_ref, rows_of)
-    fade = jnp.exp(per_head(fading_ref, rows_of))
+    offset = per_head(head_ref, 0, rows_of)
+    fade = jnp.exp(per_head(head_ref, 1, rows_of))
     xpad[0:PAD, :] = jnp.zeros((PAD, width), f32)
     xpad[PAD + blocks * BLOCK :, :] = jnp.zeros((PAD, width), f32)
 
@@ -280,8 +280,7 @@
 def mixer_kernel(
     devices,
     at_ref,
-    fading_ref,
-    direct_ref,
+    head_ref,
     *refs,
 ):
     x_ref, u_s, us_s, rows_in, wide_s, dr_s, gg_s, xw_ref, write_ref, read_ref = refs[:10]
@@ -289,14 +288,21 @@
     refs = refs[10 + devices :]
     out_ref = refs[0]
     dbc_refs = refs[1 : 1 + devices // 2]
-    xpad, bcpad, kcs_s, kr_s, row_s, st_s, car_s, sel_s, bcw_ref = refs[1 + devices // 2 :]
+    xpad, bcpad, kcs_s, kr_s, row_s, st_s, car_s, sel_s, bcw_ref, stage, sems = refs[
+        1 + devices // 2 :
+    ]
+    copies = [
+        pltpu.make_async_copy(bc_ref, stage.at[k], sems.at[k]) for k, bc_ref in enumerate(bc_refs)
+    ]
+    for copy in copies:
+        copy.start()
     blocks, _, width = x_ref.shape
     heads = width // HEAD_DIM
     pad = PAD
     lanes = min(width, BLOCK)
     per = lanes // HEAD_DIM
     all_rows = blocks * ROWS
-    fade = jnp.exp(per_head(fading_ref, lax.broadcasted_iota(jnp.int32, (ROWS, BLOCK), 0)))
+    fade = jnp.exp(per_head(head_ref, 1, lax.broadcasted_iota(jnp.int32, (ROWS, BLOCK), 0)))
 
     mine = pl.ds(pl.multiple_of(at_ref[2] * STATE, STATE), STATE)
     bcw_ref[:CONV_K, :STATE] = write_ref[:, mine]
@@ -311,9 +317,10 @@
     xpad[pad + blocks * BLOCK :, :] = jnp.zeros((pad, width), f32)
     bcpad[0:pad, :] = jnp.zeros((pad, 2 * STATE), f32)
     bcpad[pad + blocks * BLOCK :, :] = jnp.zeros((pad, 2 * STATE), f32)
-    for k, bc_ref in enumerate(bc_refs):
+    for k, copy in enumerate(copies):
+        copy.wait()
         at = pl.multiple_of((at_ref[1] ^ k) * BLOCK, BLOCK) + pad
-        bcpad[pl.ds(at, BLOCK), :] = bc_ref[...].astype(f32)
+        bcpad[pl.ds(at, BLOCK), :] = stage[k].astype(f32)
 
     def first(b, _):
         pre = conv(bcpad, b, bcw_ref, False)
@@ -425,7 +432,7 @@
         row_s[0, b] = sums[:ROWS] + by_key[:ROWS] - by_read
         row_s[1, b] = jnp.broadcast_to(before, (ROWS, BLOCK))
         row_s[2, b] = sums[2 * ROWS : 3 * ROWS]
-        skip = per_head(direct_ref, lax.broadcasted_iota(jnp.int32, (1, width), 1) // HEAD_DIM)
+        skip = per_head(head_ref, 2, lax.broadcasted_iota(jnp.int32, (1, width), 1) // HEAD_DIM)
         d_u = d_dr * w_dt + g16.astype(f32) * skip
         at = pl.multiple_of(b * BLOCK, BLOCK) + pad
         xpad[pl.ds(at, BLOCK), :] = d_u * us_s[b]
@@ -467,7 +474,7 @@
     return pl.BlockSpec(memory_space=pltpu.SMEM)
 
 
-def run_enter(offset, fading, x, drop, xw):
+def run_enter(per_heads, x, drop, xw):
     blocks, _, width = x.shape
     shape = jax.ShapeDtypeStruct
     return pl.pallas_call(
@@ -480,15 +487,15 @@
             shape((blocks, BLOCK, 2 * width), bf16),
             shape((blocks, BLOCK, 2 * width), bf16),
         ),
-        in_specs=[smem()] * 2 + [vmem()] * 3,
+        in_specs=[smem()] + [vmem()] * 3,
         out_specs=(vmem(),) * 6,
         scratch_shapes=[pltpu.VMEM((blocks * BLOCK + 2 * PAD, width), f32)],
-        compiler_params=limit(24),
+        compiler_params=limit(min(60, 12 * max(1, blocks // 8))),
         name="enter",
-    )(offset, fading, x, drop, xw)
-
-
-def run_mixer(at, fading, direct, x, entered, filters, bc):
+    )(per_heads, x, drop, xw)
+
+
+def run_mixer(at, per_heads, x, entered, filters, bc):
     blocks, _, width = x.shape
     length = blocks * BLOCK
     scratch = [
@@ -501,18 +508,22 @@
         pltpu.VMEM((blocks, STATE, 4 * width), bf16),
         pltpu.VMEM((5 * width, BLOCK), bf16),
         pltpu.VMEM((ROWS, 2 * STATE), f32),
+        pltpu.VMEM((len(bc), BLOCK, 2 * STATE), bf16),
+        pltpu.SemaphoreType.DMA((len(bc),)),
     ]
     half = len(bc) // 2
     outs = pl.pallas_call(
         functools.partial(mixer_kernel, len(bc)),
         out_shape=(jax.ShapeDtypeStruct((blocks, BLOCK + EXTRA, width), bf16),)
         + (jax.ShapeDtypeStruct((2, BLOCK, 2 * STATE), bf16),) * half,
-        in_specs=[smem()] * 3 + [vmem()] * (10 + len(bc)),
+        in_specs=[smem()] * 2
+        + [vmem()] * 10
+        + [pl.BlockSpec(memory_space=pltpu.HBM)] * len(bc),
         out_specs=(vmem(),) * (1 + half),
         scratch_shapes=scratch,
-        compiler_params=limit(36),
+        compiler_params=limit(min(60, 20 * max(1, blocks // 8))),
         name="mixer",
-    )(at, fading, direct, x, *entered, *filters, *bc)
+    )(at, per_heads, x, *entered, *filters, *bc)
     return outs[0], outs[1:]
 
 
@@ -529,7 +540,7 @@
         in_specs=specs,
         out_specs=jax.tree.map(lambda _: vmem(), outs),
         scratch_shapes=scratch,
-        compiler_params=limit(16),
+        compiler_params=limit(8),
     )(*args)
 
 
@@ -616,7 +627,14 @@
 
     acts = [lax.dynamic_slice(rows, (0, (me_d ^ k) * share), (tokens, share)) for k in range(dp)]
     acts = [acts[0]] + [swap(acts[k], "dp", k) for k in range(1, dp)]
-    gathered = call(gather_kernel, shape((dp - 1, tokens, share), bf16), at, *acts[: dp - 1])
+    drop = extra_logdrop[0].T
+    gathered, drop = call(
+        gather_kernel,
+        (shape((dp - 1, tokens, share), bf16), shape(drop.shape, f32)),
+        at,
+        drop,
+        *acts[: dp - 1],
+    )
     acts += [swap(gathered, "sp", half), swap(acts[dp - 1], "sp", half)]
 
     bc = shape((tokens, 2 * STATE), bf16)
@@ -625,11 +643,10 @@
     all_bc = [own if k == 0 else swap(own, "sp", k) for k in range(half)]
     all_bc += [other if k == 0 else swap(other, "sp", k) for k in range(half)]
 
-    entered = run_enter(
-        delta_offset, fading_exponents, heads_x, extra_logdrop[0].T, source_filter_coefs
-    )
+    per_heads = jnp.stack([delta_offset, fading_exponents, direct_factor])
+    entered = run_enter(per_heads, heads_x, drop, source_filter_coefs)
     filters = (source_filter_coefs, writer_filter_coefs, reader_filter_coefs)
-    d_x, d_bc = run_mixer(at, fading_exponents, direct_factor, heads_x, entered, filters, all_bc)
+    d_x, d_bc = run_mixer(at, per_heads, heads_x, entered, filters, all_bc)
 
     parts = [d_bc[0]] + [swap(d_bc[k], "sp", k) for k in range(1, half)]
     grads = functools.reduce(jnp.add, [p.astype(f32) for p in parts]).astype(bf16)
@@ -658,7 +675,7 @@
         out_shape=(shape((tokens, INNER), bf16), shape((HEADS, tokens), bf16)),
         in_specs=[vmem()],
         out_specs=(vmem(), vmem()),
-        compiler_params=limit(16),
+        compiler_params=limit(8),
         name="unpack",
     )(back_x)
     matrix = shape((share, GROUPS * STATE), f32)

time: 144 us -> 131 us (0.910)
  local copies, waits for them, and re-layouts: 11.4 us -> 1.57 us
  waiting for transfers between devices: 56.9 us -> 50.1 us
  Pallas kernels: 28 us -> 29.8 us
    unnamed x46 -> x24, local copies, waits for them, and re-layouts: 10.6 us -> 0.72 us
    ppermute x32, waiting for transfers between devices: 56.9 us -> 50.1 us  [swap(): return lax.ppermute(value, axis, [(i, i ^ bits) for i in range(size)])]
  transfers between devices with their start and end apart: 34 -> 34, of which waited for: 9 -> 9; matrix products, arithmetic and copies ran while one was open for 1% -> 2% of each run, Pallas kernels for 16% -> 19%
where the time goes in v2:
time: 131 us
  waiting for transfers between devices  50.1 us (38%)
  starting transfers between devices  47.3 us (36%)
  Pallas kernels  29.8 us (23%)
  local copies, waits for them, and re-layouts  1.57 us (1%)
    ppermute x32, waiting for transfers between devices, swap(): return lax.ppermute(value, axis, [(i, i ^ bits) for i in range(size)])  50.1 us
    ppermute x32, starting transfers between devices, swap(): return lax.ppermute(value, axis, [(i, i ^ bits) for i in range(size)])  35.4 us
    pallas_call x1, Pallas kernels, run_mixer(): pl.pallas_call(functools.partial(mixer_kernel, len(bc)), out_shape=(jax.S...  12.8 us
    pallas_call x5, Pallas kernels, call(): pl.pallas_call(kernel, out_shape=outs, in_specs=specs, out_specs=jax.tree...  9.12 us
    all_to_all x1, starting transfers between devices, local(): heads_x = lax.all_to_all(packed, 'sp', 0, 0, tiled=True)  7.42 us
    all_to_all x1, starting transfers between devices, local(): back_x = lax.all_to_all(d_x, 'sp', 0, 0, tiled=True)  4.48 us
    pallas_call x1, Pallas kernels, local(): pl.pallas_call(prep_kernel, grid=(steps,), in_specs=[row_spec, row_spec,...  4.29 us
    pallas_call x1, Pallas kernels, run_enter(): pl.pallas_call(enter_kernel, out_shape=(shape((blocks, BLOCK, width), f32...  2.71 us
  transfers between devices with their start and end apart: 34, of which 9 were waited for; matrix products, arithmetic and copies ran while one was open for 2% of the time, Pallas kernels for 19%

profile of v2, /device:TPU:0, one launch (start us, length us, event | category | flops | bytes accessed | tf_op | source)
XLA Modules:
  0.0 130.8 jit_solution(1188497744850677562)
XLA Ops:
  0.6 4.3 %prep.1 = (bf16[8,264,256]{2,1,0:T(8,128)(2,1)}, bf16[128,2048]{1,0:T(8,128)(2,1)}) custom-call(bf16[128,2048]{1,0:T(8,128)(2,1)} %bitcast.39, bf16[128,2048]{1,0:T(8,128)(2,1)} %bitcast.40, bf16[128,2048]{1,0:T(8,128)(2,1)} %bitcast.41, f32[1,2048]{1,0:T(1,128)} %bitcast.44, bf16[128,2048]{1,0:T(8,128)(2,1)} %bitcast.42, bf16[32,128]{1,0:T(8,128)(2,1)} %bitcast.45), custom_call_target="tpu_custom_call" | custom-call | tf_op jit(solution)/shard_map/prep/pallas_call | solution.py:598
  4.9 7.4 %all-to-all-start = ((bf16[8,264,256]{2,1,0:T(8,128)(2,1)}), bf16[8,264,256]{2,1,0:T(8,128)(2,1)S(1)}, u32[]{:S(2)}, u32[]{:S(2)}) async-start(bf16[8,264,256]{2,1,0:T(8,128)(2,1)} %get-tuple-element.31), calls=%async_computation | async-start | bytes 2162688 | tf_op jit(solution)/shard_map/all_to_all | solution.py:626
  12.6 1.6 %collective-permute-start.3 = (bf16[512,512]{1,0:T(8,128)(2,1)S(1)}, bf16[512,512]{1,0:T(8,128)(2,1)S(1)}, u32[]{:S(2)}, u32[]{:S(2)}) collective-permute-start(bf16[512,512]{1,0:T(8,128)(2,1)S(1)} %pad_maximum_fusion.refs_0_), channel_id=1, source_target_pairs={{0,2},{1,3},{2,0},{3,1},{4,6},{5,7},{6,4},{7,5},{8,10},{9,11},{10,... | collective-permute-start | bytes 1572872 | tf_op jit(solution)/shard_map/ppermute | solution.py:532
  14.1 11.9 %collective-permute-done.3.refs_2_ = bf16[512,512]{1,0:T(8,128)(2,1)S(1)} collective-permute-done((bf16[512,512]{1,0:T(8,128)(2,1)S(1)}, bf16[512,512]{1,0:T(8,128)(2,1)S(1)}, u32[]{:S(2)}, u32[]{:S(2)}) %collective-permute-start.3) | collective-permute-done | bytes 524320 | tf_op jit(solution)/shard_map/ppermute | solution.py:532
  26.0 0.8 dynamic-slice_bitcast_fusion
  26.8 0.5 collective-permute-start
  27.3 1.5 %collective-permute-start.1 = (bf16[128,512]{1,0:T(8,128)(2,1)}, bf16[128,512]{1,0:T(8,128)(2,1)}, u32[]{:S(2)}, u32[]{:S(2)}) collective-permute-start(bf16[128,512]{1,0:T(8,128)(2,1)} %get-tuple-element.57), channel_id=1, source_target_pairs={{0,2},{1,3},{2,0},{3,1},{4,6},{5,7},{6,4},{7,5},{8,10},{9,11},{10,... | collective-permute-start | bytes 393224 | tf_op jit(solution)/shard_map/ppermute | solution.py:532
  28.9 1.5 %shard_map.200 = (bf16[128,256]{1,0:T(8,128)(2,1)S(1)}, bf16[128,256]{1,0:T(8,128)(2,1)S(1)}) custom-call(s32[4]{0:T(128)S(1)} %pad_add_fusion.at_ref, bf16[128,2048]{1,0:T(8,128)(2,1)S(1)} %bitcast.37, bf16[512,512]{1,0:T(8,128)(2,1)S(1)} %pad_maximum_fusion.refs_0_, bf16[512,512]{1,0:T(8,128)(2,1)S(1)} %collective-permute-done.2.refs_1_, ...), custom_call_target="tpu_custom_call" | custom-call | tf_op jit(solution)/shard_map/pallas_call | solution.py:537
  30.5 2.7 %collective-permute-start.8 = (bf16[128,256]{1,0:T(8,128)(2,1)S(1)}, bf16[128,256]{1,0:T(8,128)(2,1)S(1)}, u32[]{:S(2)}, u32[]{:S(2)}) collective-permute-start(bf16[128,256]{1,0:T(8,128)(2,1)S(1)} %get-tuple-element.40), channel_id=1, source_target_pairs={{0,16},{4,20},{8,24},{12,28},{16,0},{20,4},{24,8},{28,12},{1,17},{... | collective-permute-start | bytes 196616 | tf_op jit(solution)/shard_map/ppermute | solution.py:532
  33.2 1.5 %collective-permute-start.5 = (bf16[128,256]{1,0:T(8,128)(2,1)S(1)}, bf16[128,256]{1,0:T(8,128)(2,1)S(1)}, u32[]{:S(2)}, u32[]{:S(2)}) collective-permute-start(bf16[128,256]{1,0:T(8,128)(2,1)S(1)} %get-tuple-element.39.refs_10_), channel_id=1, source_target_pairs={{0,4},{4,0},{8,12},{12,8},{16,20},{20,16},{24,28},{28,24},{1,5},{5... | collective-permute-start | bytes 196616 | tf_op jit(solution)/shard_map/ppermute | solution.py:532
  34.6 1.5 %collective-permute-start.6 = (bf16[128,256]{1,0:T(8,128)(2,1)S(1)}, bf16[128,256]{1,0:T(8,128)(2,1)S(1)}, u32[]{:S(2)}, u32[]{:S(2)}) collective-permute-start(bf16[128,256]{1,0:T(8,128)(2,1)S(1)} %get-tuple-element.39.refs_10_), channel_id=1, source_target_pairs={{0,8},{4,12},{8,0},{12,4},{16,24},{20,28},{24,16},{28,20},{1,9},{5... | collective-permute-start | bytes 196616 | tf_op jit(solution)/shard_map/ppermute | solution.py:532
  36.1 0.6 collective-permute-start.7
  36.7 5.1 %collective-permute-done.8.refs_14_ = bf16[128,256]{1,0:T(8,128)(2,1)S(1)} collective-permute-done((bf16[128,256]{1,0:T(8,128)(2,1)S(1)}, bf16[128,256]{1,0:T(8,128)(2,1)S(1)}, u32[]{:S(2)}, u32[]{:S(2)}) %collective-permute-start.8) | collective-permute-done | bytes 65568 | tf_op jit(solution)/shard_map/ppermute | solution.py:532
  41.7 2.9 %collective-permute-start.11 = (bf16[128,256]{1,0:T(8,128)(2,1)S(1)}, bf16[128,256]{1,0:T(8,128)(2,1)S(1)}, u32[]{:S(2)}, u32[]{:S(2)}) collective-permute-start(bf16[128,256]{1,0:T(8,128)(2,1)S(1)} %collective-permute-done.8.refs_14_), channel_id=1, source_target_pairs={{0,12},{4,8},{8,4},{12,0},{16,28},{20,24},{24,20},{28,16},{1,13},{... | collective-permute-start | bytes 196616 | tf_op jit(solution)/shard_map/ppermute | solution.py:532
  44.6 0.6 collective-permute-start.9
  45.3 1.7 %shard_map.199 = (bf16[3,128,512]{2,1,0:T(8,128)(2,1)}, f32[4,1024]{1,0:T(4,128)S(1)}) custom-call(s32[4]{0:T(128)S(1)} %pad_add_fusion.at_ref, f32[4,1024]{1,0:T(4,128)S(1)} %bitcast.38, bf16[128,512]{1,0:T(8,128)(2,1)S(1)} %get-tuple-element.59.refs_0_.refs_4_, bf16[128,512]{1,0:T(8,128)(2,1)S(1)} %collective-permute-done.refs_1_.refs_5_, ...), custom_call_target="tpu_custom_call" | custom-call | tf_op jit(solution)/shard_map/pallas_call | solution.py:537
  47.0 2.7 %enter.1 = (f32[8,128,256]{2,1,0:T(8,128)S(1)}, f32[8,128,256]{2,1,0:T(8,128)S(1)}, f32[5,8,8,128]{3,2,1,0:T(8,128)S(1)}, f32[8,384,256]{2,1,0:T(8,128)S(1)}, bf...) custom-call(f32[3,4]{1,0:T(4,128)S(1)} %pad_maximum_fusion.1.head_ref, ...), custom_call_target="tpu_custom_call" | custom-call | tf_op jit(solution)/shard_map/enter/pallas_call | solution.py:480
  49.8 12.8 %mixer.1 = (bf16[8,136,256]{2,1,0:T(8,128)(2,1)}, bf16[2,128,256]{2,1,0:T(8,128)(2,1)S(1)}, bf16[2,128,256]{2,1,0:T(8,128)(2,1)}, bf16[2,128,256]{2,1,0:T(8,128)(2,1)}, bf16[2,128,256]{2,1,0:T(8,128)(2,1)}) custom-call(s32[4]{0:T(128)S(1)} %pad_add_fusion.at_ref, f32[3,4]{1,0:T(4,128)S(1)} %pad_maximum_fusion.1.head_ref, ...), custom_call_target="tpu_custom_call" | custom-call | tf_op jit(solution)/shard_map/mixer/pallas_call | solution.py:515
  62.6 0.7 copy-done.1
  63.3 1.4 %collective-permute-start.12 = (bf16[2,128,256]{2,1,0:T(8,128)(2,1)}, bf16[2,128,256]{2,1,0:T(8,128)(2,1)S(1)}, u32[]{:S(2)}, u32[]{:S(2)}) collective-permute-start(bf16[2,128,256]{2,1,0:T(8,128)(2,1)} %get-tuple-element.42), channel_id=1, source_target_pairs={{0,4},{4,0},{8,12},{12,8},{16,20},{20,16},{24,28},{28,24},{1,5},{5... | collective-permute-start | bytes 393224 | tf_op jit(solution)/shard_map/ppermute | solution.py:532
  64.7 2.0 %collective-permute-start.14 = (bf16[2,128,256]{2,1,0:T(8,128)(2,1)}, bf16[2,128,256]{2,1,0:T(8,128)(2,1)}, u32[]{:S(2)}, u32[]{:S(2)}) collective-permute-start(bf16[2,128,256]{2,1,0:T(8,128)(2,1)} %get-tuple-element.44), channel_id=1, source_target_pairs={{0,12},{4,8},{8,4},{12,0},{16,28},{20,24},{24,20},{28,16},{1,13},{... | collective-permute-start | bytes 393224 | tf_op jit(solution)/shard_map/ppermute | solution.py:532
  66.8 0.6 collective-permute-start.20
  67.4 4.5 %all-to-all-start.1 = ((bf16[8,136,256]{2,1,0:T(8,128)(2,1)}), bf16[8,136,256]{2,1,0:T(8,128)(2,1)S(1)}, u32[]{:S(2)}, u32[]{:S(2)}) async-start(bf16[8,136,256]{2,1,0:T(8,128)(2,1)} %get-tuple-element.45), calls=%async_computation.1 | async-start | bytes 1114112 | tf_op jit(solution)/shard_map/all_to_all | solution.py:653
  71.9 2.9 %collective-permute-start.21 = (bf16[128,512]{1,0:T(8,128)(2,1)S(1)}, bf16[128,512]{1,0:T(8,128)(2,1)S(1)}, u32[]{:S(2)}, u32[]{:S(2)}) collective-permute-start(bf16[128,512]{1,0:T(8,128)(2,1)S(1)} %collective-permute-done.19.refs_7_), channel_id=1, source_target_pairs={{0,16},{4,20},{8,24},{12,28},{16,0},{20,4},{24,8},{28,12},{1,17},{... | collective-permute-start | bytes 393224 | tf_op jit(solution)/shard_map/ppermute | solution.py:532
  74.8 1.2 collective-permute-done.14
  76.0 1.0 add_convert_fusion.refs_0_
  77.0 0.3 collective-permute-start.16
  77.4 1.6 %collective-permute-start.17 = (bf16[2,128,256]{2,1,0:T(8,128)(2,1)S(1)}, bf16[2,128,256]{2,1,0:T(8,128)(2,1)S(1)}, u32[]{:S(2)}, u32[]{:S(2)}) collective-permute-start(bf16[2,128,256]{2,1,0:T(8,128)(2,1)S(1)} %add_convert_fusion.refs_0_), channel_id=1, source_target_pairs={{0,2},{1,3},{2,0},{3,1},{4,6},{5,7},{6,4},{7,5},{8,10},{9,11},{10,... | collective-permute-start | bytes 393224 | tf_op jit(solution)/shard_map/ppermute | solution.py:532
  79.0 26.7 %collective-permute-done.21.refs_9_ = bf16[128,512]{1,0:T(8,128)(2,1)S(1)} collective-permute-done((bf16[128,512]{1,0:T(8,128)(2,1)S(1)}, bf16[128,512]{1,0:T(8,128)(2,1)S(1)}, u32[]{:S(2)}, u32[]{:S(2)}) %collective-permute-start.21) | collective-permute-done | bytes 131104 | tf_op jit(solution)/shard_map/ppermute | solution.py:532
  105.7 1.7 %shard_map.202 = (bf16[128,256]{1,0:T(8,128)(2,1)S(1)}, bf16[128,256]{1,0:T(8,128)(2,1)S(1)}, bf16[128,256]{1,0:T(8,128)(2,1)S(1)}, bf16[128,256]{1,0:T(8,128)(2,1)S(1)}) custom-call(s32[4]{0:T(128)S(1)} %pad_add_fusion.at_ref, bf16[2,128,256]{2,1,0:T(8,128)(2,1)S(1)} %add_convert_fusion.refs_0_, bf16[2,128,256]{2,1,0:T(8,128)(2,1)S(1)} %collective-permute-done.16.refs_1_, ...), custom_call_target="tpu_custom_call" | custom-call | tf_op jit(solution)/shard_map/pallas_call | solution.py:537
  107.4 1.5 %collective-permute-start.22 = (bf16[128,256]{1,0:T(8,128)(2,1)S(1)}, bf16[128,256]{1,0:T(8,128)(2,1)S(1)}, u32[]{:S(2)}, u32[]{:S(2)}) collective-permute-start(bf16[128,256]{1,0:T(8,128)(2,1)S(1)} %get-tuple-element.51), channel_id=1, source_target_pairs={{0,4},{4,0},{8,12},{12,8},{16,20},{20,16},{24,28},{28,24},{1,5},{5... | collective-permute-start | bytes 196616 | tf_op jit(solution)/shard_map/ppermute | solution.py:532
  108.9 2.1 %collective-permute-start.24 = (bf16[128,256]{1,0:T(8,128)(2,1)S(1)}, bf16[128,256]{1,0:T(8,128)(2,1)S(1)}, u32[]{:S(2)}, u32[]{:S(2)}) collective-permute-start(bf16[128,256]{1,0:T(8,128)(2,1)S(1)} %get-tuple-element.53), channel_id=1, source_target_pairs={{0,12},{4,8},{8,4},{12,0},{16,28},{20,24},{24,20},{28,16},{1,13},{... | collective-permute-start | bytes 196616 | tf_op jit(solution)/shard_map/ppermute | solution.py:532
  111.0 0.8 collective-permute-done.22
  111.7 1.5 %collective-permute-done.23 = bf16[128,256]{1,0:T(8,128)(2,1)S(1)} collective-permute-done((bf16[128,256]{1,0:T(8,128)(2,1)S(1)}, bf16[128,256]{1,0:T(8,128)(2,1)S(1)}, u32[]{:S(2)}, u32[]{:S(2)}) %collective-permute-start.23) | collective-permute-done | bytes 65568 | tf_op jit(solution)/shard_map/ppermute | solution.py:532
  113.2 0.9 collective-permute-done.24
  114.2 2.1 %collective-permute-start.28 = (bf16[128,256]{1,0:T(8,128)(2,1)S(1)}, bf16[128,256]{1,0:T(8,128)(2,1)S(1)}, u32[]{:S(2)}, u32[]{:S(2)}) collective-permute-start(bf16[128,256]{1,0:T(8,128)(2,1)S(1)} %add_convert_fusion.1.refs_0_), channel_id=1, source_target_pairs={{0,16},{4,20},{8,24},{12,28},{16,0},{20,4},{24,8},{28,12},{1,17},{... | collective-permute-start | bytes 196616 | tf_op jit(solution)/shard_map/ppermute | solution.py:532
  116.3 0.9 collective-permute-start.15
  117.2 1.3 collective-permute-start.25
  118.4 1.3 collective-permute-start.26
  119.7 0.9 collective-permute-start.27
  120.7 1.3 collective-permute-start.29
  121.9 0.7 collective-permute-done.15.other_ref
  122.6 0.6 collective-permute-start.30
  123.2 1.2 collective-permute-start.31
  124.4 2.7 %shard_map.201 = bf16[128,2048]{1,0:T(8,128)(2,1)} custom-call(s32[4]{0:T(128)S(1)} %pad_add_fusion.at_ref, bf16[128,256]{1,0:T(8,128)(2,1)S(1)} %get-tuple-element.65.own_ref, bf16[128,256]{1,0:T(8,128)(2,1)S(1)} %collective-permute-done.15.other_ref, bf16[512,512]{1,0:T(8,128)(2,1)S(1)} %pad_maximum_fusion.refs_0_, ...), custom_call_target="tpu_custom_call" | custom-call | tf_op jit(solution)/shard_map/pallas_call | solution.py:537
  127.1 1.3 %collective-permute-done.31.refs_7_ = bf16[128,256]{1,0:T(8,128)(2,1)S(1)} collective-permute-done((bf16[128,256]{1,0:T(8,128)(2,1)S(1)}, bf16[128,256]{1,0:T(8,128)(2,1)S(1)}, u32[]{:S(2)}, u32[]{:S(2)}) %collective-permute-start.31) | collective-permute-done | bytes 65568 | tf_op jit(solution)/shard_map/ppermute | solution.py:532
  128.4 1.6 %shard_map.203 = (f32[512,256]{1,0:T(8,128)}, f32[512,256]{1,0:T(8,128)}) custom-call(s32[4]{0:T(128)S(1)} %pad_add_fusion.at_ref, bf16[128,256]{1,0:T(8,128)(2,1)S(1)} %add_convert_fusion.1.refs_0_, bf16[128,256]{1,0:T(8,128)(2,1)S(1)} %collective-permute-done.25.refs_1_, bf16[128,256]{1,0:T(8,128)(2,1)S(1)} %collective-permute-done.26.refs_2_, ...), custom_call_target="tpu_custom_call" | custom-call | tf_op jit(solution)/shard_map/pallas_call | solution.py:537
  130.0 0.8 unpack.1
  (61 shorter events, 0.5 us)
Async XLA Ops:
  4.9 7.4 %copy-start.7 = (bf16[512,256]{1,0:T(8,128)(2,1)S(1)}, bf16[512,256]{1,0:T(8,128)(2,1)}, u32[]{:S(2)}) copy-start(bf16[512,256]{1,0:T(8,128)(2,1)} %param.17) | copy-start | bytes 786436
  4.9 7.4 %copy-start.8 = (bf16[512,256]{1,0:T(8,128)(2,1)S(1)}, bf16[512,256]{1,0:T(8,128)(2,1)}, u32[]{:S(2)}) copy-start(bf16[512,256]{1,0:T(8,128)(2,1)} %param.18) | copy-start | bytes 786436
  4.9 42.0 %all-to-all-start = ((bf16[8,264,256]{2,1,0:T(8,128)(2,1)}), bf16[8,264,256]{2,1,0:T(8,128)(2,1)S(1)}, u32[]{:S(2)}, u32[]{:S(2)}) async-start(bf16[8,264,256]{2,1,0:T(8,128)(2,1)} %get-tuple-element.31), calls=%async_computation | async-start | bytes 2162688 | tf_op jit(solution)/shard_map/all_to_all | solution.py:626
  12.4 13.6 %copy-start = (bf16[1,128,2048]{2,1,0:T(8,128)(2,1)S(1)}, bf16[1,128,2048]{2,1,0:T(8,128)(2,1)}, u32[]{:S(2)}) copy-start(bf16[1,128,2048]{2,1,0:T(8,128)(2,1)} %param.16) | copy-start | bytes 1572868
  12.6 13.4 %collective-permute-start.3 = (bf16[512,512]{1,0:T(8,128)(2,1)S(1)}, bf16[512,512]{1,0:T(8,128)(2,1)S(1)}, u32[]{:S(2)}, u32[]{:S(2)}) collective-permute-start(bf16[512,512]{1,0:T(8,128)(2,1)S(1)} %pad_maximum_fusion.refs_0_), channel_id=1, source_target_pairs={{0,2},{1,3},{2,0},{3,1},{4,6},{5,7},{6,4},{7,5},{8,10},{9,11},{10,... | collective-permute-start | bytes 1572872 | tf_op jit(solution)/shard_map/ppermute | solution.py:532
  14.1 14.7 %collective-permute-start.2 = (bf16[512,512]{1,0:T(8,128)(2,1)S(1)}, bf16[512,512]{1,0:T(8,128)(2,1)S(1)}, u32[]{:S(2)}, u32[]{:S(2)}) collective-permute-start(bf16[512,512]{1,0:T(8,128)(2,1)S(1)} %pad_maximum_fusion.refs_0_), channel_id=1, source_target_pairs={{0,1},{1,0},{2,3},{3,2},{4,5},{5,4},{6,7},{7,6},{8,9},{9,8},{10,11... | collective-permute-start | bytes 1572872 | tf_op jit(solution)/shard_map/ppermute | solution.py:532
  26.0 2.9 %collective-permute-start.4 = (bf16[512,512]{1,0:T(8,128)(2,1)S(1)}, bf16[512,512]{1,0:T(8,128)(2,1)}, u32[]{:S(2)}, u32[]{:S(2)}) collective-permute-start(bf16[512,512]{1,0:T(8,128)(2,1)S(1)} %collective-permute-done.3.refs_2_), channel_id=1, source_target_pairs={{0,1},{1,0},{2,3},{3,2},{4,5},{5,4},{6,7},{7,6},{8,9},{9,8},{10,11... | collective-permute-start | bytes 1572872 | tf_op jit(solution)/shard_map/ppermute | solution.py:532
  26.8 9.3 %collective-permute-start = (bf16[128,512]{1,0:T(8,128)(2,1)}, bf16[128,512]{1,0:T(8,128)(2,1)S(1)}, u32[]{:S(2)}, u32[]{:S(2)}) collective-permute-start(bf16[128,512]{1,0:T(8,128)(2,1)} %get-tuple-element.58), channel_id=1, source_target_pairs={{0,1},{1,0},{2,3},{3,2},{4,5},{5,4},{6,7},{7,6},{8,9},{9,8},{10,11... | collective-permute-start | bytes 393224 | tf_op jit(solution)/shard_map/ppermute | solution.py:532
  27.3 14.5 %collective-permute-start.1 = (bf16[128,512]{1,0:T(8,128)(2,1)}, bf16[128,512]{1,0:T(8,128)(2,1)}, u32[]{:S(2)}, u32[]{:S(2)}) collective-permute-start(bf16[128,512]{1,0:T(8,128)(2,1)} %get-tuple-element.57), channel_id=1, source_target_pairs={{0,2},{1,3},{2,0},{3,1},{4,6},{5,7},{6,4},{7,5},{8,10},{9,11},{10,... | collective-permute-start | bytes 393224 | tf_op jit(solution)/shard_map/ppermute | solution.py:532
  28.9 16.4 %copy-start.9 = (f32[4]{0:T(128)S(1)}, f32[4]{0:T(128)}, u32[]{:S(2)}) copy-start(f32[4]{0:T(128)} %param.30) | copy-start | bytes 52
  28.9 16.4 %copy-start.10 = (f32[4]{0:T(128)S(1)}, f32[4]{0:T(128)}, u32[]{:S(2)}) copy-start(f32[4]{0:T(128)} %param.29) | copy-start | bytes 52
  28.9 16.4 %copy-start.11 = (f32[4]{0:T(128)S(1)}, f32[4]{0:T(128)}, u32[]{:S(2)}) copy-start(f32[4]{0:T(128)} %param.28) | copy-start | bytes 52
  28.9 16.4 %copy-start.4 = (f32[1,1024,4]{1,2,0:T(4,128)S(1)}, f32[1,1024,4]{1,2,0:T(4,128)}, u32[]{:S(2)}) copy-start(f32[1,1024,4]{1,2,0:T(4,128)} %param.24) | copy-start | bytes 49156
  28.9 18.0 %copy-start.3 = (f32[5,256]{1,0:T(8,128)S(1)}, f32[5,256]{1,0:T(8,128)}, u32[]{:S(2)}) copy-start(f32[5,256]{1,0:T(8,128)} %refs_7_.1) | copy-start | bytes 15364
  30.5 19.4 %copy-start.5 = (f32[5,256]{1,0:T(8,128)S(1)}, f32[5,256]{1,0:T(8,128)}, u32[]{:S(2)}) copy-start(f32[5,256]{1,0:T(8,128)} %refs_8_.1) | copy-start | bytes 15364
  30.5 19.4 %copy-start.6 = (f32[5,256]{1,0:T(8,128)S(1)}, f32[5,256]{1,0:T(8,128)}, u32[]{:S(2)}) copy-start(f32[5,256]{1,0:T(8,128)} %refs_9_.1) | copy-start | bytes 15364
  30.5 11.3 %collective-permute-start.8 = (bf16[128,256]{1,0:T(8,128)(2,1)S(1)}, bf16[128,256]{1,0:T(8,128)(2,1)S(1)}, u32[]{:S(2)}, u32[]{:S(2)}) collective-permute-start(bf16[128,256]{1,0:T(8,128)(2,1)S(1)} %get-tuple-element.40), channel_id=1, source_target_pairs={{0,16},{4,20},{8,24},{12,28},{16,0},{20,4},{24,8},{28,12},{1,17},{... | collective-permute-start | bytes 196616 | tf_op jit(solution)/shard_map/ppermute | solution.py:532
  33.2 11.4 %collective-permute-start.5 = (bf16[128,256]{1,0:T(8,128)(2,1)S(1)}, bf16[128,256]{1,0:T(8,128)(2,1)S(1)}, u32[]{:S(2)}, u32[]{:S(2)}) collective-permute-start(bf16[128,256]{1,0:T(8,128)(2,1)S(1)} %get-tuple-element.39.refs_10_), channel_id=1, source_target_pairs={{0,4},{4,0},{8,12},{12,8},{16,20},{20,16},{24,28},{28,24},{1,5},{5... | collective-permute-start | bytes 196616 | tf_op jit(solution)/shard_map/ppermute | solution.py:532
  34.6 15.0 %collective-permute-start.6 = (bf16[128,256]{1,0:T(8,128)(2,1)S(1)}, bf16[128,256]{1,0:T(8,128)(2,1)S(1)}, u32[]{:S(2)}, u32[]{:S(2)}) collective-permute-start(bf16[128,256]{1,0:T(8,128)(2,1)S(1)} %get-tuple-element.39.refs_10_), channel_id=1, source_target_pairs={{0,8},{4,12},{8,0},{12,4},{16,24},{20,28},{24,16},{28,20},{1,9},{5... | collective-permute-start | bytes 196616 | tf_op jit(solution)/shard_map/ppermute | solution.py:532
  36.1 13.7 %collective-permute-start.7 = (bf16[128,256]{1,0:T(8,128)(2,1)S(1)}, bf16[128,256]{1,0:T(8,128)(2,1)S(1)}, u32[]{:S(2)}, u32[]{:S(2)}) collective-permute-start(bf16[128,256]{1,0:T(8,128)(2,1)S(1)} %get-tuple-element.39.refs_10_), channel_id=1, source_target_pairs={{0,12},{4,8},{8,4},{12,0},{16,28},{20,24},{24,20},{28,16},{1,13},{... | collective-permute-start | bytes 196616 | tf_op jit(solution)/shard_map/ppermute | solution.py:532
  41.7 8.0 %collective-permute-start.10 = (bf16[128,256]{1,0:T(8,128)(2,1)S(1)}, bf16[128,256]{1,0:T(8,128)(2,1)S(1)}, u32[]{:S(2)}, u32[]{:S(2)}) collective-permute-start(bf16[128,256]{1,0:T(8,128)(2,1)S(1)} %collective-permute-done.8.refs_14_), channel_id=1, source_target_pairs={{0,8},{4,12},{8,0},{12,4},{16,24},{20,28},{24,16},{28,20},{1,9},{5... | collective-permute-start | bytes 196616 | tf_op jit(solution)/shard_map/ppermute | solution.py:532
  41.7 8.1 %collective-permute-start.11 = (bf16[128,256]{1,0:T(8,128)(2,1)S(1)}, bf16[128,256]{1,0:T(8,128)(2,1)S(1)}, u32[]{:S(2)}, u32[]{:S(2)}) collective-permute-start(bf16[128,256]{1,0:T(8,128)(2,1)S(1)} %collective-permute-done.8.refs_14_), channel_id=1, source_target_pairs={{0,12},{4,8},{8,4},{12,0},{16,28},{20,24},{24,20},{28,16},{1,13},{... | collective-permute-start | bytes 196616 | tf_op jit(solution)/shard_map/ppermute | solution.py:532
  44.6 5.2 %collective-permute-start.9 = (bf16[128,256]{1,0:T(8,128)(2,1)S(1)}, bf16[128,256]{1,0:T(8,128)(2,1)}, u32[]{:S(2)}, u32[]{:S(2)}) collective-permute-start(bf16[128,256]{1,0:T(8,128)(2,1)S(1)} %collective-permute-done.8.refs_14_), channel_id=1, source_target_pairs={{0,4},{4,0},{8,12},{12,8},{16,20},{20,16},{24,28},{28,24},{1,5},{5... | collective-permute-start | bytes 196616 | tf_op jit(solution)/shard_map/ppermute | solution.py:532
  49.7 22.2 %collective-permute-start.19 = (bf16[128,512]{1,0:T(8,128)(2,1)}, bf16[128,512]{1,0:T(8,128)(2,1)S(1)}, u32[]{:S(2)}, u32[]{:S(2)}) collective-permute-start(bf16[128,512]{1,0:T(8,128)(2,1)} %get-tuple-element.56), channel_id=1, source_target_pairs={{0,3},{1,2},{2,1},{3,0},{4,7},{5,6},{6,5},{7,4},{8,11},{9,10},{10,... | collective-permute-start | bytes 393224 | tf_op jit(solution)/shard_map/ppermute | solution.py:532
  62.6 0.7 copy-start.1
  63.3 12.7 %copy-start.2 = (bf16[2,128,256]{2,1,0:T(8,128)(2,1)S(1)}, bf16[2,128,256]{2,1,0:T(8,128)(2,1)}, u32[]{:S(2)}) copy-start(bf16[2,128,256]{2,1,0:T(8,128)(2,1)} %copy-done.1) | copy-start | bytes 393220
  63.3 11.5 %collective-permute-start.12 = (bf16[2,128,256]{2,1,0:T(8,128)(2,1)}, bf16[2,128,256]{2,1,0:T(8,128)(2,1)S(1)}, u32[]{:S(2)}, u32[]{:S(2)}) collective-permute-start(bf16[2,128,256]{2,1,0:T(8,128)(2,1)} %get-tuple-element.42), channel_id=1, source_target_pairs={{0,4},{4,0},{8,12},{12,8},{16,20},{20,16},{24,28},{28,24},{1,5},{5... | collective-permute-start | bytes 393224 | tf_op jit(solution)/shard_map/ppermute | solution.py:532
  64.7 10.1 %collective-permute-start.13 = (bf16[2,128,256]{2,1,0:T(8,128)(2,1)}, bf16[2,128,256]{2,1,0:T(8,128)(2,1)}, u32[]{:S(2)}, u32[]{:S(2)}) collective-permute-start(bf16[2,128,256]{2,1,0:T(8,128)(2,1)} %get-tuple-element.43), channel_id=1, source_target_pairs={{0,8},{4,12},{8,0},{12,4},{16,24},{20,28},{24,16},{28,20},{1,9},{5... | collective-permute-start | bytes 393224 | tf_op jit(solution)/shard_map/ppermute | solution.py:532
  64.7 11.2 %collective-permute-start.14 = (bf16[2,128,256]{2,1,0:T(8,128)(2,1)}, bf16[2,128,256]{2,1,0:T(8,128)(2,1)}, u32[]{:S(2)}, u32[]{:S(2)}) collective-permute-start(bf16[2,128,256]{2,1,0:T(8,128)(2,1)} %get-tuple-element.44), channel_id=1, source_target_pairs={{0,12},{4,8},{8,4},{12,0},{16,28},{20,24},{24,20},{28,16},{1,13},{... | collective-permute-start | bytes 393224 | tf_op jit(solution)/shard_map/ppermute | solution.py:532
  66.8 38.9 %collective-permute-start.20 = (bf16[3,128,512]{2,1,0:T(8,128)(2,1)}, bf16[3,128,512]{2,1,0:T(8,128)(2,1)S(1)}, u32[]{:S(2)}, u32[]{:S(2)}) collective-permute-start(bf16[3,128,512]{2,1,0:T(8,128)(2,1)} %get-tuple-element.49), channel_id=1, source_target_pairs={{0,16},{4,20},{8,24},{12,28},{16,0},{20,4},{24,8},{28,12},{1,17},{... | collective-permute-start | bytes 1179656 | tf_op jit(solution)/shard_map/ppermute | solution.py:532
  67.4 62.6 %all-to-all-start.1 = ((bf16[8,136,256]{2,1,0:T(8,128)(2,1)}), bf16[8,136,256]{2,1,0:T(8,128)(2,1)S(1)}, u32[]{:S(2)}, u32[]{:S(2)}) async-start(bf16[8,136,256]{2,1,0:T(8,128)(2,1)} %get-tuple-element.45), calls=%async_computation.1 | async-start | bytes 1114112 | tf_op jit(solution)/shard_map/all_to_all | solution.py:653
  71.9 33.8 %collective-permute-start.21 = (bf16[128,512]{1,0:T(8,128)(2,1)S(1)}, bf16[128,512]{1,0:T(8,128)(2,1)S(1)}, u32[]{:S(2)}, u32[]{:S(2)}) collective-permute-start(bf16[128,512]{1,0:T(8,128)(2,1)S(1)} %collective-permute-done.19.refs_7_), channel_id=1, source_target_pairs={{0,16},{4,20},{8,24},{12,28},{16,0},{20,4},{24,8},{28,12},{1,17},{... | collective-permute-start | bytes 393224 | tf_op jit(solution)/shard_map/ppermute | solution.py:532
  77.0 28.7 %collective-permute-start.16 = (bf16[2,128,256]{2,1,0:T(8,128)(2,1)S(1)}, bf16[2,128,256]{2,1,0:T(8,128)(2,1)S(1)}, u32[]{:S(2)}, u32[]{:S(2)}) collective-permute-start(bf16[2,128,256]{2,1,0:T(8,128)(2,1)S(1)} %add_convert_fusion.refs_0_), channel_id=1, source_target_pairs={{0,1},{1,0},{2,3},{3,2},{4,5},{5,4},{6,7},{7,6},{8,9},{9,8},{10,11... | collective-permute-start | bytes 393224 | tf_op jit(solution)/shard_map/ppermute | solution.py:532
  77.4 28.4 %collective-permute-start.17 = (bf16[2,128,256]{2,1,0:T(8,128)(2,1)S(1)}, bf16[2,128,256]{2,1,0:T(8,128)(2,1)S(1)}, u32[]{:S(2)}, u32[]{:S(2)}) collective-permute-start(bf16[2,128,256]{2,1,0:T(8,128)(2,1)S(1)} %add_convert_fusion.refs_0_), channel_id=1, source_target_pairs={{0,2},{1,3},{2,0},{3,1},{4,6},{5,7},{6,4},{7,5},{8,10},{9,11},{10,... | collective-permute-start | bytes 393224 | tf_op jit(solution)/shard_map/ppermute | solution.py:532
  78.9 26.8 %collective-permute-start.18 = (bf16[2,128,256]{2,1,0:T(8,128)(2,1)S(1)}, bf16[2,128,256]{2,1,0:T(8,128)(2,1)S(1)}, u32[]{:S(2)}, u32[]{:S(2)}) collective-permute-start(bf16[2,128,256]{2,1,0:T(8,128)(2,1)S(1)} %add_convert_fusion.refs_0_), channel_id=1, source_target_pairs={{0,3},{1,2},{2,1},{3,0},{4,7},{5,6},{6,5},{7,4},{8,11},{9,10},{10,... | collective-permute-start | bytes 393224 | tf_op jit(solution)/shard_map/ppermute | solution.py:532
  107.4 4.3 %collective-permute-start.22 = (bf16[128,256]{1,0:T(8,128)(2,1)S(1)}, bf16[128,256]{1,0:T(8,128)(2,1)S(1)}, u32[]{:S(2)}, u32[]{:S(2)}) collective-permute-start(bf16[128,256]{1,0:T(8,128)(2,1)S(1)} %get-tuple-element.51), channel_id=1, source_target_pairs={{0,4},{4,0},{8,12},{12,8},{16,20},{20,16},{24,28},{28,24},{1,5},{5... | collective-permute-start | bytes 196616 | tf_op jit(solution)/shard_map/ppermute | solution.py:532
  108.9 4.3 %collective-permute-start.23 = (bf16[128,256]{1,0:T(8,128)(2,1)S(1)}, bf16[128,256]{1,0:T(8,128)(2,1)S(1)}, u32[]{:S(2)}, u32[]{:S(2)}) collective-permute-start(bf16[128,256]{1,0:T(8,128)(2,1)S(1)} %get-tuple-element.52), channel_id=1, source_target_pairs={{0,8},{4,12},{8,0},{12,4},{16,24},{20,28},{24,16},{28,20},{1,9},{5... | collective-permute-start | bytes 196616 | tf_op jit(solution)/shard_map/ppermute | solution.py:532
  108.9 5.2 %collective-permute-start.24 = (bf16[128,256]{1,0:T(8,128)(2,1)S(1)}, bf16[128,256]{1,0:T(8,128)(2,1)S(1)}, u32[]{:S(2)}, u32[]{:S(2)}) collective-permute-start(bf16[128,256]{1,0:T(8,128)(2,1)S(1)} %get-tuple-element.53), channel_id=1, source_target_pairs={{0,12},{4,8},{8,4},{12,0},{16,28},{20,24},{24,20},{28,16},{1,13},{... | collective-permute-start | bytes 196616 | tf_op jit(solution)/shard_map/ppermute | solution.py:532
  114.2 6.5 %collective-permute-start.28 = (bf16[128,256]{1,0:T(8,128)(2,1)S(1)}, bf16[128,256]{1,0:T(8,128)(2,1)S(1)}, u32[]{:S(2)}, u32[]{:S(2)}) collective-permute-start(bf16[128,256]{1,0:T(8,128)(2,1)S(1)} %add_convert_fusion.1.refs_0_), channel_id=1, source_target_pairs={{0,16},{4,20},{8,24},{12,28},{16,0},{20,4},{24,8},{28,12},{1,17},{... | collective-permute-start | bytes 196616 | tf_op jit(solution)/shard_map/ppermute | solution.py:532
  116.3 6.4 %collective-permute-start.15 = (bf16[128,256]{1,0:T(8,128)(2,1)S(1)}, bf16[128,256]{1,0:T(8,128)(2,1)S(1)}, u32[]{:S(2)}, u32[]{:S(2)}) collective-permute-start(bf16[128,256]{1,0:T(8,128)(2,1)S(1)} %get-tuple-element.64), channel_id=1, source_target_pairs={{0,16},{4,20},{8,24},{12,28},{16,0},{20,4},{24,8},{28,12},{1,17},{... | collective-permute-start | bytes 196616 | tf_op jit(solution)/shard_map/ppermute | solution.py:532
  117.2 6.1 %collective-permute-start.25 = (bf16[128,256]{1,0:T(8,128)(2,1)S(1)}, bf16[128,256]{1,0:T(8,128)(2,1)S(1)}, u32[]{:S(2)}, u32[]{:S(2)}) collective-permute-start(bf16[128,256]{1,0:T(8,128)(2,1)S(1)} %add_convert_fusion.1.refs_0_), channel_id=1, source_target_pairs={{0,4},{4,0},{8,12},{12,8},{16,20},{20,16},{24,28},{28,24},{1,5},{5... | collective-permute-start | bytes 196616 | tf_op jit(solution)/shard_map/ppermute | solution.py:532
  118.4 8.6 %collective-permute-start.26 = (bf16[128,256]{1,0:T(8,128)(2,1)S(1)}, bf16[128,256]{1,0:T(8,128)(2,1)S(1)}, u32[]{:S(2)}, u32[]{:S(2)}) collective-permute-start(bf16[128,256]{1,0:T(8,128)(2,1)S(1)} %add_convert_fusion.1.refs_0_), channel_id=1, source_target_pairs={{0,8},{4,12},{8,0},{12,4},{16,24},{20,28},{24,16},{28,20},{1,9},{5... | collective-permute-start | bytes 196616 | tf_op jit(solution)/shard_map/ppermute | solution.py:532
  119.7 7.3 %collective-permute-start.27 = (bf16[128,256]{1,0:T(8,128)(2,1)S(1)}, bf16[128,256]{1,0:T(8,128)(2,1)S(1)}, u32[]{:S(2)}, u32[]{:S(2)}) collective-permute-start(bf16[128,256]{1,0:T(8,128)(2,1)S(1)} %add_convert_fusion.1.refs_0_), channel_id=1, source_target_pairs={{0,12},{4,8},{8,4},{12,0},{16,28},{20,24},{24,20},{28,16},{1,13},{... | collective-permute-start | bytes 196616 | tf_op jit(solution)/shard_map/ppermute | solution.py:532
  120.7 6.4 %collective-permute-start.29 = (bf16[128,256]{1,0:T(8,128)(2,1)S(1)}, bf16[128,256]{1,0:T(8,128)(2,1)S(1)}, u32[]{:S(2)}, u32[]{:S(2)}) collective-permute-start(bf16[128,256]{1,0:T(8,128)(2,1)S(1)} %collective-permute-done.28.refs_4_), channel_id=1, source_target_pairs={{0,4},{4,0},{8,12},{12,8},{16,20},{20,16},{24,28},{28,24},{1,5},{5... | collective-permute-start | bytes 196616 | tf_op jit(solution)/shard_map/ppermute | solution.py:532
  122.6 4.4 %collective-permute-start.30 = (bf16[128,256]{1,0:T(8,128)(2,1)S(1)}, bf16[128,256]{1,0:T(8,128)(2,1)S(1)}, u32[]{:S(2)}, u32[]{:S(2)}) collective-permute-start(bf16[128,256]{1,0:T(8,128)(2,1)S(1)} %collective-permute-done.28.refs_4_), channel_id=1, source_target_pairs={{0,8},{4,12},{8,0},{12,4},{16,24},{20,28},{24,16},{28,20},{1,9},{5... | collective-permute-start | bytes 196616 | tf_op jit(solution)/shard_map/ppermute | solution.py:532
  123.2 5.2 %collective-permute-start.31 = (bf16[128,256]{1,0:T(8,128)(2,1)S(1)}, bf16[128,256]{1,0:T(8,128)(2,1)S(1)}, u32[]{:S(2)}, u32[]{:S(2)}) collective-permute-start(bf16[128,256]{1,0:T(8,128)(2,1)S(1)} %collective-permute-done.28.refs_4_), channel_id=1, source_target_pairs={{0,12},{4,8},{8,4},{12,0},{16,28},{20,24},{24,20},{28,16},{1,13},{... | collective-permute-start | bytes 196616 | tf_op jit(solution)/shard_map/ppermute | solution.py:532

commit v3 on v2

--- a/solution.py
+++ b/solution.py
@@ -490,7 +490,7 @@
         in_specs=[smem()] + [vmem()] * 3,
         out_specs=(vmem(),) * 6,
         scratch_shapes=[pltpu.VMEM((blocks * BLOCK + 2 * PAD, width), f32)],
-        compiler_params=limit(min(60, 12 * max(1, blocks // 8))),
+        compiler_params=limit(min(60, 24 * max(1, blocks // 8))),
         name="enter",
     )(per_heads, x, drop, xw)
 
@@ -521,7 +521,7 @@
         + [pl.BlockSpec(memory_space=pltpu.HBM)] * len(bc),
         out_specs=(vmem(),) * (1 + half),
         scratch_shapes=scratch,
-        compiler_params=limit(min(60, 20 * max(1, blocks // 8))),
+        compiler_params=limit(min(60, 40 * max(1, blocks // 8))),
         name="mixer",
     )(at, per_heads, x, *entered, *filters, *bc)
     return outs[0], outs[1:]
@@ -540,7 +540,7 @@
         in_specs=specs,
         out_specs=jax.tree.map(lambda _: vmem(), outs),
         scratch_shapes=scratch,
-        compiler_params=limit(8),
+        compiler_params=limit(16),
     )(*args)
 
 
@@ -675,7 +675,7 @@
         out_shape=(shape((tokens, INNER), bf16), shape((HEADS, tokens), bf16)),
         in_specs=[vmem()],
         out_specs=(vmem(), vmem()),
-        compiler_params=limit(8),
+        compiler_params=limit(16),
         name="unpack",
     )(back_x)
     matrix = shape((share, GROUPS * STATE), f32)

time: 131 us -> 131 us (level)
  no operation moved by 1% of the time
where the time goes in v3:
time: 131 us
  waiting for transfers between devices  50.2 us (38%)
  starting transfers between devices  47.3 us (36%)
  Pallas kernels  29.8 us (23%)
  local copies, waits for them, and re-layouts  1.55 us (1%)
    ppermute x32, waiting for transfers between devices, swap(): return lax.ppermute(value, axis, [(i, i ^ bits) for i in range(size)])  50.2 us
    ppermute x32, starting transfers between devices, swap(): return lax.ppermute(value, axis, [(i, i ^ bits) for i in range(size)])  35.4 us
    pallas_call x1, Pallas kernels, run_mixer(): pl.pallas_call(functools.partial(mixer_kernel, len(bc)), out_shape=(jax.S...  12.8 us
    pallas_call x5, Pallas kernels, call(): pl.pallas_call(kernel, out_shape=outs, in_specs=specs, out_specs=jax.tree...  9.13 us
    all_to_all x1, starting transfers between devices, local(): heads_x = lax.all_to_all(packed, 'sp', 0, 0, tiled=True)  7.42 us
    all_to_all x1, starting transfers between devices, local(): back_x = lax.all_to_all(d_x, 'sp', 0, 0, tiled=True)  4.48 us
    pallas_call x1, Pallas kernels, local(): pl.pallas_call(prep_kernel, grid=(steps,), in_specs=[row_spec, row_spec,...  4.29 us
    pallas_call x1, Pallas kernels, run_enter(): pl.pallas_call(enter_kernel, out_shape=(shape((blocks, BLOCK, width), f32...  2.71 us
  transfers between devices with their start and end apart: 34, of which 9 were waited for; matrix products, arithmetic and copies ran while one was open for 2% of the time, Pallas kernels for 19%

profile of v3, /device:TPU:0, one launch (start us, length us, event | category | flops | bytes accessed | tf_op | source)
XLA Modules:
  0.0 130.8 jit_solution(12947457346721375749)
XLA Ops:
  0.6 4.3 %prep.1 = (bf16[8,264,256]{2,1,0:T(8,128)(2,1)}, bf16[128,2048]{1,0:T(8,128)(2,1)}) custom-call(bf16[128,2048]{1,0:T(8,128)(2,1)} %bitcast.39, bf16[128,2048]{1,0:T(8,128)(2,1)} %bitcast.40, bf16[128,2048]{1,0:T(8,128)(2,1)} %bitcast.41, f32[1,2048]{1,0:T(1,128)} %bitcast.44, bf16[128,2048]{1,0:T(8,128)(2,1)} %bitcast.42, bf16[32,128]{1,0:T(8,128)(2,1)} %bitcast.45), custom_call_target="tpu_custom_call" | custom-call | tf_op jit(solution)/shard_map/prep/pallas_call | solution.py:598
  4.9 7.4 %all-to-all-start = ((bf16[8,264,256]{2,1,0:T(8,128)(2,1)}), bf16[8,264,256]{2,1,0:T(8,128)(2,1)S(1)}, u32[]{:S(2)}, u32[]{:S(2)}) async-start(bf16[8,264,256]{2,1,0:T(8,128)(2,1)} %get-tuple-element.31), calls=%async_computation | async-start | bytes 2162688 | tf_op jit(solution)/shard_map/all_to_all | solution.py:626
  12.6 1.6 %collective-permute-start.3 = (bf16[512,512]{1,0:T(8,128)(2,1)S(1)}, bf16[512,512]{1,0:T(8,128)(2,1)S(1)}, u32[]{:S(2)}, u32[]{:S(2)}) collective-permute-start(bf16[512,512]{1,0:T(8,128)(2,1)S(1)} %pad_maximum_fusion.refs_0_), channel_id=1, source_target_pairs={{0,2},{1,3},{2,0},{3,1},{4,6},{5,7},{6,4},{7,5},{8,10},{9,11},{10,... | collective-permute-start | bytes 1572872 | tf_op jit(solution)/shard_map/ppermute | solution.py:532
  14.1 11.9 %collective-permute-done.3.refs_2_ = bf16[512,512]{1,0:T(8,128)(2,1)S(1)} collective-permute-done((bf16[512,512]{1,0:T(8,128)(2,1)S(1)}, bf16[512,512]{1,0:T(8,128)(2,1)S(1)}, u32[]{:S(2)}, u32[]{:S(2)}) %collective-permute-start.3) | collective-permute-done | bytes 524320 | tf_op jit(solution)/shard_map/ppermute | solution.py:532
  26.0 0.8 dynamic-slice_bitcast_fusion
  26.8 0.5 collective-permute-start
  27.3 1.5 %collective-permute-start.1 = (bf16[128,512]{1,0:T(8,128)(2,1)}, bf16[128,512]{1,0:T(8,128)(2,1)}, u32[]{:S(2)}, u32[]{:S(2)}) collective-permute-start(bf16[128,512]{1,0:T(8,128)(2,1)} %get-tuple-element.57), channel_id=1, source_target_pairs={{0,2},{1,3},{2,0},{3,1},{4,6},{5,7},{6,4},{7,5},{8,10},{9,11},{10,... | collective-permute-start | bytes 393224 | tf_op jit(solution)/shard_map/ppermute | solution.py:532
  28.9 1.5 %shard_map.200 = (bf16[128,256]{1,0:T(8,128)(2,1)S(1)}, bf16[128,256]{1,0:T(8,128)(2,1)S(1)}) custom-call(s32[4]{0:T(128)S(1)} %pad_add_fusion.at_ref, bf16[128,2048]{1,0:T(8,128)(2,1)S(1)} %bitcast.37, bf16[512,512]{1,0:T(8,128)(2,1)S(1)} %pad_maximum_fusion.refs_0_, bf16[512,512]{1,0:T(8,128)(2,1)S(1)} %collective-permute-done.2.refs_1_, ...), custom_call_target="tpu_custom_call" | custom-call | tf_op jit(solution)/shard_map/pallas_call | solution.py:537
  30.5 2.7 %collective-permute-start.8 = (bf16[128,256]{1,0:T(8,128)(2,1)S(1)}, bf16[128,256]{1,0:T(8,128)(2,1)S(1)}, u32[]{:S(2)}, u32[]{:S(2)}) collective-permute-start(bf16[128,256]{1,0:T(8,128)(2,1)S(1)} %get-tuple-element.40), channel_id=1, source_target_pairs={{0,16},{4,20},{8,24},{12,28},{16,0},{20,4},{24,8},{28,12},{1,17},{... | collective-permute-start | bytes 196616 | tf_op jit(solution)/shard_map/ppermute | solution.py:532
  33.2 1.5 %collective-permute-start.5 = (bf16[128,256]{1,0:T(8,128)(2,1)S(1)}, bf16[128,256]{1,0:T(8,128)(2,1)S(1)}, u32[]{:S(2)}, u32[]{:S(2)}) collective-permute-start(bf16[128,256]{1,0:T(8,128)(2,1)S(1)} %get-tuple-element.39.refs_10_), channel_id=1, source_target_pairs={{0,4},{4,0},{8,12},{12,8},{16,20},{20,16},{24,28},{28,24},{1,5},{5... | collective-permute-start | bytes 196616 | tf_op jit(solution)/shard_map/ppermute | solution.py:532
  34.6 1.5 %collective-permute-start.6 = (bf16[128,256]{1,0:T(8,128)(2,1)S(1)}, bf16[128,256]{1,0:T(8,128)(2,1)S(1)}, u32[]{:S(2)}, u32[]{:S(2)}) collective-permute-start(bf16[128,256]{1,0:T(8,128)(2,1)S(1)} %get-tuple-element.39.refs_10_), channel_id=1, source_target_pairs={{0,8},{4,12},{8,0},{12,4},{16,24},{20,28},{24,16},{28,20},{1,9},{5... | collective-permute-start | bytes 196616 | tf_op jit(solution)/shard_map/ppermute | solution.py:532
  36.1 0.6 collective-permute-start.7
  36.7 5.1 %collective-permute-done.8.refs_14_ = bf16[128,256]{1,0:T(8,128)(2,1)S(1)} collective-permute-done((bf16[128,256]{1,0:T(8,128)(2,1)S(1)}, bf16[128,256]{1,0:T(8,128)(2,1)S(1)}, u32[]{:S(2)}, u32[]{:S(2)}) %collective-permute-start.8) | collective-permute-done | bytes 65568 | tf_op jit(solution)/shard_map/ppermute | solution.py:532
  41.7 2.9 %collective-permute-start.11 = (bf16[128,256]{1,0:T(8,128)(2,1)S(1)}, bf16[128,256]{1,0:T(8,128)(2,1)S(1)}, u32[]{:S(2)}, u32[]{:S(2)}) collective-permute-start(bf16[128,256]{1,0:T(8,128)(2,1)S(1)} %collective-permute-done.8.refs_14_), channel_id=1, source_target_pairs={{0,12},{4,8},{8,4},{12,0},{16,28},{20,24},{24,20},{28,16},{1,13},{... | collective-permute-start | bytes 196616 | tf_op jit(solution)/shard_map/ppermute | solution.py:532
  44.6 0.6 collective-permute-start.9
  45.3 1.7 %shard_map.199 = (bf16[3,128,512]{2,1,0:T(8,128)(2,1)}, f32[4,1024]{1,0:T(4,128)S(1)}) custom-call(s32[4]{0:T(128)S(1)} %pad_add_fusion.at_ref, f32[4,1024]{1,0:T(4,128)S(1)} %bitcast.38, bf16[128,512]{1,0:T(8,128)(2,1)S(1)} %get-tuple-element.59.refs_0_.refs_4_, bf16[128,512]{1,0:T(8,128)(2,1)S(1)} %collective-permute-done.refs_1_.refs_5_, ...), custom_call_target="tpu_custom_call" | custom-call | tf_op jit(solution)/shard_map/pallas_call | solution.py:537
  47.0 2.7 %enter.1 = (f32[8,128,256]{2,1,0:T(8,128)S(1)}, f32[8,128,256]{2,1,0:T(8,128)S(1)}, f32[5,8,8,128]{3,2,1,0:T(8,128)S(1)}, f32[8,384,256]{2,1,0:T(8,128)S(1)}, bf...) custom-call(f32[3,4]{1,0:T(4,128)S(1)} %pad_maximum_fusion.1.head_ref, ...), custom_call_target="tpu_custom_call" | custom-call | tf_op jit(solution)/shard_map/enter/pallas_call | solution.py:480
  49.8 12.8 %mixer.1 = (bf16[8,136,256]{2,1,0:T(8,128)(2,1)}, bf16[2,128,256]{2,1,0:T(8,128)(2,1)S(1)}, bf16[2,128,256]{2,1,0:T(8,128)(2,1)}, bf16[2,128,256]{2,1,0:T(8,128)(2,1)}, bf16[2,128,256]{2,1,0:T(8,128)(2,1)}) custom-call(s32[4]{0:T(128)S(1)} %pad_add_fusion.at_ref, f32[3,4]{1,0:T(4,128)S(1)} %pad_maximum_fusion.1.head_ref, ...), custom_call_target="tpu_custom_call" | custom-call | tf_op jit(solution)/shard_map/mixer/pallas_call | solution.py:515
  62.6 0.6 copy-done.1
  63.3 1.4 %collective-permute-start.12 = (bf16[2,128,256]{2,1,0:T(8,128)(2,1)}, bf16[2,128,256]{2,1,0:T(8,128)(2,1)S(1)}, u32[]{:S(2)}, u32[]{:S(2)}) collective-permute-start(bf16[2,128,256]{2,1,0:T(8,128)(2,1)} %get-tuple-element.42), channel_id=1, source_target_pairs={{0,4},{4,0},{8,12},{12,8},{16,20},{20,16},{24,28},{28,24},{1,5},{5... | collective-permute-start | bytes 393224 | tf_op jit(solution)/shard_map/ppermute | solution.py:532
  64.7 2.0 %collective-permute-start.14 = (bf16[2,128,256]{2,1,0:T(8,128)(2,1)}, bf16[2,128,256]{2,1,0:T(8,128)(2,1)}, u32[]{:S(2)}, u32[]{:S(2)}) collective-permute-start(bf16[2,128,256]{2,1,0:T(8,128)(2,1)} %get-tuple-element.44), channel_id=1, source_target_pairs={{0,12},{4,8},{8,4},{12,0},{16,28},{20,24},{24,20},{28,16},{1,13},{... | collective-permute-start | bytes 393224 | tf_op jit(solution)/shard_map/ppermute | solution.py:532
  66.8 0.6 collective-permute-start.20
  67.4 4.5 %all-to-all-start.1 = ((bf16[8,136,256]{2,1,0:T(8,128)(2,1)}), bf16[8,136,256]{2,1,0:T(8,128)(2,1)S(1)}, u32[]{:S(2)}, u32[]{:S(2)}) async-start(bf16[8,136,256]{2,1,0:T(8,128)(2,1)} %get-tuple-element.45), calls=%async_computation.1 | async-start | bytes 1114112 | tf_op jit(solution)/shard_map/all_to_all | solution.py:653
  71.8 2.9 %collective-permute-start.21 = (bf16[128,512]{1,0:T(8,128)(2,1)S(1)}, bf16[128,512]{1,0:T(8,128)(2,1)S(1)}, u32[]{:S(2)}, u32[]{:S(2)}) collective-permute-start(bf16[128,512]{1,0:T(8,128)(2,1)S(1)} %collective-permute-done.19.refs_7_), channel_id=1, source_target_pairs={{0,16},{4,20},{8,24},{12,28},{16,0},{20,4},{24,8},{28,12},{1,17},{... | collective-permute-start | bytes 393224 | tf_op jit(solution)/shard_map/ppermute | solution.py:532
  74.8 1.2 collective-permute-done.14
  76.0 1.0 add_convert_fusion.refs_0_
  76.9 0.3 collective-permute-start.16
  77.3 1.6 %collective-permute-start.17 = (bf16[2,128,256]{2,1,0:T(8,128)(2,1)S(1)}, bf16[2,128,256]{2,1,0:T(8,128)(2,1)S(1)}, u32[]{:S(2)}, u32[]{:S(2)}) collective-permute-start(bf16[2,128,256]{2,1,0:T(8,128)(2,1)S(1)} %add_convert_fusion.refs_0_), channel_id=1, source_target_pairs={{0,2},{1,3},{2,0},{3,1},{4,6},{5,7},{6,4},{7,5},{8,10},{9,11},{10,... | collective-permute-start | bytes 393224 | tf_op jit(solution)/shard_map/ppermute | solution.py:532
  78.9 26.8 %collective-permute-done.21.refs_9_ = bf16[128,512]{1,0:T(8,128)(2,1)S(1)} collective-permute-done((bf16[128,512]{1,0:T(8,128)(2,1)S(1)}, bf16[128,512]{1,0:T(8,128)(2,1)S(1)}, u32[]{:S(2)}, u32[]{:S(2)}) %collective-permute-start.21) | collective-permute-done | bytes 131104 | tf_op jit(solution)/shard_map/ppermute | solution.py:532
  105.7 1.7 %shard_map.202 = (bf16[128,256]{1,0:T(8,128)(2,1)S(1)}, bf16[128,256]{1,0:T(8,128)(2,1)S(1)}, bf16[128,256]{1,0:T(8,128)(2,1)S(1)}, bf16[128,256]{1,0:T(8,128)(2,1)S(1)}) custom-call(s32[4]{0:T(128)S(1)} %pad_add_fusion.at_ref, bf16[2,128,256]{2,1,0:T(8,128)(2,1)S(1)} %add_convert_fusion.refs_0_, bf16[2,128,256]{2,1,0:T(8,128)(2,1)S(1)} %collective-permute-done.16.refs_1_, ...), custom_call_target="tpu_custom_call" | custom-call | tf_op jit(solution)/shard_map/pallas_call | solution.py:537
  107.4 1.5 %collective-permute-start.22 = (bf16[128,256]{1,0:T(8,128)(2,1)S(1)}, bf16[128,256]{1,0:T(8,128)(2,1)S(1)}, u32[]{:S(2)}, u32[]{:S(2)}) collective-permute-start(bf16[128,256]{1,0:T(8,128)(2,1)S(1)} %get-tuple-element.51), channel_id=1, source_target_pairs={{0,4},{4,0},{8,12},{12,8},{16,20},{20,16},{24,28},{28,24},{1,5},{5... | collective-permute-start | bytes 196616 | tf_op jit(solution)/shard_map/ppermute | solution.py:532
  108.9 2.1 %collective-permute-start.24 = (bf16[128,256]{1,0:T(8,128)(2,1)S(1)}, bf16[128,256]{1,0:T(8,128)(2,1)S(1)}, u32[]{:S(2)}, u32[]{:S(2)}) collective-permute-start(bf16[128,256]{1,0:T(8,128)(2,1)S(1)} %get-tuple-element.53), channel_id=1, source_target_pairs={{0,12},{4,8},{8,4},{12,0},{16,28},{20,24},{24,20},{28,16},{1,13},{... | collective-permute-start | bytes 196616 | tf_op jit(solution)/shard_map/ppermute | solution.py:532
  111.0 0.8 collective-permute-done.22
  111.7 1.5 %collective-permute-done.23 = bf16[128,256]{1,0:T(8,128)(2,1)S(1)} collective-permute-done((bf16[128,256]{1,0:T(8,128)(2,1)S(1)}, bf16[128,256]{1,0:T(8,128)(2,1)S(1)}, u32[]{:S(2)}, u32[]{:S(2)}) %collective-permute-start.23) | collective-permute-done | bytes 65568 | tf_op jit(solution)/shard_map/ppermute | solution.py:532
  113.2 0.9 collective-permute-done.24
  114.1 2.1 %collective-permute-start.28 = (bf16[128,256]{1,0:T(8,128)(2,1)S(1)}, bf16[128,256]{1,0:T(8,128)(2,1)S(1)}, u32[]{:S(2)}, u32[]{:S(2)}) collective-permute-start(bf16[128,256]{1,0:T(8,128)(2,1)S(1)} %add_convert_fusion.1.refs_0_), channel_id=1, source_target_pairs={{0,16},{4,20},{8,24},{12,28},{16,0},{20,4},{24,8},{28,12},{1,17},{... | collective-permute-start | bytes 196616 | tf_op jit(solution)/shard_map/ppermute | solution.py:532
  116.2 0.9 collective-permute-start.15
  117.1 1.3 collective-permute-start.25
  118.4 1.3 collective-permute-start.26
  119.7 0.9 collective-permute-start.27
  120.6 1.3 collective-permute-start.29
  121.9 0.7 collective-permute-done.15.other_ref
  122.6 0.6 collective-permute-start.30
  123.2 1.2 collective-permute-start.31
  124.4 2.7 %shard_map.201 = bf16[128,2048]{1,0:T(8,128)(2,1)} custom-call(s32[4]{0:T(128)S(1)} %pad_add_fusion.at_ref, bf16[128,256]{1,0:T(8,128)(2,1)S(1)} %get-tuple-element.65.own_ref, bf16[128,256]{1,0:T(8,128)(2,1)S(1)} %collective-permute-done.15.other_ref, bf16[512,512]{1,0:T(8,128)(2,1)S(1)} %pad_maximum_fusion.refs_0_, ...), custom_call_target="tpu_custom_call" | custom-call | tf_op jit(solution)/shard_map/pallas_call | solution.py:537
  127.0 1.3 %collective-permute-done.31.refs_7_ = bf16[128,256]{1,0:T(8,128)(2,1)S(1)} collective-permute-done((bf16[128,256]{1,0:T(8,128)(2,1)S(1)}, bf16[128,256]{1,0:T(8,128)(2,1)S(1)}, u32[]{:S(2)}, u32[]{:S(2)}) %collective-permute-start.31) | collective-permute-done | bytes 65568 | tf_op jit(solution)/shard_map/ppermute | solution.py:532
  128.4 1.6 %shard_map.203 = (f32[512,256]{1,0:T(8,128)}, f32[512,256]{1,0:T(8,128)}) custom-call(s32[4]{0:T(128)S(1)} %pad_add_fusion.at_ref, bf16[128,256]{1,0:T(8,128)(2,1)S(1)} %add_convert_fusion.1.refs_0_, bf16[128,256]{1,0:T(8,128)(2,1)S(1)} %collective-permute-done.25.refs_1_, bf16[128,256]{1,0:T(8,128)(2,1)S(1)} %collective-permute-done.26.refs_2_, ...), custom_call_target="tpu_custom_call" | custom-call | tf_op jit(solution)/shard_map/pallas_call | solution.py:537
  130.0 0.8 unpack.1
  (61 shorter events, 0.5 us)
Async XLA Ops:
  4.9 7.4 %copy-start.7 = (bf16[512,256]{1,0:T(8,128)(2,1)S(1)}, bf16[512,256]{1,0:T(8,128)(2,1)}, u32[]{:S(2)}) copy-start(bf16[512,256]{1,0:T(8,128)(2,1)} %param.17) | copy-start | bytes 786436
  4.9 7.4 %copy-start.8 = (bf16[512,256]{1,0:T(8,128)(2,1)S(1)}, bf16[512,256]{1,0:T(8,128)(2,1)}, u32[]{:S(2)}) copy-start(bf16[512,256]{1,0:T(8,128)(2,1)} %param.18) | copy-start | bytes 786436
  4.9 42.0 %all-to-all-start = ((bf16[8,264,256]{2,1,0:T(8,128)(2,1)}), bf16[8,264,256]{2,1,0:T(8,128)(2,1)S(1)}, u32[]{:S(2)}, u32[]{:S(2)}) async-start(bf16[8,264,256]{2,1,0:T(8,128)(2,1)} %get-tuple-element.31), calls=%async_computation | async-start | bytes 2162688 | tf_op jit(solution)/shard_map/all_to_all | solution.py:626
  12.4 13.6 %copy-start = (bf16[1,128,2048]{2,1,0:T(8,128)(2,1)S(1)}, bf16[1,128,2048]{2,1,0:T(8,128)(2,1)}, u32[]{:S(2)}) copy-start(bf16[1,128,2048]{2,1,0:T(8,128)(2,1)} %param.16) | copy-start | bytes 1572868
  12.6 13.4 %collective-permute-start.3 = (bf16[512,512]{1,0:T(8,128)(2,1)S(1)}, bf16[512,512]{1,0:T(8,128)(2,1)S(1)}, u32[]{:S(2)}, u32[]{:S(2)}) collective-permute-start(bf16[512,512]{1,0:T(8,128)(2,1)S(1)} %pad_maximum_fusion.refs_0_), channel_id=1, source_target_pairs={{0,2},{1,3},{2,0},{3,1},{4,6},{5,7},{6,4},{7,5},{8,10},{9,11},{10,... | collective-permute-start | bytes 1572872 | tf_op jit(solution)/shard_map/ppermute | solution.py:532
  14.1 14.7 %collective-permute-start.2 = (bf16[512,512]{1,0:T(8,128)(2,1)S(1)}, bf16[512,512]{1,0:T(8,128)(2,1)S(1)}, u32[]{:S(2)}, u32[]{:S(2)}) collective-permute-start(bf16[512,512]{1,0:T(8,128)(2,1)S(1)} %pad_maximum_fusion.refs_0_), channel_id=1, source_target_pairs={{0,1},{1,0},{2,3},{3,2},{4,5},{5,4},{6,7},{7,6},{8,9},{9,8},{10,11... | collective-permute-start | bytes 1572872 | tf_op jit(solution)/shard_map/ppermute | solution.py:532
  26.0 2.9 %collective-permute-start.4 = (bf16[512,512]{1,0:T(8,128)(2,1)S(1)}, bf16[512,512]{1,0:T(8,128)(2,1)}, u32[]{:S(2)}, u32[]{:S(2)}) collective-permute-start(bf16[512,512]{1,0:T(8,128)(2,1)S(1)} %collective-permute-done.3.refs_2_), channel_id=1, source_target_pairs={{0,1},{1,0},{2,3},{3,2},{4,5},{5,4},{6,7},{7,6},{8,9},{9,8},{10,11... | collective-permute-start | bytes 1572872 | tf_op jit(solution)/shard_map/ppermute | solution.py:532
  26.8 9.3 %collective-permute-start = (bf16[128,512]{1,0:T(8,128)(2,1)}, bf16[128,512]{1,0:T(8,128)(2,1)S(1)}, u32[]{:S(2)}, u32[]{:S(2)}) collective-permute-start(bf16[128,512]{1,0:T(8,128)(2,1)} %get-tuple-element.58), channel_id=1, source_target_pairs={{0,1},{1,0},{2,3},{3,2},{4,5},{5,4},{6,7},{7,6},{8,9},{9,8},{10,11... | collective-permute-start | bytes 393224 | tf_op jit(solution)/shard_map/ppermute | solution.py:532
  27.3 14.5 %collective-permute-start.1 = (bf16[128,512]{1,0:T(8,128)(2,1)}, bf16[128,512]{1,0:T(8,128)(2,1)}, u32[]{:S(2)}, u32[]{:S(2)}) collective-permute-start(bf16[128,512]{1,0:T(8,128)(2,1)} %get-tuple-element.57), channel_id=1, source_target_pairs={{0,2},{1,3},{2,0},{3,1},{4,6},{5,7},{6,4},{7,5},{8,10},{9,11},{10,... | collective-permute-start | bytes 393224 | tf_op jit(solution)/shard_map/ppermute | solution.py:532
  28.9 16.4 %copy-start.9 = (f32[4]{0:T(128)S(1)}, f32[4]{0:T(128)}, u32[]{:S(2)}) copy-start(f32[4]{0:T(128)} %param.30) | copy-start | bytes 52
  28.9 16.4 %copy-start.10 = (f32[4]{0:T(128)S(1)}, f32[4]{0:T(128)}, u32[]{:S(2)}) copy-start(f32[4]{0:T(128)} %param.29) | copy-start | bytes 52
  28.9 16.4 %copy-start.11 = (f32[4]{0:T(128)S(1)}, f32[4]{0:T(128)}, u32[]{:S(2)}) copy-start(f32[4]{0:T(128)} %param.28) | copy-start | bytes 52
  28.9 16.4 %copy-start.4 = (f32[1,1024,4]{1,2,0:T(4,128)S(1)}, f32[1,1024,4]{1,2,0:T(4,128)}, u32[]{:S(2)}) copy-start(f32[1,1024,4]{1,2,0:T(4,128)} %param.24) | copy-start | bytes 49156
  28.9 18.0 %copy-start.3 = (f32[5,256]{1,0:T(8,128)S(1)}, f32[5,256]{1,0:T(8,128)}, u32[]{:S(2)}) copy-start(f32[5,256]{1,0:T(8,128)} %refs_7_.1) | copy-start | bytes 15364
  30.5 19.4 %copy-start.5 = (f32[5,256]{1,0:T(8,128)S(1)}, f32[5,256]{1,0:T(8,128)}, u32[]{:S(2)}) copy-start(f32[5,256]{1,0:T(8,128)} %refs_8_.1) | copy-start | bytes 15364
  30.5 19.4 %copy-start.6 = (f32[5,256]{1,0:T(8,128)S(1)}, f32[5,256]{1,0:T(8,128)}, u32[]{:S(2)}) copy-start(f32[5,256]{1,0:T(8,128)} %refs_9_.1) | copy-start | bytes 15364
  30.5 11.3 %collective-permute-start.8 = (bf16[128,256]{1,0:T(8,128)(2,1)S(1)}, bf16[128,256]{1,0:T(8,128)(2,1)S(1)}, u32[]{:S(2)}, u32[]{:S(2)}) collective-permute-start(bf16[128,256]{1,0:T(8,128)(2,1)S(1)} %get-tuple-element.40), channel_id=1, source_target_pairs={{0,16},{4,20},{8,24},{12,28},{16,0},{20,4},{24,8},{28,12},{1,17},{... | collective-permute-start | bytes 196616 | tf_op jit(solution)/shard_map/ppermute | solution.py:532
  33.2 11.4 %collective-permute-start.5 = (bf16[128,256]{1,0:T(8,128)(2,1)S(1)}, bf16[128,256]{1,0:T(8,128)(2,1)S(1)}, u32[]{:S(2)}, u32[]{:S(2)}) collective-permute-start(bf16[128,256]{1,0:T(8,128)(2,1)S(1)} %get-tuple-element.39.refs_10_), channel_id=1, source_target_pairs={{0,4},{4,0},{8,12},{12,8},{16,20},{20,16},{24,28},{28,24},{1,5},{5... | collective-permute-start | bytes 196616 | tf_op jit(solution)/shard_map/ppermute | solution.py:532
  34.6 15.0 %collective-permute-start.6 = (bf16[128,256]{1,0:T(8,128)(2,1)S(1)}, bf16[128,256]{1,0:T(8,128)(2,1)S(1)}, u32[]{:S(2)}, u32[]{:S(2)}) collective-permute-start(bf16[128,256]{1,0:T(8,128)(2,1)S(1)} %get-tuple-element.39.refs_10_), channel_id=1, source_target_pairs={{0,8},{4,12},{8,0},{12,4},{16,24},{20,28},{24,16},{28,20},{1,9},{5... | collective-permute-start | bytes 196616 | tf_op jit(solution)/shard_map/ppermute | solution.py:532
  36.1 13.7 %collective-permute-start.7 = (bf16[128,256]{1,0:T(8,128)(2,1)S(1)}, bf16[128,256]{1,0:T(8,128)(2,1)S(1)}, u32[]{:S(2)}, u32[]{:S(2)}) collective-permute-start(bf16[128,256]{1,0:T(8,128)(2,1)S(1)} %get-tuple-element.39.refs_10_), channel_id=1, source_target_pairs={{0,12},{4,8},{8,4},{12,0},{16,28},{20,24},{24,20},{28,16},{1,13},{... | collective-permute-start | bytes 196616 | tf_op jit(solution)/shard_map/ppermute | solution.py:532
  41.7 8.0 %collective-permute-start.10 = (bf16[128,256]{1,0:T(8,128)(2,1)S(1)}, bf16[128,256]{1,0:T(8,128)(2,1)S(1)}, u32[]{:S(2)}, u32[]{:S(2)}) collective-permute-start(bf16[128,256]{1,0:T(8,128)(2,1)S(1)} %collective-permute-done.8.refs_14_), channel_id=1, source_target_pairs={{0,8},{4,12},{8,0},{12,4},{16,24},{20,28},{24,16},{28,20},{1,9},{5... | collective-permute-start | bytes 196616 | tf_op jit(solution)/shard_map/ppermute | solution.py:532
  41.7 8.1 %collective-permute-start.11 = (bf16[128,256]{1,0:T(8,128)(2,1)S(1)}, bf16[128,256]{1,0:T(8,128)(2,1)S(1)}, u32[]{:S(2)}, u32[]{:S(2)}) collective-permute-start(bf16[128,256]{1,0:T(8,128)(2,1)S(1)} %collective-permute-done.8.refs_14_), channel_id=1, source_target_pairs={{0,12},{4,8},{8,4},{12,0},{16,28},{20,24},{24,20},{28,16},{1,13},{... | collective-permute-start | bytes 196616 | tf_op jit(solution)/shard_map/ppermute | solution.py:532
  44.6 5.2 %collective-permute-start.9 = (bf16[128,256]{1,0:T(8,128)(2,1)S(1)}, bf16[128,256]{1,0:T(8,128)(2,1)}, u32[]{:S(2)}, u32[]{:S(2)}) collective-permute-start(bf16[128,256]{1,0:T(8,128)(2,1)S(1)} %collective-permute-done.8.refs_14_), channel_id=1, source_target_pairs={{0,4},{4,0},{8,12},{12,8},{16,20},{20,16},{24,28},{28,24},{1,5},{5... | collective-permute-start | bytes 196616 | tf_op jit(solution)/shard_map/ppermute | solution.py:532
  49.7 22.1 %collective-permute-start.19 = (bf16[128,512]{1,0:T(8,128)(2,1)}, bf16[128,512]{1,0:T(8,128)(2,1)S(1)}, u32[]{:S(2)}, u32[]{:S(2)}) collective-permute-start(bf16[128,512]{1,0:T(8,128)(2,1)} %get-tuple-element.56), channel_id=1, source_target_pairs={{0,3},{1,2},{2,1},{3,0},{4,7},{5,6},{6,5},{7,4},{8,11},{9,10},{10,... | collective-permute-start | bytes 393224 | tf_op jit(solution)/shard_map/ppermute | solution.py:532
  62.6 0.6 copy-start.1
  63.3 12.7 %copy-start.2 = (bf16[2,128,256]{2,1,0:T(8,128)(2,1)S(1)}, bf16[2,128,256]{2,1,0:T(8,128)(2,1)}, u32[]{:S(2)}) copy-start(bf16[2,128,256]{2,1,0:T(8,128)(2,1)} %copy-done.1) | copy-start | bytes 393220
  63.3 11.5 %collective-permute-start.12 = (bf16[2,128,256]{2,1,0:T(8,128)(2,1)}, bf16[2,128,256]{2,1,0:T(8,128)(2,1)S(1)}, u32[]{:S(2)}, u32[]{:S(2)}) collective-permute-start(bf16[2,128,256]{2,1,0:T(8,128)(2,1)} %get-tuple-element.42), channel_id=1, source_target_pairs={{0,4},{4,0},{8,12},{12,8},{16,20},{20,16},{24,28},{28,24},{1,5},{5... | collective-permute-start | bytes 393224 | tf_op jit(solution)/shard_map/ppermute | solution.py:532
  64.7 10.1 %collective-permute-start.13 = (bf16[2,128,256]{2,1,0:T(8,128)(2,1)}, bf16[2,128,256]{2,1,0:T(8,128)(2,1)S(1)}, u32[]{:S(2)}, u32[]{:S(2)}) collective-permute-start(bf16[2,128,256]{2,1,0:T(8,128)(2,1)} %get-tuple-element.43), channel_id=1, source_target_pairs={{0,8},{4,12},{8,0},{12,4},{16,24},{20,28},{24,16},{28,20},{1,9},{5... | collective-permute-start | bytes 393224 | tf_op jit(solution)/shard_map/ppermute | solution.py:532
  64.7 11.2 %collective-permute-start.14 = (bf16[2,128,256]{2,1,0:T(8,128)(2,1)}, bf16[2,128,256]{2,1,0:T(8,128)(2,1)}, u32[]{:S(2)}, u32[]{:S(2)}) collective-permute-start(bf16[2,128,256]{2,1,0:T(8,128)(2,1)} %get-tuple-element.44), channel_id=1, source_target_pairs={{0,12},{4,8},{8,4},{12,0},{16,28},{20,24},{24,20},{28,16},{1,13},{... | collective-permute-start | bytes 393224 | tf_op jit(solution)/shard_map/ppermute | solution.py:532
  66.8 38.9 %collective-permute-start.20 = (bf16[3,128,512]{2,1,0:T(8,128)(2,1)}, bf16[3,128,512]{2,1,0:T(8,128)(2,1)S(1)}, u32[]{:S(2)}, u32[]{:S(2)}) collective-permute-start(bf16[3,128,512]{2,1,0:T(8,128)(2,1)} %get-tuple-element.49), channel_id=1, source_target_pairs={{0,16},{4,20},{8,24},{12,28},{16,0},{20,4},{24,8},{28,12},{1,17},{... | collective-permute-start | bytes 1179656 | tf_op jit(solution)/shard_map/ppermute | solution.py:532
  67.4 62.6 %all-to-all-start.1 = ((bf16[8,136,256]{2,1,0:T(8,128)(2,1)}), bf16[8,136,256]{2,1,0:T(8,128)(2,1)S(1)}, u32[]{:S(2)}, u32[]{:S(2)}) async-start(bf16[8,136,256]{2,1,0:T(8,128)(2,1)} %get-tuple-element.45), calls=%async_computation.1 | async-start | bytes 1114112 | tf_op jit(solution)/shard_map/all_to_all | solution.py:653
  71.8 33.8 %collective-permute-start.21 = (bf16[128,512]{1,0:T(8,128)(2,1)S(1)}, bf16[128,512]{1,0:T(8,128)(2,1)S(1)}, u32[]{:S(2)}, u32[]{:S(2)}) collective-permute-start(bf16[128,512]{1,0:T(8,128)(2,1)S(1)} %collective-permute-done.19.refs_7_), channel_id=1, source_target_pairs={{0,16},{4,20},{8,24},{12,28},{16,0},{20,4},{24,8},{28,12},{1,17},{... | collective-permute-start | bytes 393224 | tf_op jit(solution)/shard_map/ppermute | solution.py:532
  76.9 28.8 %collective-permute-start.16 = (bf16[2,128,256]{2,1,0:T(8,128)(2,1)S(1)}, bf16[2,128,256]{2,1,0:T(8,128)(2,1)S(1)}, u32[]{:S(2)}, u32[]{:S(2)}) collective-permute-start(bf16[2,128,256]{2,1,0:T(8,128)(2,1)S(1)} %add_convert_fusion.refs_0_), channel_id=1, source_target_pairs={{0,1},{1,0},{2,3},{3,2},{4,5},{5,4},{6,7},{7,6},{8,9},{9,8},{10,11... | collective-permute-start | bytes 393224 | tf_op jit(solution)/shard_map/ppermute | solution.py:532
  77.3 28.4 %collective-permute-start.17 = (bf16[2,128,256]{2,1,0:T(8,128)(2,1)S(1)}, bf16[2,128,256]{2,1,0:T(8,128)(2,1)S(1)}, u32[]{:S(2)}, u32[]{:S(2)}) collective-permute-start(bf16[2,128,256]{2,1,0:T(8,128)(2,1)S(1)} %add_convert_fusion.refs_0_), channel_id=1, source_target_pairs={{0,2},{1,3},{2,0},{3,1},{4,6},{5,7},{6,4},{7,5},{8,10},{9,11},{10,... | collective-permute-start | bytes 393224 | tf_op jit(solution)/shard_map/ppermute | solution.py:532
  78.8 26.9 %collective-permute-start.18 = (bf16[2,128,256]{2,1,0:T(8,128)(2,1)S(1)}, bf16[2,128,256]{2,1,0:T(8,128)(2,1)S(1)}, u32[]{:S(2)}, u32[]{:S(2)}) collective-permute-start(bf16[2,128,256]{2,1,0:T(8,128)(2,1)S(1)} %add_convert_fusion.refs_0_), channel_id=1, source_target_pairs={{0,3},{1,2},{2,1},{3,0},{4,7},{5,6},{6,5},{7,4},{8,11},{9,10},{10,... | collective-permute-start | bytes 393224 | tf_op jit(solution)/shard_map/ppermute | solution.py:532
  107.4 4.3 %collective-permute-start.22 = (bf16[128,256]{1,0:T(8,128)(2,1)S(1)}, bf16[128,256]{1,0:T(8,128)(2,1)S(1)}, u32[]{:S(2)}, u32[]{:S(2)}) collective-permute-start(bf16[128,256]{1,0:T(8,128)(2,1)S(1)} %get-tuple-element.51), channel_id=1, source_target_pairs={{0,4},{4,0},{8,12},{12,8},{16,20},{20,16},{24,28},{28,24},{1,5},{5... | collective-permute-start | bytes 196616 | tf_op jit(solution)/shard_map/ppermute | solution.py:532
  108.9 4.3 %collective-permute-start.23 = (bf16[128,256]{1,0:T(8,128)(2,1)S(1)}, bf16[128,256]{1,0:T(8,128)(2,1)S(1)}, u32[]{:S(2)}, u32[]{:S(2)}) collective-permute-start(bf16[128,256]{1,0:T(8,128)(2,1)S(1)} %get-tuple-element.52), channel_id=1, source_target_pairs={{0,8},{4,12},{8,0},{12,4},{16,24},{20,28},{24,16},{28,20},{1,9},{5... | collective-permute-start | bytes 196616 | tf_op jit(solution)/shard_map/ppermute | solution.py:532
  108.9 5.2 %collective-permute-start.24 = (bf16[128,256]{1,0:T(8,128)(2,1)S(1)}, bf16[128,256]{1,0:T(8,128)(2,1)S(1)}, u32[]{:S(2)}, u32[]{:S(2)}) collective-permute-start(bf16[128,256]{1,0:T(8,128)(2,1)S(1)} %get-tuple-element.53), channel_id=1, source_target_pairs={{0,12},{4,8},{8,4},{12,0},{16,28},{20,24},{24,20},{28,16},{1,13},{... | collective-permute-start | bytes 196616 | tf_op jit(solution)/shard_map/ppermute | solution.py:532
  114.1 6.5 %collective-permute-start.28 = (bf16[128,256]{1,0:T(8,128)(2,1)S(1)}, bf16[128,256]{1,0:T(8,128)(2,1)S(1)}, u32[]{:S(2)}, u32[]{:S(2)}) collective-permute-start(bf16[128,256]{1,0:T(8,128)(2,1)S(1)} %add_convert_fusion.1.refs_0_), channel_id=1, source_target_pairs={{0,16},{4,20},{8,24},{12,28},{16,0},{20,4},{24,8},{28,12},{1,17},{... | collective-permute-start | bytes 196616 | tf_op jit(solution)/shard_map/ppermute | solution.py:532
  116.2 6.4 %collective-permute-start.15 = (bf16[128,256]{1,0:T(8,128)(2,1)S(1)}, bf16[128,256]{1,0:T(8,128)(2,1)S(1)}, u32[]{:S(2)}, u32[]{:S(2)}) collective-permute-start(bf16[128,256]{1,0:T(8,128)(2,1)S(1)} %get-tuple-element.64), channel_id=1, source_target_pairs={{0,16},{4,20},{8,24},{12,28},{16,0},{20,4},{24,8},{28,12},{1,17},{... | collective-permute-start | bytes 196616 | tf_op jit(solution)/shard_map/ppermute | solution.py:532
  117.1 6.1 %collective-permute-start.25 = (bf16[128,256]{1,0:T(8,128)(2,1)S(1)}, bf16[128,256]{1,0:T(8,128)(2,1)S(1)}, u32[]{:S(2)}, u32[]{:S(2)}) collective-permute-start(bf16[128,256]{1,0:T(8,128)(2,1)S(1)} %add_convert_fusion.1.refs_0_), channel_id=1, source_target_pairs={{0,4},{4,0},{8,12},{12,8},{16,20},{20,16},{24,28},{28,24},{1,5},{5... | collective-permute-start | bytes 196616 | tf_op jit(solution)/shard_map/ppermute | solution.py:532
  118.4 8.6 %collective-permute-start.26 = (bf16[128,256]{1,0:T(8,128)(2,1)S(1)}, bf16[128,256]{1,0:T(8,128)(2,1)S(1)}, u32[]{:S(2)}, u32[]{:S(2)}) collective-permute-start(bf16[128,256]{1,0:T(8,128)(2,1)S(1)} %add_convert_fusion.1.refs_0_), channel_id=1, source_target_pairs={{0,8},{4,12},{8,0},{12,4},{16,24},{20,28},{24,16},{28,20},{1,9},{5... | collective-permute-start | bytes 196616 | tf_op jit(solution)/shard_map/ppermute | solution.py:532
  119.7 7.3 %collective-permute-start.27 = (bf16[128,256]{1,0:T(8,128)(2,1)S(1)}, bf16[128,256]{1,0:T(8,128)(2,1)S(1)}, u32[]{:S(2)}, u32[]{:S(2)}) collective-permute-start(bf16[128,256]{1,0:T(8,128)(2,1)S(1)} %add_convert_fusion.1.refs_0_), channel_id=1, source_target_pairs={{0,12},{4,8},{8,4},{12,0},{16,28},{20,24},{24,20},{28,16},{1,13},{... | collective-permute-start | bytes 196616 | tf_op jit(solution)/shard_map/ppermute | solution.py:532
  120.6 6.4 %collective-permute-start.29 = (bf16[128,256]{1,0:T(8,128)(2,1)S(1)}, bf16[128,256]{1,0:T(8,128)(2,1)S(1)}, u32[]{:S(2)}, u32[]{:S(2)}) collective-permute-start(bf16[128,256]{1,0:T(8,128)(2,1)S(1)} %collective-permute-done.28.refs_4_), channel_id=1, source_target_pairs={{0,4},{4,0},{8,12},{12,8},{16,20},{20,16},{24,28},{28,24},{1,5},{5... | collective-permute-start | bytes 196616 | tf_op jit(solution)/shard_map/ppermute | solution.py:532
  122.6 4.4 %collective-permute-start.30 = (bf16[128,256]{1,0:T(8,128)(2,1)S(1)}, bf16[128,256]{1,0:T(8,128)(2,1)S(1)}, u32[]{:S(2)}, u32[]{:S(2)}) collective-permute-start(bf16[128,256]{1,0:T(8,128)(2,1)S(1)} %collective-permute-done.28.refs_4_), channel_id=1, source_target_pairs={{0,8},{4,12},{8,0},{12,4},{16,24},{20,28},{24,16},{28,20},{1,9},{5... | collective-permute-start | bytes 196616 | tf_op jit(solution)/shard_map/ppermute | solution.py:532
  123.2 5.2 %collective-permute-start.31 = (bf16[128,256]{1,0:T(8,128)(2,1)S(1)}, bf16[128,256]{1,0:T(8,128)(2,1)S(1)}, u32[]{:S(2)}, u32[]{:S(2)}) collective-permute-start(bf16[128,256]{1,0:T(8,128)(2,1)S(1)} %collective-permute-done.28.refs_4_), channel_id=1, source_target_pairs={{0,12},{4,8},{8,4},{12,0},{16,28},{20,24},{24,20},{28,16},{1,13},{... | collective-permute-start | bytes 196616 | tf_op jit(solution)/shard_map/ppermute | solution.py:532

commit v4 on v3

--- a/solution.py
+++ b/solution.py
@@ -342,7 +342,7 @@
             decay = wide_s[b][2 * BLOCK - 1 : 2 * BLOCK]
             return carry * decay + st_s[b, :, at]
 
-        lax.fori_loop(0, blocks, step, jnp.zeros((STATE, width), f32))
+        lax.fori_loop(0, blocks, step, jnp.zeros((STATE, width), f32), unroll=4)
 
     scan(0, False)
     scan(1, True)
@@ -439,7 +439,7 @@
         bcpad[pl.ds(at, BLOCK), :] = jnp.concatenate([d_k, d_r], axis=1) * kcs_s[b]
         return 0
 
-    lax.fori_loop(0, blocks, second, 0, unroll=2)
+    lax.fori_loop(0, blocks, second, 0, unroll=4)
 
     sums = nn(
         jnp.concatenate(split(row_s[0].reshape(all_rows, BLOCK), 3), axis=0),
@@ -459,7 +459,7 @@
         out_ref[b, BLOCK:, :] = pack_rows(row_s[0, b][:heads], width).astype(bf16)
         return 0
 
-    lax.fori_loop(0, blocks, last, 0)
+    lax.fori_loop(0, blocks, last, 0, unroll=2)
 
 
 def limit(mib):

time: 131 us -> 131 us (level)
  no operation moved by 1% of the time
where the time goes in v4:
time: 131 us
  waiting for transfers between devices  50.2 us (38%)
  starting transfers between devices  47.2 us (36%)
  Pallas kernels  29.7 us (23%)
  local copies, waits for them, and re-layouts  1.55 us (1%)
    ppermute x32, waiting for transfers between devices, swap(): return lax.ppermute(value, axis, [(i, i ^ bits) for i in range(size)])  50.2 us
    ppermute x32, starting transfers between devices, swap(): return lax.ppermute(value, axis, [(i, i ^ bits) for i in range(size)])  35.4 us
    pallas_call x1, Pallas kernels, run_mixer(): pl.pallas_call(functools.partial(mixer_kernel, len(bc)), out_shape=(jax.S...  12.7 us
    pallas_call x5, Pallas kernels, call(): pl.pallas_call(kernel, out_shape=outs, in_specs=specs, out_specs=jax.tree...  9.12 us
    all_to_all x1, starting transfers between devices, local(): heads_x = lax.all_to_all(packed, 'sp', 0, 0, tiled=True)  7.42 us
    all_to_all x1, starting transfers between devices, local(): back_x = lax.all_to_all(d_x, 'sp', 0, 0, tiled=True)  4.45 us
    pallas_call x1, Pallas kernels, local(): pl.pallas_call(prep_kernel, grid=(steps,), in_specs=[row_spec, row_spec,...  4.29 us
    pallas_call x1, Pallas kernels, run_enter(): pl.pallas_call(enter_kernel, out_shape=(shape((blocks, BLOCK, width), f32...  2.71 us
  transfers between devices with their start and end apart: 34, of which 9 were waited for; matrix products, arithmetic and copies ran while one was open for 2% of the time, Pallas kernels for 19%

profile of v4, /device:TPU:0, one launch (start us, length us, event | category | flops | bytes accessed | tf_op | source)
XLA Modules:
  0.0 130.7 jit_solution(15842661006072443242)
XLA Ops:
  0.6 4.3 %prep.1 = (bf16[8,264,256]{2,1,0:T(8,128)(2,1)}, bf16[128,2048]{1,0:T(8,128)(2,1)}) custom-call(bf16[128,2048]{1,0:T(8,128)(2,1)} %bitcast.39, bf16[128,2048]{1,0:T(8,128)(2,1)} %bitcast.40, bf16[128,2048]{1,0:T(8,128)(2,1)} %bitcast.41, f32[1,2048]{1,0:T(1,128)} %bitcast.44, bf16[128,2048]{1,0:T(8,128)(2,1)} %bitcast.42, bf16[32,128]{1,0:T(8,128)(2,1)} %bitcast.45), custom_call_target="tpu_custom_call" | custom-call | tf_op jit(solution)/shard_map/prep/pallas_call | solution.py:598
  4.9 7.4 %all-to-all-start = ((bf16[8,264,256]{2,1,0:T(8,128)(2,1)}), bf16[8,264,256]{2,1,0:T(8,128)(2,1)S(1)}, u32[]{:S(2)}, u32[]{:S(2)}) async-start(bf16[8,264,256]{2,1,0:T(8,128)(2,1)} %get-tuple-element.31), calls=%async_computation | async-start | bytes 2162688 | tf_op jit(solution)/shard_map/all_to_all | solution.py:626
  12.6 1.6 %collective-permute-start.3 = (bf16[512,512]{1,0:T(8,128)(2,1)S(1)}, bf16[512,512]{1,0:T(8,128)(2,1)S(1)}, u32[]{:S(2)}, u32[]{:S(2)}) collective-permute-start(bf16[512,512]{1,0:T(8,128)(2,1)S(1)} %pad_maximum_fusion.refs_0_), channel_id=1, source_target_pairs={{0,2},{1,3},{2,0},{3,1},{4,6},{5,7},{6,4},{7,5},{8,10},{9,11},{10,... | collective-permute-start | bytes 1572872 | tf_op jit(solution)/shard_map/ppermute | solution.py:532
  14.1 11.9 %collective-permute-done.3.refs_2_ = bf16[512,512]{1,0:T(8,128)(2,1)S(1)} collective-permute-done((bf16[512,512]{1,0:T(8,128)(2,1)S(1)}, bf16[512,512]{1,0:T(8,128)(2,1)S(1)}, u32[]{:S(2)}, u32[]{:S(2)}) %collective-permute-start.3) | collective-permute-done | bytes 524320 | tf_op jit(solution)/shard_map/ppermute | solution.py:532
  26.0 0.8 dynamic-slice_bitcast_fusion
  26.8 0.5 collective-permute-start
  27.3 1.5 %collective-permute-start.1 = (bf16[128,512]{1,0:T(8,128)(2,1)}, bf16[128,512]{1,0:T(8,128)(2,1)}, u32[]{:S(2)}, u32[]{:S(2)}) collective-permute-start(bf16[128,512]{1,0:T(8,128)(2,1)} %get-tuple-element.57), channel_id=1, source_target_pairs={{0,2},{1,3},{2,0},{3,1},{4,6},{5,7},{6,4},{7,5},{8,10},{9,11},{10,... | collective-permute-start | bytes 393224 | tf_op jit(solution)/shard_map/ppermute | solution.py:532
  28.9 1.5 %shard_map.200 = (bf16[128,256]{1,0:T(8,128)(2,1)S(1)}, bf16[128,256]{1,0:T(8,128)(2,1)S(1)}) custom-call(s32[4]{0:T(128)S(1)} %pad_add_fusion.at_ref, bf16[128,2048]{1,0:T(8,128)(2,1)S(1)} %bitcast.37, bf16[512,512]{1,0:T(8,128)(2,1)S(1)} %pad_maximum_fusion.refs_0_, bf16[512,512]{1,0:T(8,128)(2,1)S(1)} %collective-permute-done.2.refs_1_, ...), custom_call_target="tpu_custom_call" | custom-call | tf_op jit(solution)/shard_map/pallas_call | solution.py:537
  30.5 2.7 %collective-permute-start.8 = (bf16[128,256]{1,0:T(8,128)(2,1)S(1)}, bf16[128,256]{1,0:T(8,128)(2,1)S(1)}, u32[]{:S(2)}, u32[]{:S(2)}) collective-permute-start(bf16[128,256]{1,0:T(8,128)(2,1)S(1)} %get-tuple-element.40), channel_id=1, source_target_pairs={{0,16},{4,20},{8,24},{12,28},{16,0},{20,4},{24,8},{28,12},{1,17},{... | collective-permute-start | bytes 196616 | tf_op jit(solution)/shard_map/ppermute | solution.py:532
  33.2 1.5 %collective-permute-start.5 = (bf16[128,256]{1,0:T(8,128)(2,1)S(1)}, bf16[128,256]{1,0:T(8,128)(2,1)S(1)}, u32[]{:S(2)}, u32[]{:S(2)}) collective-permute-start(bf16[128,256]{1,0:T(8,128)(2,1)S(1)} %get-tuple-element.39.refs_10_), channel_id=1, source_target_pairs={{0,4},{4,0},{8,12},{12,8},{16,20},{20,16},{24,28},{28,24},{1,5},{5... | collective-permute-start | bytes 196616 | tf_op jit(solution)/shard_map/ppermute | solution.py:532
  34.6 1.5 %collective-permute-start.6 = (bf16[128,256]{1,0:T(8,128)(2,1)S(1)}, bf16[128,256]{1,0:T(8,128)(2,1)S(1)}, u32[]{:S(2)}, u32[]{:S(2)}) collective-permute-start(bf16[128,256]{1,0:T(8,128)(2,1)S(1)} %get-tuple-element.39.refs_10_), channel_id=1, source_target_pairs={{0,8},{4,12},{8,0},{12,4},{16,24},{20,28},{24,16},{28,20},{1,9},{5... | collective-permute-start | bytes 196616 | tf_op jit(solution)/shard_map/ppermute | solution.py:532
  36.1 0.6 collective-permute-start.7
  36.7 5.1 %collective-permute-done.8.refs_14_ = bf16[128,256]{1,0:T(8,128)(2,1)S(1)} collective-permute-done((bf16[128,256]{1,0:T(8,128)(2,1)S(1)}, bf16[128,256]{1,0:T(8,128)(2,1)S(1)}, u32[]{:S(2)}, u32[]{:S(2)}) %collective-permute-start.8) | collective-permute-done | bytes 65568 | tf_op jit(solution)/shard_map/ppermute | solution.py:532
  41.7 2.9 %collective-permute-start.11 = (bf16[128,256]{1,0:T(8,128)(2,1)S(1)}, bf16[128,256]{1,0:T(8,128)(2,1)S(1)}, u32[]{:S(2)}, u32[]{:S(2)}) collective-permute-start(bf16[128,256]{1,0:T(8,128)(2,1)S(1)} %collective-permute-done.8.refs_14_), channel_id=1, source_target_pairs={{0,12},{4,8},{8,4},{12,0},{16,28},{20,24},{24,20},{28,16},{1,13},{... | collective-permute-start | bytes 196616 | tf_op jit(solution)/shard_map/ppermute | solution.py:532
  44.6 0.6 collective-permute-start.9
  45.3 1.7 %shard_map.199 = (bf16[3,128,512]{2,1,0:T(8,128)(2,1)}, f32[4,1024]{1,0:T(4,128)S(1)}) custom-call(s32[4]{0:T(128)S(1)} %pad_add_fusion.at_ref, f32[4,1024]{1,0:T(4,128)S(1)} %bitcast.38, bf16[128,512]{1,0:T(8,128)(2,1)S(1)} %get-tuple-element.59.refs_0_.refs_4_, bf16[128,512]{1,0:T(8,128)(2,1)S(1)} %collective-permute-done.refs_1_.refs_5_, ...), custom_call_target="tpu_custom_call" | custom-call | tf_op jit(solution)/shard_map/pallas_call | solution.py:537
  47.0 2.7 %enter.1 = (f32[8,128,256]{2,1,0:T(8,128)S(1)}, f32[8,128,256]{2,1,0:T(8,128)S(1)}, f32[5,8,8,128]{3,2,1,0:T(8,128)S(1)}, f32[8,384,256]{2,1,0:T(8,128)S(1)}, bf...) custom-call(f32[3,4]{1,0:T(4,128)S(1)} %pad_maximum_fusion.1.head_ref, ...), custom_call_target="tpu_custom_call" | custom-call | tf_op jit(solution)/shard_map/enter/pallas_call | solution.py:480
  49.8 12.7 %mixer.1 = (bf16[8,136,256]{2,1,0:T(8,128)(2,1)}, bf16[2,128,256]{2,1,0:T(8,128)(2,1)S(1)}, bf16[2,128,256]{2,1,0:T(8,128)(2,1)}, bf16[2,128,256]{2,1,0:T(8,128)(2,1)}, bf16[2,128,256]{2,1,0:T(8,128)(2,1)}) custom-call(s32[4]{0:T(128)S(1)} %pad_add_fusion.at_ref, f32[3,4]{1,0:T(4,128)S(1)} %pad_maximum_fusion.1.head_ref, ...), custom_call_target="tpu_custom_call" | custom-call | tf_op jit(solution)/shard_map/mixer/pallas_call | solution.py:515
  62.6 0.6 copy-done.1
  63.2 1.4 %collective-permute-start.12 = (bf16[2,128,256]{2,1,0:T(8,128)(2,1)}, bf16[2,128,256]{2,1,0:T(8,128)(2,1)S(1)}, u32[]{:S(2)}, u32[]{:S(2)}) collective-permute-start(bf16[2,128,256]{2,1,0:T(8,128)(2,1)} %get-tuple-element.42), channel_id=1, source_target_pairs={{0,4},{4,0},{8,12},{12,8},{16,20},{20,16},{24,28},{28,24},{1,5},{5... | collective-permute-start | bytes 393224 | tf_op jit(solution)/shard_map/ppermute | solution.py:532
  64.7 2.0 %collective-permute-start.14 = (bf16[2,128,256]{2,1,0:T(8,128)(2,1)}, bf16[2,128,256]{2,1,0:T(8,128)(2,1)}, u32[]{:S(2)}, u32[]{:S(2)}) collective-permute-start(bf16[2,128,256]{2,1,0:T(8,128)(2,1)} %get-tuple-element.44), channel_id=1, source_target_pairs={{0,12},{4,8},{8,4},{12,0},{16,28},{20,24},{24,20},{28,16},{1,13},{... | collective-permute-start | bytes 393224 | tf_op jit(solution)/shard_map/ppermute | solution.py:532
  66.7 0.6 collective-permute-start.20
  67.3 4.5 %all-to-all-start.1 = ((bf16[8,136,256]{2,1,0:T(8,128)(2,1)}), bf16[8,136,256]{2,1,0:T(8,128)(2,1)S(1)}, u32[]{:S(2)}, u32[]{:S(2)}) async-start(bf16[8,136,256]{2,1,0:T(8,128)(2,1)} %get-tuple-element.45), calls=%async_computation.1 | async-start | bytes 1114112 | tf_op jit(solution)/shard_map/all_to_all | solution.py:653
  71.8 2.9 %collective-permute-start.21 = (bf16[128,512]{1,0:T(8,128)(2,1)S(1)}, bf16[128,512]{1,0:T(8,128)(2,1)S(1)}, u32[]{:S(2)}, u32[]{:S(2)}) collective-permute-start(bf16[128,512]{1,0:T(8,128)(2,1)S(1)} %collective-permute-done.19.refs_7_), channel_id=1, source_target_pairs={{0,16},{4,20},{8,24},{12,28},{16,0},{20,4},{24,8},{28,12},{1,17},{... | collective-permute-start | bytes 393224 | tf_op jit(solution)/shard_map/ppermute | solution.py:532
  74.7 1.2 collective-permute-done.14
  75.9 1.0 add_convert_fusion.refs_0_
  76.9 0.3 collective-permute-start.16
  77.2 1.5 %collective-permute-start.17 = (bf16[2,128,256]{2,1,0:T(8,128)(2,1)S(1)}, bf16[2,128,256]{2,1,0:T(8,128)(2,1)S(1)}, u32[]{:S(2)}, u32[]{:S(2)}) collective-permute-start(bf16[2,128,256]{2,1,0:T(8,128)(2,1)S(1)} %add_convert_fusion.refs_0_), channel_id=1, source_target_pairs={{0,2},{1,3},{2,0},{3,1},{4,6},{5,7},{6,4},{7,5},{8,10},{9,11},{10,... | collective-permute-start | bytes 393224 | tf_op jit(solution)/shard_map/ppermute | solution.py:532
  78.8 26.8 %collective-permute-done.21.refs_9_ = bf16[128,512]{1,0:T(8,128)(2,1)S(1)} collective-permute-done((bf16[128,512]{1,0:T(8,128)(2,1)S(1)}, bf16[128,512]{1,0:T(8,128)(2,1)S(1)}, u32[]{:S(2)}, u32[]{:S(2)}) %collective-permute-start.21) | collective-permute-done | bytes 131104 | tf_op jit(solution)/shard_map/ppermute | solution.py:532
  105.6 1.7 %shard_map.202 = (bf16[128,256]{1,0:T(8,128)(2,1)S(1)}, bf16[128,256]{1,0:T(8,128)(2,1)S(1)}, bf16[128,256]{1,0:T(8,128)(2,1)S(1)}, bf16[128,256]{1,0:T(8,128)(2,1)S(1)}) custom-call(s32[4]{0:T(128)S(1)} %pad_add_fusion.at_ref, bf16[2,128,256]{2,1,0:T(8,128)(2,1)S(1)} %add_convert_fusion.refs_0_, bf16[2,128,256]{2,1,0:T(8,128)(2,1)S(1)} %collective-permute-done.16.refs_1_, ...), custom_call_target="tpu_custom_call" | custom-call | tf_op jit(solution)/shard_map/pallas_call | solution.py:537
  107.3 1.5 %collective-permute-start.22 = (bf16[128,256]{1,0:T(8,128)(2,1)S(1)}, bf16[128,256]{1,0:T(8,128)(2,1)S(1)}, u32[]{:S(2)}, u32[]{:S(2)}) collective-permute-start(bf16[128,256]{1,0:T(8,128)(2,1)S(1)} %get-tuple-element.51), channel_id=1, source_target_pairs={{0,4},{4,0},{8,12},{12,8},{16,20},{20,16},{24,28},{28,24},{1,5},{5... | collective-permute-start | bytes 196616 | tf_op jit(solution)/shard_map/ppermute | solution.py:532
  108.8 2.1 %collective-permute-start.24 = (bf16[128,256]{1,0:T(8,128)(2,1)S(1)}, bf16[128,256]{1,0:T(8,128)(2,1)S(1)}, u32[]{:S(2)}, u32[]{:S(2)}) collective-permute-start(bf16[128,256]{1,0:T(8,128)(2,1)S(1)} %get-tuple-element.53), channel_id=1, source_target_pairs={{0,12},{4,8},{8,4},{12,0},{16,28},{20,24},{24,20},{28,16},{1,13},{... | collective-permute-start | bytes 196616 | tf_op jit(solution)/shard_map/ppermute | solution.py:532
  110.9 0.8 collective-permute-done.22
  111.7 1.5 %collective-permute-done.23 = bf16[128,256]{1,0:T(8,128)(2,1)S(1)} collective-permute-done((bf16[128,256]{1,0:T(8,128)(2,1)S(1)}, bf16[128,256]{1,0:T(8,128)(2,1)S(1)}, u32[]{:S(2)}, u32[]{:S(2)}) %collective-permute-start.23) | collective-permute-done | bytes 65568 | tf_op jit(solution)/shard_map/ppermute | solution.py:532
  113.1 0.9 collective-permute-done.24
  114.1 2.1 %collective-permute-start.28 = (bf16[128,256]{1,0:T(8,128)(2,1)S(1)}, bf16[128,256]{1,0:T(8,128)(2,1)S(1)}, u32[]{:S(2)}, u32[]{:S(2)}) collective-permute-start(bf16[128,256]{1,0:T(8,128)(2,1)S(1)} %add_convert_fusion.1.refs_0_), channel_id=1, source_target_pairs={{0,16},{4,20},{8,24},{12,28},{16,0},{20,4},{24,8},{28,12},{1,17},{... | collective-permute-start | bytes 196616 | tf_op jit(solution)/shard_map/ppermute | solution.py:532
  116.2 0.9 collective-permute-start.15
  117.1 1.3 collective-permute-start.25
  118.3 1.3 %collective-permute-start.26 = (bf16[128,256]{1,0:T(8,128)(2,1)S(1)}, bf16[128,256]{1,0:T(8,128)(2,1)S(1)}, u32[]{:S(2)}, u32[]{:S(2)}) collective-permute-start(bf16[128,256]{1,0:T(8,128)(2,1)S(1)} %add_convert_fusion.1.refs_0_), channel_id=1, source_target_pairs={{0,8},{4,12},{8,0},{12,4},{16,24},{20,28},{24,16},{28,20},{1,9},{5... | collective-permute-start | bytes 196616 | tf_op jit(solution)/shard_map/ppermute | solution.py:532
  119.6 0.9 collective-permute-start.27
  120.6 1.3 collective-permute-start.29
  121.8 0.7 collective-permute-done.15.other_ref
  122.5 0.6 collective-permute-start.30
  123.1 1.1 collective-permute-start.31
  124.3 2.6 %shard_map.201 = bf16[128,2048]{1,0:T(8,128)(2,1)} custom-call(s32[4]{0:T(128)S(1)} %pad_add_fusion.at_ref, bf16[128,256]{1,0:T(8,128)(2,1)S(1)} %get-tuple-element.65.own_ref, bf16[128,256]{1,0:T(8,128)(2,1)S(1)} %collective-permute-done.15.other_ref, bf16[512,512]{1,0:T(8,128)(2,1)S(1)} %pad_maximum_fusion.refs_0_, ...), custom_call_target="tpu_custom_call" | custom-call | tf_op jit(solution)/shard_map/pallas_call | solution.py:537
  127.0 1.3 %collective-permute-done.31.refs_7_ = bf16[128,256]{1,0:T(8,128)(2,1)S(1)} collective-permute-done((bf16[128,256]{1,0:T(8,128)(2,1)S(1)}, bf16[128,256]{1,0:T(8,128)(2,1)S(1)}, u32[]{:S(2)}, u32[]{:S(2)}) %collective-permute-start.31) | collective-permute-done | bytes 65568 | tf_op jit(solution)/shard_map/ppermute | solution.py:532
  128.3 1.6 %shard_map.203 = (f32[512,256]{1,0:T(8,128)}, f32[512,256]{1,0:T(8,128)}) custom-call(s32[4]{0:T(128)S(1)} %pad_add_fusion.at_ref, bf16[128,256]{1,0:T(8,128)(2,1)S(1)} %add_convert_fusion.1.refs_0_, bf16[128,256]{1,0:T(8,128)(2,1)S(1)} %collective-permute-done.25.refs_1_, bf16[128,256]{1,0:T(8,128)(2,1)S(1)} %collective-permute-done.26.refs_2_, ...), custom_call_target="tpu_custom_call" | custom-call | tf_op jit(solution)/shard_map/pallas_call | solution.py:537
  129.9 0.8 unpack.1
  (61 shorter events, 0.6 us)
Async XLA Ops:
  4.9 7.4 %copy-start.7 = (bf16[512,256]{1,0:T(8,128)(2,1)S(1)}, bf16[512,256]{1,0:T(8,128)(2,1)}, u32[]{:S(2)}) copy-start(bf16[512,256]{1,0:T(8,128)(2,1)} %param.17) | copy-start | bytes 786436
  4.9 7.4 %copy-start.8 = (bf16[512,256]{1,0:T(8,128)(2,1)S(1)}, bf16[512,256]{1,0:T(8,128)(2,1)}, u32[]{:S(2)}) copy-start(bf16[512,256]{1,0:T(8,128)(2,1)} %param.18) | copy-start | bytes 786436
  4.9 42.0 %all-to-all-start = ((bf16[8,264,256]{2,1,0:T(8,128)(2,1)}), bf16[8,264,256]{2,1,0:T(8,128)(2,1)S(1)}, u32[]{:S(2)}, u32[]{:S(2)}) async-start(bf16[8,264,256]{2,1,0:T(8,128)(2,1)} %get-tuple-element.31), calls=%async_computation | async-start | bytes 2162688 | tf_op jit(solution)/shard_map/all_to_all | solution.py:626
  12.4 13.6 %copy-start = (bf16[1,128,2048]{2,1,0:T(8,128)(2,1)S(1)}, bf16[1,128,2048]{2,1,0:T(8,128)(2,1)}, u32[]{:S(2)}) copy-start(bf16[1,128,2048]{2,1,0:T(8,128)(2,1)} %param.16) | copy-start | bytes 1572868
  12.6 13.4 %collective-permute-start.3 = (bf16[512,512]{1,0:T(8,128)(2,1)S(1)}, bf16[512,512]{1,0:T(8,128)(2,1)S(1)}, u32[]{:S(2)}, u32[]{:S(2)}) collective-permute-start(bf16[512,512]{1,0:T(8,128)(2,1)S(1)} %pad_maximum_fusion.refs_0_), channel_id=1, source_target_pairs={{0,2},{1,3},{2,0},{3,1},{4,6},{5,7},{6,4},{7,5},{8,10},{9,11},{10,... | collective-permute-start | bytes 1572872 | tf_op jit(solution)/shard_map/ppermute | solution.py:532
  14.1 14.7 %collective-permute-start.2 = (bf16[512,512]{1,0:T(8,128)(2,1)S(1)}, bf16[512,512]{1,0:T(8,128)(2,1)S(1)}, u32[]{:S(2)}, u32[]{:S(2)}) collective-permute-start(bf16[512,512]{1,0:T(8,128)(2,1)S(1)} %pad_maximum_fusion.refs_0_), channel_id=1, source_target_pairs={{0,1},{1,0},{2,3},{3,2},{4,5},{5,4},{6,7},{7,6},{8,9},{9,8},{10,11... | collective-permute-start | bytes 1572872 | tf_op jit(solution)/shard_map/ppermute | solution.py:532
  26.0 2.9 %collective-permute-start.4 = (bf16[512,512]{1,0:T(8,128)(2,1)S(1)}, bf16[512,512]{1,0:T(8,128)(2,1)}, u32[]{:S(2)}, u32[]{:S(2)}) collective-permute-start(bf16[512,512]{1,0:T(8,128)(2,1)S(1)} %collective-permute-done.3.refs_2_), channel_id=1, source_target_pairs={{0,1},{1,0},{2,3},{3,2},{4,5},{5,4},{6,7},{7,6},{8,9},{9,8},{10,11... | collective-permute-start | bytes 1572872 | tf_op jit(solution)/shard_map/ppermute | solution.py:532
  26.8 9.3 %collective-permute-start = (bf16[128,512]{1,0:T(8,128)(2,1)}, bf16[128,512]{1,0:T(8,128)(2,1)S(1)}, u32[]{:S(2)}, u32[]{:S(2)}) collective-permute-start(bf16[128,512]{1,0:T(8,128)(2,1)} %get-tuple-element.58), channel_id=1, source_target_pairs={{0,1},{1,0},{2,3},{3,2},{4,5},{5,4},{6,7},{7,6},{8,9},{9,8},{10,11... | collective-permute-start | bytes 393224 | tf_op jit(solution)/shard_map/ppermute | solution.py:532
  27.3 14.5 %collective-permute-start.1 = (bf16[128,512]{1,0:T(8,128)(2,1)}, bf16[128,512]{1,0:T(8,128)(2,1)}, u32[]{:S(2)}, u32[]{:S(2)}) collective-permute-start(bf16[128,512]{1,0:T(8,128)(2,1)} %get-tuple-element.57), channel_id=1, source_target_pairs={{0,2},{1,3},{2,0},{3,1},{4,6},{5,7},{6,4},{7,5},{8,10},{9,11},{10,... | collective-permute-start | bytes 393224 | tf_op jit(solution)/shard_map/ppermute | solution.py:532
  28.9 16.4 %copy-start.9 = (f32[4]{0:T(128)S(1)}, f32[4]{0:T(128)}, u32[]{:S(2)}) copy-start(f32[4]{0:T(128)} %param.30) | copy-start | bytes 52
  28.9 16.4 %copy-start.10 = (f32[4]{0:T(128)S(1)}, f32[4]{0:T(128)}, u32[]{:S(2)}) copy-start(f32[4]{0:T(128)} %param.29) | copy-start | bytes 52
  28.9 16.4 %copy-start.11 = (f32[4]{0:T(128)S(1)}, f32[4]{0:T(128)}, u32[]{:S(2)}) copy-start(f32[4]{0:T(128)} %param.28) | copy-start | bytes 52
  28.9 16.4 %copy-start.4 = (f32[1,1024,4]{1,2,0:T(4,128)S(1)}, f32[1,1024,4]{1,2,0:T(4,128)}, u32[]{:S(2)}) copy-start(f32[1,1024,4]{1,2,0:T(4,128)} %param.24) | copy-start | bytes 49156
  28.9 18.0 %copy-start.3 = (f32[5,256]{1,0:T(8,128)S(1)}, f32[5,256]{1,0:T(8,128)}, u32[]{:S(2)}) copy-start(f32[5,256]{1,0:T(8,128)} %refs_7_.1) | copy-start | bytes 15364
  30.5 19.4 %copy-start.5 = (f32[5,256]{1,0:T(8,128)S(1)}, f32[5,256]{1,0:T(8,128)}, u32[]{:S(2)}) copy-start(f32[5,256]{1,0:T(8,128)} %refs_8_.1) | copy-start | bytes 15364
  30.5 19.4 %copy-start.6 = (f32[5,256]{1,0:T(8,128)S(1)}, f32[5,256]{1,0:T(8,128)}, u32[]{:S(2)}) copy-start(f32[5,256]{1,0:T(8,128)} %refs_9_.1) | copy-start | bytes 15364
  30.5 11.3 %collective-permute-start.8 = (bf16[128,256]{1,0:T(8,128)(2,1)S(1)}, bf16[128,256]{1,0:T(8,128)(2,1)S(1)}, u32[]{:S(2)}, u32[]{:S(2)}) collective-permute-start(bf16[128,256]{1,0:T(8,128)(2,1)S(1)} %get-tuple-element.40), channel_id=1, source_target_pairs={{0,16},{4,20},{8,24},{12,28},{16,0},{20,4},{24,8},{28,12},{1,17},{... | collective-permute-start | bytes 196616 | tf_op jit(solution)/shard_map/ppermute | solution.py:532
  33.2 11.4 %collective-permute-start.5 = (bf16[128,256]{1,0:T(8,128)(2,1)S(1)}, bf16[128,256]{1,0:T(8,128)(2,1)S(1)}, u32[]{:S(2)}, u32[]{:S(2)}) collective-permute-start(bf16[128,256]{1,0:T(8,128)(2,1)S(1)} %get-tuple-element.39.refs_10_), channel_id=1, source_target_pairs={{0,4},{4,0},{8,12},{12,8},{16,20},{20,16},{24,28},{28,24},{1,5},{5... | collective-permute-start | bytes 196616 | tf_op jit(solution)/shard_map/ppermute | solution.py:532
  34.6 15.0 %collective-permute-start.6 = (bf16[128,256]{1,0:T(8,128)(2,1)S(1)}, bf16[128,256]{1,0:T(8,128)(2,1)S(1)}, u32[]{:S(2)}, u32[]{:S(2)}) collective-permute-start(bf16[128,256]{1,0:T(8,128)(2,1)S(1)} %get-tuple-element.39.refs_10_), channel_id=1, source_target_pairs={{0,8},{4,12},{8,0},{12,4},{16,24},{20,28},{24,16},{28,20},{1,9},{5... | collective-permute-start | bytes 196616 | tf_op jit(solution)/shard_map/ppermute | solution.py:532
  36.1 13.7 %collective-permute-start.7 = (bf16[128,256]{1,0:T(8,128)(2,1)S(1)}, bf16[128,256]{1,0:T(8,128)(2,1)S(1)}, u32[]{:S(2)}, u32[]{:S(2)}) collective-permute-start(bf16[128,256]{1,0:T(8,128)(2,1)S(1)} %get-tuple-element.39.refs_10_), channel_id=1, source_target_pairs={{0,12},{4,8},{8,4},{12,0},{16,28},{20,24},{24,20},{28,16},{1,13},{... | collective-permute-start | bytes 196616 | tf_op jit(solution)/shard_map/ppermute | solution.py:532
  41.7 8.0 %collective-permute-start.10 = (bf16[128,256]{1,0:T(8,128)(2,1)S(1)}, bf16[128,256]{1,0:T(8,128)(2,1)S(1)}, u32[]{:S(2)}, u32[]{:S(2)}) collective-permute-start(bf16[128,256]{1,0:T(8,128)(2,1)S(1)} %collective-permute-done.8.refs_14_), channel_id=1, source_target_pairs={{0,8},{4,12},{8,0},{12,4},{16,24},{20,28},{24,16},{28,20},{1,9},{5... | collective-permute-start | bytes 196616 | tf_op jit(solution)/shard_map/ppermute | solution.py:532
  41.7 8.1 %collective-permute-start.11 = (bf16[128,256]{1,0:T(8,128)(2,1)S(1)}, bf16[128,256]{1,0:T(8,128)(2,1)S(1)}, u32[]{:S(2)}, u32[]{:S(2)}) collective-permute-start(bf16[128,256]{1,0:T(8,128)(2,1)S(1)} %collective-permute-done.8.refs_14_), channel_id=1, source_target_pairs={{0,12},{4,8},{8,4},{12,0},{16,28},{20,24},{24,20},{28,16},{1,13},{... | collective-permute-start | bytes 196616 | tf_op jit(solution)/shard_map/ppermute | solution.py:532
  44.6 5.2 %collective-permute-start.9 = (bf16[128,256]{1,0:T(8,128)(2,1)S(1)}, bf16[128,256]{1,0:T(8,128)(2,1)}, u32[]{:S(2)}, u32[]{:S(2)}) collective-permute-start(bf16[128,256]{1,0:T(8,128)(2,1)S(1)} %collective-permute-done.8.refs_14_), channel_id=1, source_target_pairs={{0,4},{4,0},{8,12},{12,8},{16,20},{20,16},{24,28},{28,24},{1,5},{5... | collective-permute-start | bytes 196616 | tf_op jit(solution)/shard_map/ppermute | solution.py:532
  49.7 22.1 %collective-permute-start.19 = (bf16[128,512]{1,0:T(8,128)(2,1)}, bf16[128,512]{1,0:T(8,128)(2,1)S(1)}, u32[]{:S(2)}, u32[]{:S(2)}) collective-permute-start(bf16[128,512]{1,0:T(8,128)(2,1)} %get-tuple-element.56), channel_id=1, source_target_pairs={{0,3},{1,2},{2,1},{3,0},{4,7},{5,6},{6,5},{7,4},{8,11},{9,10},{10,... | collective-permute-start | bytes 393224 | tf_op jit(solution)/shard_map/ppermute | solution.py:532
  62.5 0.6 copy-start.1
  63.2 12.7 %copy-start.2 = (bf16[2,128,256]{2,1,0:T(8,128)(2,1)S(1)}, bf16[2,128,256]{2,1,0:T(8,128)(2,1)}, u32[]{:S(2)}) copy-start(bf16[2,128,256]{2,1,0:T(8,128)(2,1)} %copy-done.1) | copy-start | bytes 393220
  63.2 11.5 %collective-permute-start.12 = (bf16[2,128,256]{2,1,0:T(8,128)(2,1)}, bf16[2,128,256]{2,1,0:T(8,128)(2,1)S(1)}, u32[]{:S(2)}, u32[]{:S(2)}) collective-permute-start(bf16[2,128,256]{2,1,0:T(8,128)(2,1)} %get-tuple-element.42), channel_id=1, source_target_pairs={{0,4},{4,0},{8,12},{12,8},{16,20},{20,16},{24,28},{28,24},{1,5},{5... | collective-permute-start | bytes 393224 | tf_op jit(solution)/shard_map/ppermute | solution.py:532
  64.6 10.1 %collective-permute-start.13 = (bf16[2,128,256]{2,1,0:T(8,128)(2,1)}, bf16[2,128,256]{2,1,0:T(8,128)(2,1)S(1)}, u32[]{:S(2)}, u32[]{:S(2)}) collective-permute-start(bf16[2,128,256]{2,1,0:T(8,128)(2,1)} %get-tuple-element.43), channel_id=1, source_target_pairs={{0,8},{4,12},{8,0},{12,4},{16,24},{20,28},{24,16},{28,20},{1,9},{5... | collective-permute-start | bytes 393224 | tf_op jit(solution)/shard_map/ppermute | solution.py:532
  64.7 11.2 %collective-permute-start.14 = (bf16[2,128,256]{2,1,0:T(8,128)(2,1)}, bf16[2,128,256]{2,1,0:T(8,128)(2,1)}, u32[]{:S(2)}, u32[]{:S(2)}) collective-permute-start(bf16[2,128,256]{2,1,0:T(8,128)(2,1)} %get-tuple-element.44), channel_id=1, source_target_pairs={{0,12},{4,8},{8,4},{12,0},{16,28},{20,24},{24,20},{28,16},{1,13},{... | collective-permute-start | bytes 393224 | tf_op jit(solution)/shard_map/ppermute | solution.py:532
  66.7 38.9 %collective-permute-start.20 = (bf16[3,128,512]{2,1,0:T(8,128)(2,1)}, bf16[3,128,512]{2,1,0:T(8,128)(2,1)S(1)}, u32[]{:S(2)}, u32[]{:S(2)}) collective-permute-start(bf16[3,128,512]{2,1,0:T(8,128)(2,1)} %get-tuple-element.49), channel_id=1, source_target_pairs={{0,16},{4,20},{8,24},{12,28},{16,0},{20,4},{24,8},{28,12},{1,17},{... | collective-permute-start | bytes 1179656 | tf_op jit(solution)/shard_map/ppermute | solution.py:532
  67.3 62.6 %all-to-all-start.1 = ((bf16[8,136,256]{2,1,0:T(8,128)(2,1)}), bf16[8,136,256]{2,1,0:T(8,128)(2,1)S(1)}, u32[]{:S(2)}, u32[]{:S(2)}) async-start(bf16[8,136,256]{2,1,0:T(8,128)(2,1)} %get-tuple-element.45), calls=%async_computation.1 | async-start | bytes 1114112 | tf_op jit(solution)/shard_map/all_to_all | solution.py:653
  71.8 33.9 %collective-permute-start.21 = (bf16[128,512]{1,0:T(8,128)(2,1)S(1)}, bf16[128,512]{1,0:T(8,128)(2,1)S(1)}, u32[]{:S(2)}, u32[]{:S(2)}) collective-permute-start(bf16[128,512]{1,0:T(8,128)(2,1)S(1)} %collective-permute-done.19.refs_7_), channel_id=1, source_target_pairs={{0,16},{4,20},{8,24},{12,28},{16,0},{20,4},{24,8},{28,12},{1,17},{... | collective-permute-start | bytes 393224 | tf_op jit(solution)/shard_map/ppermute | solution.py:532
  76.9 28.8 %collective-permute-start.16 = (bf16[2,128,256]{2,1,0:T(8,128)(2,1)S(1)}, bf16[2,128,256]{2,1,0:T(8,128)(2,1)S(1)}, u32[]{:S(2)}, u32[]{:S(2)}) collective-permute-start(bf16[2,128,256]{2,1,0:T(8,128)(2,1)S(1)} %add_convert_fusion.refs_0_), channel_id=1, source_target_pairs={{0,1},{1,0},{2,3},{3,2},{4,5},{5,4},{6,7},{7,6},{8,9},{9,8},{10,11... | collective-permute-start | bytes 393224 | tf_op jit(solution)/shard_map/ppermute | solution.py:532
  77.2 28.4 %collective-permute-start.17 = (bf16[2,128,256]{2,1,0:T(8,128)(2,1)S(1)}, bf16[2,128,256]{2,1,0:T(8,128)(2,1)S(1)}, u32[]{:S(2)}, u32[]{:S(2)}) collective-permute-start(bf16[2,128,256]{2,1,0:T(8,128)(2,1)S(1)} %add_convert_fusion.refs_0_), channel_id=1, source_target_pairs={{0,2},{1,3},{2,0},{3,1},{4,6},{5,7},{6,4},{7,5},{8,10},{9,11},{10,... | collective-permute-start | bytes 393224 | tf_op jit(solution)/shard_map/ppermute | solution.py:532
  78.7 26.9 %collective-permute-start.18 = (bf16[2,128,256]{2,1,0:T(8,128)(2,1)S(1)}, bf16[2,128,256]{2,1,0:T(8,128)(2,1)S(1)}, u32[]{:S(2)}, u32[]{:S(2)}) collective-permute-start(bf16[2,128,256]{2,1,0:T(8,128)(2,1)S(1)} %add_convert_fusion.refs_0_), channel_id=1, source_target_pairs={{0,3},{1,2},{2,1},{3,0},{4,7},{5,6},{6,5},{7,4},{8,11},{9,10},{10,... | collective-permute-start | bytes 393224 | tf_op jit(solution)/shard_map/ppermute | solution.py:532
  107.3 4.3 %collective-permute-start.22 = (bf16[128,256]{1,0:T(8,128)(2,1)S(1)}, bf16[128,256]{1,0:T(8,128)(2,1)S(1)}, u32[]{:S(2)}, u32[]{:S(2)}) collective-permute-start(bf16[128,256]{1,0:T(8,128)(2,1)S(1)} %get-tuple-element.51), channel_id=1, source_target_pairs={{0,4},{4,0},{8,12},{12,8},{16,20},{20,16},{24,28},{28,24},{1,5},{5... | collective-permute-start | bytes 196616 | tf_op jit(solution)/shard_map/ppermute | solution.py:532
  108.8 4.3 %collective-permute-start.23 = (bf16[128,256]{1,0:T(8,128)(2,1)S(1)}, bf16[128,256]{1,0:T(8,128)(2,1)S(1)}, u32[]{:S(2)}, u32[]{:S(2)}) collective-permute-start(bf16[128,256]{1,0:T(8,128)(2,1)S(1)} %get-tuple-element.52), channel_id=1, source_target_pairs={{0,8},{4,12},{8,0},{12,4},{16,24},{20,28},{24,16},{28,20},{1,9},{5... | collective-permute-start | bytes 196616 | tf_op jit(solution)/shard_map/ppermute | solution.py:532
  108.8 5.2 %collective-permute-start.24 = (bf16[128,256]{1,0:T(8,128)(2,1)S(1)}, bf16[128,256]{1,0:T(8,128)(2,1)S(1)}, u32[]{:S(2)}, u32[]{:S(2)}) collective-permute-start(bf16[128,256]{1,0:T(8,128)(2,1)S(1)} %get-tuple-element.53), channel_id=1, source_target_pairs={{0,12},{4,8},{8,4},{12,0},{16,28},{20,24},{24,20},{28,16},{1,13},{... | collective-permute-start | bytes 196616 | tf_op jit(solution)/shard_map/ppermute | solution.py:532
  114.1 6.5 %collective-permute-start.28 = (bf16[128,256]{1,0:T(8,128)(2,1)S(1)}, bf16[128,256]{1,0:T(8,128)(2,1)S(1)}, u32[]{:S(2)}, u32[]{:S(2)}) collective-permute-start(bf16[128,256]{1,0:T(8,128)(2,1)S(1)} %add_convert_fusion.1.refs_0_), channel_id=1, source_target_pairs={{0,16},{4,20},{8,24},{12,28},{16,0},{20,4},{24,8},{28,12},{1,17},{... | collective-permute-start | bytes 196616 | tf_op jit(solution)/shard_map/ppermute | solution.py:532
  116.2 6.4 %collective-permute-start.15 = (bf16[128,256]{1,0:T(8,128)(2,1)S(1)}, bf16[128,256]{1,0:T(8,128)(2,1)S(1)}, u32[]{:S(2)}, u32[]{:S(2)}) collective-permute-start(bf16[128,256]{1,0:T(8,128)(2,1)S(1)} %get-tuple-element.64), channel_id=1, source_target_pairs={{0,16},{4,20},{8,24},{12,28},{16,0},{20,4},{24,8},{28,12},{1,17},{... | collective-permute-start | bytes 196616 | tf_op jit(solution)/shard_map/ppermute | solution.py:532
  117.1 6.1 %collective-permute-start.25 = (bf16[128,256]{1,0:T(8,128)(2,1)S(1)}, bf16[128,256]{1,0:T(8,128)(2,1)S(1)}, u32[]{:S(2)}, u32[]{:S(2)}) collective-permute-start(bf16[128,256]{1,0:T(8,128)(2,1)S(1)} %add_convert_fusion.1.refs_0_), channel_id=1, source_target_pairs={{0,4},{4,0},{8,12},{12,8},{16,20},{20,16},{24,28},{28,24},{1,5},{5... | collective-permute-start | bytes 196616 | tf_op jit(solution)/shard_map/ppermute | solution.py:532
  118.3 8.6 %collective-permute-start.26 = (bf16[128,256]{1,0:T(8,128)(2,1)S(1)}, bf16[128,256]{1,0:T(8,128)(2,1)S(1)}, u32[]{:S(2)}, u32[]{:S(2)}) collective-permute-start(bf16[128,256]{1,0:T(8,128)(2,1)S(1)} %add_convert_fusion.1.refs_0_), channel_id=1, source_target_pairs={{0,8},{4,12},{8,0},{12,4},{16,24},{20,28},{24,16},{28,20},{1,9},{5... | collective-permute-start | bytes 196616 | tf_op jit(solution)/shard_map/ppermute | solution.py:532
  119.6 7.3 %collective-permute-start.27 = (bf16[128,256]{1,0:T(8,128)(2,1)S(1)}, bf16[128,256]{1,0:T(8,128)(2,1)S(1)}, u32[]{:S(2)}, u32[]{:S(2)}) collective-permute-start(bf16[128,256]{1,0:T(8,128)(2,1)S(1)} %add_convert_fusion.1.refs_0_), channel_id=1, source_target_pairs={{0,12},{4,8},{8,4},{12,0},{16,28},{20,24},{24,20},{28,16},{1,13},{... | collective-permute-start | bytes 196616 | tf_op jit(solution)/shard_map/ppermute | solution.py:532
  120.6 6.4 %collective-permute-start.29 = (bf16[128,256]{1,0:T(8,128)(2,1)S(1)}, bf16[128,256]{1,0:T(8,128)(2,1)S(1)}, u32[]{:S(2)}, u32[]{:S(2)}) collective-permute-start(bf16[128,256]{1,0:T(8,128)(2,1)S(1)} %collective-permute-done.28.refs_4_), channel_id=1, source_target_pairs={{0,4},{4,0},{8,12},{12,8},{16,20},{20,16},{24,28},{28,24},{1,5},{5... | collective-permute-start | bytes 196616 | tf_op jit(solution)/shard_map/ppermute | solution.py:532
  122.5 4.4 %collective-permute-start.30 = (bf16[128,256]{1,0:T(8,128)(2,1)S(1)}, bf16[128,256]{1,0:T(8,128)(2,1)S(1)}, u32[]{:S(2)}, u32[]{:S(2)}) collective-permute-start(bf16[128,256]{1,0:T(8,128)(2,1)S(1)} %collective-permute-done.28.refs_4_), channel_id=1, source_target_pairs={{0,8},{4,12},{8,0},{12,4},{16,24},{20,28},{24,16},{28,20},{1,9},{5... | collective-permute-start | bytes 196616 | tf_op jit(solution)/shard_map/ppermute | solution.py:532
  123.1 5.2 %collective-permute-start.31 = (bf16[128,256]{1,0:T(8,128)(2,1)S(1)}, bf16[128,256]{1,0:T(8,128)(2,1)S(1)}, u32[]{:S(2)}, u32[]{:S(2)}) collective-permute-start(bf16[128,256]{1,0:T(8,128)(2,1)S(1)} %collective-permute-done.28.refs_4_), channel_id=1, source_target_pairs={{0,12},{4,8},{8,4},{12,0},{16,28},{20,24},{24,20},{28,16},{1,13},{... | collective-permute-start | bytes 196616 | tf_op jit(solution)/shard_map/ppermute | solution.py:532
